TPU v7x, 128 devices: a whole 4x4x4 slice. The times are simulated.
128 devices in a mesh: sp: 32 (over z, y, core), tp: 4 (over x).
Axes of the slice: x: 4, y: 4, z: 4, core: 2. Of those that a mesh axis runs over, the one named last changes fastest.
Arguments:
- queries: bfloat16 [32768, 1024], P('sp', 'tp'), may hold values from -6 to 6
- keys: bfloat16 [32768, 1024], P('sp', 'tp'), may hold values from -6 to 6
- values: bfloat16 [32768, 1024], P('sp', 'tp'), may hold values from -6 to 6
- gates: bfloat16 [32768, 1024], P('sp', 'tp'), may hold values from -6 to 6
- log_decay: float32 [32768, 8], P('sp', 'tp'), may hold values from -1.6 to 0, as said below
- norm_gain: float32 [8, 128], P('tp'), may hold values from 0.1 to 1.9
- out_weight: bfloat16 [1024, 2048], P('tp'), may hold values from -0.1875 to 0.1875
- resid: bfloat16 [32768, 2048], P(('sp', 'tp')), may hold values from -6 to 6
- post_mix_gain: float32 [2048], replicated, may hold values from 0.1 to 1.9
- pre_ffn_gain: float32 [2048], replicated, may hold values from 0.1 to 1.9
- w_gate: bfloat16 [2048, 5632], P('sp', 'tp'), may hold values from -0.125 to 0.125
- w_up: bfloat16 [2048, 5632], P('sp', 'tp'), may hold values from -0.125 to 0.125
- w_down: bfloat16 [5632, 2048], P('tp', 'sp'), may hold values from -0.078125 to 0.078125
- post_ffn_gain: float32 [2048], replicated, may hold values from 0.1 to 1.9
Outputs:
- updated: bfloat16 [32768, 2048], P(('sp', 'tp'))
Inputs may be any that keep to these rules, and one draw needn't show every extreme that they name: `log_decay`: every entry is negative.
All inputs are finite; a program needn't handle non-finite values.
Results may differ from a plain program's by a relative error of at most 0.02.
Values may be sent and summed in bfloat16 or wider, within the bound.
No kernel may reach another device: no remote copies, remote signals or barrier semaphores. Data moves between devices by JAX's collectives and lax.ppermute only.
A program may use at most 128 MiB of HBM per device.

v0:
```python
import functools

import jax
import jax.numpy as jnp
from jax import lax
from jax.experimental import pallas as pl
from jax.experimental.pallas import tpu as pltpu
from jax.sharding import Mesh
from jax.sharding import PartitionSpec as P


BLOCK = 512
SP = ("sp_0", "sp_1", "sp_2")
SP_TP = ("sp_0", "sp_1", "sp_2", "tp")
RING = 4
EPSILON = 1e-06


def along(step):
    return [(i, (i + step) % RING) for i in range(RING)]


def role_shift(first, step):
    pairs = []
    for z in range(RING):
        for y in range(RING):
            for c in range(2):
                if (c == 0) == first:
                    to = (z, (y + step) % RING)
                else:
                    to = ((z + step) % RING, y)
                pairs.append((z * 8 + y * 2 + c, to[0] * 8 + to[1] * 2 + c))
    return pairs


def flipped(size, bit):
    return [(i, i ^ bit) for i in range(size)]


def gather_weights(w_gate, w_up, w_down):
    mine = jnp.stack([w_gate, w_up, w_down.T])
    near = functools.partial(role_shift, True)
    wide = functools.partial(role_shift, False)
    right = lax.ppermute(mine, SP, near(1))
    left = lax.ppermute(mine, SP, near(-1))
    far = lax.ppermute(mine, SP, near(2))
    s0 = jnp.stack([mine, right])
    s1 = jnp.stack([left, far])
    ra = lax.ppermute(s0, SP, wide(1))
    lb = lax.ppermute(s1, SP, wide(-1))
    fa = lax.ppermute(ra, SP, wide(1))
    fb = lax.ppermute(lb, SP, wide(-1))
    rb = lax.ppermute(s1, SP, wide(1))
    la = lax.ppermute(s0, SP, wide(-1))
    own = [s0, s1, ra, lb, fa, fb, rb, la]
    return own + [lax.ppermute(v, "sp_2", flipped(2, 1)) for v in own]


PIECES = ((0, 0), (2, 0), (0, 3), (2, 1), (0, 2), (2, 2), (2, 3), (0, 1))


def ffn_body(n_in, n_out, coord, *refs):
    xs = refs[:n_in]
    count = 2 * len(PIECES)
    pieces = refs[n_in : n_in + count]
    outs = refs[n_in + count : n_in + count + n_out]
    w, x, gate, up, hid, sem_gu, sem_d = refs[n_in + count + n_out :]
    z, y, c = coord[0], coord[1], coord[2]
    offs = (0, RING - 1, 1, 2)

    def plan(low):
        items = []
        for side in range(2):
            core = side if low else 1 - side
            for i, (first, away) in enumerate(PIECES):
                for k in range(2):
                    near = offs[first + k]
                    dz, dy = (away, near) if core == 0 else (near, away)
                    chip = ((z + dz) % RING) * RING + (y + dy) % RING
                    items.append((dz, pieces[side * len(PIECES) + i], k, core, chip))
        return [item[1:] for item in sorted(items, key=lambda item: item[0])]

    def gu_copy(src, k, core, chip):
        return pltpu.make_async_copy(
            src.at[k, pl.ds(0, 2)], w.at[pl.ds(0, 2), chip, core], sem_gu.at[core, chip]
        )

    def d_copy(src, k, core, chip):
        return pltpu.make_async_copy(src.at[k, 2], w.at[2, chip, core], sem_d.at[core, chip])

    for low in (True, False):

        @pl.when((c == 0) == low)
        def _():
            items = plan(low)
            for item in items:
                gu_copy(*item).start()
            for item in items:
                d_copy(*item).start()

    rows = x.shape[0]
    per = rows // n_in
    for i in range(n_in):
        x[i * per : (i + 1) * per, :] = xs[i][...]
    gate[...] = jnp.zeros_like(gate)
    up[...] = jnp.zeros_like(up)
    depth = 512
    width = gate.shape[1]

    def load(which, k):
        return w[which, pl.ds(4 * k, 4)].reshape(depth, width)

    def enter(step, carry):
        k = (z + step) % RING
        for core in range(2):
            for j in range(4):
                gu_copy(pieces[0], 0, core, 4 * k + j).wait()
        xk = x[:, pl.ds(pl.multiple_of(k * depth, depth), depth)]
        gate[...] += jnp.dot(xk, load(0, k), preferred_element_type=jnp.float32)
        up[...] += jnp.dot(xk, load(1, k), preferred_element_type=jnp.float32)
        return carry

    lax.fori_loop(0, RING, enter, 0)
    g = gate[...]
    hid[...] = (g * (1.0 / (1.0 + jnp.exp(-g))) * up[...]).astype(jnp.bfloat16)
    per_out = rows // n_out

    def leave(step, carry):
        k = (z + step) % RING
        for core in range(2):
            for j in range(4):
                d_copy(pieces[0], 0, core, 4 * k + j).wait()
        part = lax.dot_general(
            hid[...], load(2, k), (((1,), (1,)), ((), ())), preferred_element_type=jnp.float32
        ).astype(jnp.bfloat16)
        for i in range(n_out):
            outs[i][:, pl.ds(pl.multiple_of(k * depth, depth), depth)] = part[
                i * per_out : (i + 1) * per_out
            ]
        return carry

    lax.fori_loop(0, RING, leave, 0)


def ffn(coord, weights, xs, n_out):
    rows = sum(v.shape[0] for v in xs)
    model = xs[0].shape[1]
    width = weights[0].shape[-1]
    vm = pl.BlockSpec(memory_space=pltpu.VMEM)
    hb = pl.BlockSpec(memory_space=pltpu.HBM)
    flops = 6 * rows * model * width
    return pl.pallas_call(
        functools.partial(ffn_body, len(xs), n_out),
        out_shape=[jax.ShapeDtypeStruct((rows // n_out, model), jnp.bfloat16)] * n_out,
        in_specs=[pl.BlockSpec(memory_space=pltpu.SMEM)] + [vm] * len(xs) + [hb] * len(weights),
        out_specs=[vm] * n_out,
        scratch_shapes=[
            pltpu.VMEM((3, 16, 2, 64, width), jnp.bfloat16),
            pltpu.VMEM((rows, model), jnp.bfloat16),
            pltpu.VMEM((rows, width), jnp.float32),
            pltpu.VMEM((rows, width), jnp.float32),
            pltpu.VMEM((rows, width), jnp.bfloat16),
            pltpu.SemaphoreType.DMA((2, 16)),
            pltpu.SemaphoreType.DMA((2, 16)),
        ],
        compiler_params=pltpu.CompilerParams(vmem_limit_bytes=48 * 1024 * 1024),
        cost_estimate=pl.CostEstimate(
            flops=flops, bytes_accessed=6 * model * width, transcendentals=rows * width
        ),
        name="ffn_rows",
    )(coord, *xs, *weights)


def summed_decay(ld, scratch, span):
    scratch[...] = jnp.zeros_like(scratch)
    scratch[0:2, :] = ld[...]
    v = scratch[0:8, :]
    lane = lax.broadcasted_iota(jnp.int32, v.shape, 1) % span
    step = 1
    while step < span:
        v = v + jnp.where(lane >= step, pltpu.roll(v, step, 1), 0.0)
        step *= 2
    scratch[0:8, :] = v
    return v, scratch[...].T


def times_wide(q, state):
    high = state.astype(jnp.bfloat16)
    low = (state - high.astype(jnp.float32)).astype(jnp.bfloat16)
    return jnp.dot(q, high, preferred_element_type=jnp.float32) + jnp.dot(
        q, low, preferred_element_type=jnp.float32
    )


def state_body(ld, k, v, whole, message, first, scratch):
    rows, heads, depth = k.shape[0], ld.shape[0], first.shape[1]
    row, col = summed_decay(ld, scratch, BLOCK)
    scale = depth ** (-0.5)
    for h in range(heads):
        lanes = slice(h * depth, (h + 1) * depth)
        state = None
        total = 0.0
        for b in range(rows // BLOCK):
            here = slice(b * BLOCK, (b + 1) * BLOCK)
            last = row[h : h + 1, (b + 1) * BLOCK - 1 : (b + 1) * BLOCK]
            to_end = jnp.exp(last - col[here, h : h + 1]) * scale
            scaled = (k[here, lanes].astype(jnp.float32) * to_end).astype(jnp.bfloat16)
            added = lax.dot_general(
                scaled, v[here, lanes], (((0,), (0,)), ((), ())), preferred_element_type=jnp.float32
            )
            total = total + last
            if b == 0:
                first[h] = added
                state = added
            else:
                state = jnp.exp(last) * state + added
        decay = jnp.broadcast_to(jnp.exp(total), (1, depth))
        write_state(whole, h, decay, state)
        write_state(message, h, decay, state)


def within_body(ld, q, k, v, first, out, scratch):
    rows, heads, depth = q.shape[0], ld.shape[0], first.shape[1]
    row, col = summed_decay(ld, scratch, BLOCK)
    scale = depth ** (-0.5)
    tile = BLOCK // 2
    for h in range(heads):
        lanes = slice(h * depth, (h + 1) * depth)
        for b in range(rows // BLOCK):
            for i in range(2):
                t0 = b * BLOCK + i * tile
                seen = slice(b * BLOCK, t0 + tile)
                here = slice(t0, t0 + tile)
                span = (i + 1) * tile
                products = lax.dot_general(
                    q[here, lanes],
                    k[seen, lanes],
                    (((1,), (1,)), ((), ())),
                    preferred_element_type=jnp.float32,
                )
                gap = col[here, h : h + 1] - row[h : h + 1, seen]
                at = lax.broadcasted_iota(jnp.int32, (tile, span), 0) + i * tile
                causal = at >= lax.broadcasted_iota(jnp.int32, (tile, span), 1)
                weight = jnp.where(causal, jnp.exp(jnp.minimum(gap, 0.0)), 0.0)
                scores = (products * scale * weight).astype(jnp.bfloat16)
                result = jnp.dot(scores, v[seen, lanes], preferred_element_type=jnp.float32)
                if b > 0:
                    result = result + times_wide(q[here, lanes], first[h]) * jnp.exp(
                        col[here, h : h + 1]
                    )
                out[here, lanes] = result


def finish_body(coord, ld, q, within, gates, before, far3, far2, far1, gain, o0, o1, o2, o3, scratch, sums):
    rows, heads, depth = q.shape[0], ld.shape[0], before.shape[2]
    _, sums[...] = summed_decay(ld, scratch, rows)
    states = []
    for h in range(heads):
        state = read_state(far3, h)[1]
        for ref in (far2, far1):
            decay, more = read_state(ref, h)
            state = decay * state + more
        states.append(before[h, depth : depth + 1, :] * state + before[h, 0:depth, :])
    quarter = rows // RING
    for k, out in enumerate((o0, o1, o2, o3)):
        here = pl.ds(pl.multiple_of(((coord[3] + k) % RING) * quarter, quarter), quarter)
        for h in range(heads):
            lanes = slice(h * depth, (h + 1) * depth)
            retention = within[here, lanes] + times_wide(q[here, lanes], states[h]) * jnp.exp(
                sums[here, h : h + 1]
            )
            centered = retention - jnp.mean(retention, axis=-1, keepdims=True)
            variance = jnp.mean(centered * centered, axis=-1, keepdims=True)
            normed = centered * lax.rsqrt(variance + EPSILON) * gain[h : h + 1, :]
            g = gates[here, lanes].astype(jnp.float32)
            out[:, lanes] = (g * (1.0 / (1.0 + jnp.exp(-g))) * normed).astype(jnp.bfloat16)


def vmem_call(body, out_shape, *args, scratch=(), smem=0):
    vm = pl.BlockSpec(memory_space=pltpu.VMEM)
    return pl.pallas_call(
        body,
        out_shape=out_shape,
        in_specs=[pl.BlockSpec(memory_space=pltpu.SMEM)] * smem + [vm] * (len(args) - smem),
        out_specs=jax.tree.map(lambda _: vm, out_shape),
        scratch_shapes=list(scratch),
        compiler_params=pltpu.CompilerParams(vmem_limit_bytes=40 * 1024 * 1024),
    )(*args)


def mix_body(coord, r0, r1, r2, r3, own, near, near2, far, far2, resid, gain1, gain2, middle, out_a, out_b, acc):
    half = own.shape[0] // 2
    low = coord[2] == 0

    def part(cols, piece):
        return jnp.dot(cols, piece[...], preferred_element_type=jnp.float32)

    def rounded(v):
        return v.astype(jnp.bfloat16).astype(jnp.float32)

    def chosen(one, other):
        return jnp.where(low, one.astype(jnp.float32), other.astype(jnp.float32)).astype(jnp.bfloat16)

    left, right = r1[...], r3[...]
    far_a, far_b = r2[:, 0:half], r2[:, half:]
    acc[...] = rounded(part(r0[...], own))
    acc[...] += rounded(part(chosen(left, right), near))
    acc[...] += rounded(part(chosen(right, left), near2))
    far = part(chosen(far_a, far_b), far) + part(chosen(far_b, far_a), far2)
    mixed = rounded(acc[...] + rounded(far))
    mean = jnp.mean(mixed * mixed, axis=-1, keepdims=True)
    mid = resid[...].astype(jnp.float32) + mixed * lax.rsqrt(mean + EPSILON) * gain1[...]
    mid = mid.astype(jnp.bfloat16)
    middle[...] = mid
    mid = mid.astype(jnp.float32)
    mean = jnp.mean(mid * mid, axis=-1, keepdims=True)
    h = (mid * lax.rsqrt(mean + EPSILON) * gain2[...]).astype(jnp.bfloat16)
    out_a[...] = h[: h.shape[0] // 2]
    out_b[...] = h[h.shape[0] // 2 :]


def final_body(own_a, own_b, sum_a, sum_b, near_a, near_b, middle, gain, out):
    half = own_a.shape[0]
    for i, refs in enumerate(((own_a, sum_a, near_a), (own_b, sum_b, near_b))):
        here = slice(i * half, (i + 1) * half)
        total = sum(r[...].astype(jnp.float32) for r in refs)
        total = total.astype(jnp.bfloat16).astype(jnp.float32)
        mean = jnp.mean(total * total, axis=-1, keepdims=True)
        mid = middle[here, :].astype(jnp.float32)
        out[here, :] = (mid + total * lax.rsqrt(mean + EPSILON) * gain[...]).astype(jnp.bfloat16)


def read_state(ref, h):
    depth = ref.shape[2]
    state = ref[h, 0:depth, :].astype(jnp.float32)
    if ref.dtype == jnp.float32:
        return ref[h, depth : depth + 1, :], state
    tail = ref[h, depth : depth + 16, :].astype(jnp.float32)
    return tail[0:1] + tail[1:2], state


def write_state(ref, h, decay, state):
    depth = ref.shape[2]
    if ref.dtype == jnp.float32:
        ref[h, 0:depth, :] = state
        ref[h, depth : depth + 8, :] = jnp.broadcast_to(decay, (8, depth))
        return
    wide = jnp.broadcast_to(decay, (16, depth))
    high = wide.astype(jnp.bfloat16)
    low = (wide - high.astype(jnp.float32)).astype(jnp.bfloat16)
    at = lax.broadcasted_iota(jnp.int32, (16, depth), 0)
    ref[h, 0:depth, :] = state.astype(jnp.bfloat16)
    ref[h, depth : depth + 16, :] = jnp.where(at == 0, high, low)


def joined(earlier, later):
    return (earlier[0] * later[0], later[0] * earlier[1] + later[1])


def either(flag, one, other):
    return tuple(jnp.where(flag, a, b) for a, b in zip(one, other))


def pair_body(coord, total, got, new_total, before, message):
    upper = coord[2] == 1
    for h in range(total.shape[0]):
        mine, other = read_state(total, h), read_state(got, h)
        nothing = (jnp.ones_like(mine[0]), jnp.zeros_like(mine[1]))
        both = either(upper, joined(other, mine), joined(mine, other))
        write_state(new_total, h, *both)
        write_state(message, h, *both)
        write_state(before, h, *either(upper, other, nothing))


def plane_body(coord, total, inner, b1, b2, b3, before, message):
    y = coord[1]
    for h in range(total.shape[0]):
        mine = read_state(total, h)
        nothing = (jnp.ones_like(mine[0]), jnp.zeros_like(mine[1]))
        back = [read_state(r, h) for r in (b1, b2, b3)]
        past = nothing
        for k in (3, 2, 1):
            past = joined(past, either(y >= k, back[k - 1], nothing))
        whole = joined(past, mine)
        for k in (3, 2, 1):
            whole = joined(whole, either(y < k, back[k - 1], nothing))
        write_state(message, h, *whole)
        write_state(before, h, *joined(past, read_state(inner, h)))


def kernel(body, out_shape, *args, **more):
    return vmem_call(body, out_shape, *args, **more)


def shaped(dtype, *dims):
    return jax.ShapeDtypeStruct(dims, dtype)


def layer(
    queries,
    keys,
    values,
    gates,
    log_decay,
    norm_gain,
    out_weight,
    resid,
    post_mix_gain,
    pre_ffn_gain,
    w_gate,
    w_up,
    w_down,
    post_ffn_gain,
):
    f32, bf16 = jnp.float32, jnp.bfloat16
    z, y, c = (lax.axis_index(a) for a in SP)
    x = lax.axis_index("tp")
    coord = jnp.stack([z, y, c, x]).astype(jnp.int32)
    up1, down1 = along(1), along(-1)
    weights = gather_weights(w_gate, w_up, w_down)
    o_half = out_weight.shape[0] // 2
    turn = [(i, (i + 1) % RING) for i in range(RING)]
    turn += [(RING + i, RING + (i - 1) % RING) for i in range(RING)]
    o_near = lax.ppermute(out_weight, ("sp_2", "tp"), turn)
    o_fore = lax.dynamic_slice_in_dim(o_near, c * o_half, o_half, 0)
    o_far = lax.ppermute(o_fore, ("sp_2", "tp"), turn)
    o_near2 = lax.ppermute(o_near, "sp_2", flipped(2, 1))
    o_far2 = lax.ppermute(o_far, "sp_2", flipped(2, 1))

    rows, width = queries.shape
    heads = log_decay.shape[1]
    depth = width // heads
    ld = log_decay.T
    sums = pltpu.VMEM((128, rows), f32)
    total_shape = shaped(f32, heads, depth + 8, depth)
    message_shape = shaped(bf16, heads, depth + 16, depth)
    total, message, first = kernel(
        state_body,
        (total_shape, message_shape, shaped(f32, heads, depth, depth)),
        ld, keys, values,
        scratch=(sums,),
    )
    within = kernel(
        within_body, shaped(f32, rows, width), ld, queries, keys, values, first, scratch=(sums,)
    )
    got = lax.ppermute(message, "sp_2", flipped(2, 1))
    total, inner, message = kernel(
        pair_body, (total_shape, total_shape, message_shape), coord, total, got, smem=1
    )
    back = [lax.ppermute(message, "sp_1", along(k)) for k in (1, 2, 3)]
    before, message = kernel(
        plane_body, (total_shape, message_shape), coord, total, inner, *back, smem=1
    )
    back = [lax.ppermute(message, "sp_0", [(i, i + k) for i in range(RING - k)]) for k in (3, 2, 1)]
    quarter, model = resid.shape
    piece = shaped(bf16, quarter, width)
    turned = kernel(
        finish_body,
        (piece,) * RING,
        coord, ld, queries, within, gates, before, *back, norm_gain,
        scratch=(sums, pltpu.VMEM((rows, 128), f32)),
        smem=1,
    )
    turned = (turned[0], *(lax.ppermute(turned[k], "tp", along(k)) for k in (1, 2, 3)))
    half = quarter // 2
    middle, h_a, h_b = kernel(
        mix_body,
        (shaped(bf16, quarter, model), shaped(bf16, half, model), shaped(bf16, half, model)),
        coord, *turned, out_weight, o_near, o_near2, o_far, o_far2, resid,
        post_mix_gain.reshape(1, -1), pre_ffn_gain.reshape(1, -1),
        scratch=(pltpu.VMEM((quarter, model), f32),),
        smem=1,
    )

    r_a = lax.ppermute(h_a, "tp", up1)
    l_b = lax.ppermute(h_b, "tp", down1)
    far_a = lax.ppermute(r_a, "tp", up1)
    far_b = lax.ppermute(l_b, "tp", down1)
    r_b = lax.ppermute(h_b, "tp", up1)
    l_a = lax.ppermute(h_a, "tp", down1)

    def feed(*xs):
        return ffn(coord, weights, xs, 2)

    right_a, left_b = feed(r_a, l_b)
    opp_a, opp_b = feed(far_a, far_b)
    right_b, left_a = feed(r_b, l_a)
    own_a, own_b = feed(h_a, h_b)
    near_b = lax.ppermute(left_b, "tp", up1)
    near_a = lax.ppermute(right_a, "tp", down1)
    far_in_a = lax.ppermute(opp_a, "tp", up1)
    far_in_b = lax.ppermute(opp_b, "tp", down1)
    wide = lambda v: v.astype(f32)
    sum_a = lax.ppermute((wide(left_a) + wide(far_in_a)).astype(bf16), "tp", up1)
    sum_b = lax.ppermute((wide(right_b) + wide(far_in_b)).astype(bf16), "tp", down1)
    return kernel(
        final_body,
        shaped(bf16, quarter, model),
        own_a, own_b, sum_a, sum_b, near_a, near_b, middle, post_ffn_gain.reshape(1, -1),
    )


def solution(mesh):
    split = Mesh(mesh.devices.reshape(4, 4, 2, mesh.shape["tp"]), ("sp_0", "sp_1", "sp_2", "tp"))
    placed = (
        P(SP, "tp"),
        P(SP, "tp"),
        P(SP, "tp"),
        P(SP, "tp"),
        P(SP, "tp"),
        P("tp", None),
        P("tp", None),
        P(SP_TP, None),
        P(),
        P(),
        P(SP, "tp"),
        P(SP, "tp"),
        P("tp", SP),
        P(),
    )
    return jax.shard_map(
        layer, mesh=split, in_specs=placed, out_specs=P(SP_TP, None), check_vma=False
    )
```

profile of v0, /device:TPU:1, one launch (start us, length us, event | category | flops | bytes accessed | tf_op | source)
XLA Modules:
  0.0 181.0 jit_solution(13328176882554892900)
XLA Ops:
  0.0 2.2 %fusion = (bf16[1,3,64,1408]{3,2,1,0:T(8,128)(2,1)}, bf16[3,64,1408]{2,1,0:T(8,128)(2,1)}) fusion(bf16[1,64,1408]{2,1,0:T(8,128)(2,1)} %bitcast.25, bf16[1,64,1408]{2,1,0:T(8,128)(2,1)} %bitcast.26, bf16[1,64,1408]{2,1,0:T(8,128)(2,1)} %bitcast.27), kind=kLoop, calls=%fused_computation.7 | loop fusion | flops 540672 | bytes 1622016 | tf_op jit(solution)/shard_map/stack | solution.py:47
  2.3 4.6 %collective-permute-start.15 = (bf16[3,64,1408]{2,1,0:T(8,128)(2,1)}, bf16[3,64,1408]{2,1,0:T(8,128)(2,1)S(1)}, u32[]{:S(2)}, u32[]{:S(2)}) collective-permute-start(bf16[3,64,1408]{2,1,0:T(8,128)(2,1)} %get-tuple-element.52), channel_id=1, source_target_pairs={{0,24},{4,100},{8,0},{12,108},{16,8},{20,116},{24,16},{28,124},{32... | collective-permute-start | bytes 1622024 | tf_op jit(solution)/shard_map/ppermute | solution.py:45
  6.8 2.5 %collective-permute-start.10 = (bf16[256,2048]{1,0:T(8,128)(2,1)}, bf16[256,2048]{1,0:T(8,128)(2,1)S(1)}, u32[]{:S(2)}, u32[]{:S(2)}) collective-permute-start(bf16[256,2048]{1,0:T(8,128)(2,1)} %own.1), channel_id=1, source_target_pairs={{0,1},{1,2},{2,3},{3,0},{4,7},{5,4},{6,5},{7,6},{8,9},{9,10},{10,1... | collective-permute-start | bytes 3145736 | tf_op jit(solution)/shard_map/ppermute | solution.py:424
  9.3 1.8 shard_map.136
  13.0 2.8 %collective-permute-start.3 = (bf16[2,144,128]{2,1,0:T(8,128)(2,1)S(1)}, bf16[2,144,128]{2,1,0:T(8,128)(2,1)S(1)}, u32[]{:S(2)}, u32[]{:S(2)}) collective-permute-start(bf16[2,144,128]{2,1,0:T(8,128)(2,1)S(1)} %get-tuple-element.33), channel_id=1, source_target_pairs={{0,24},{8,0},{16,8},{24,16},{1,25},{9,1},{17,9},{25,17},{2,26},{10... | collective-permute-start | bytes 221192 | tf_op jit(solution)/shard_map/ppermute | solution.py:450
  16.2 3.1 %collective-permute-done.15 = bf16[3,64,1408]{2,1,0:T(8,128)(2,1)S(1)} collective-permute-done((bf16[3,64,1408]{2,1,0:T(8,128)(2,1)}, bf16[3,64,1408]{2,1,0:T(8,128)(2,1)S(1)}, u32[]{:S(2)}, u32[]{:S(2)}) %collective-permute-start.15) | collective-permute-done | bytes 540704 | tf_op jit(solution)/shard_map/ppermute | solution.py:45
  21.9 2.4 %collective-permute-start.24 = (bf16[2,3,64,1408]{3,2,1,0:T(8,128)(2,1)S(1)}, bf16[2,3,64,1408]{3,2,1,0:T(8,128)(2,1)}, u32[]{:S(2)}, u32[]{:S(2)}) collective-permute-start(bf16[2,3,64,1408]{3,2,1,0:T(8,128)(2,1)S(1)} %pad_maximum_fusion.1.refs_3_), channel_id=1, source_target_pairs={{0,4},{4,0},{1,5},{5,1},{2,6},{6,2},{3,7},{7,3},{8,12},{12,8},{9,1... | collective-permute-start | bytes 3244040 | tf_op jit(solution)/shard_map/ppermute | solution.py:56
  25.3 3.5 %collective-permute-start.6 = (bf16[2,144,128]{2,1,0:T(8,128)(2,1)S(1)}, bf16[2,144,128]{2,1,0:T(8,128)(2,1)S(1)}, u32[]{:S(2)}, u32[]{:S(2)}) collective-permute-start(bf16[2,144,128]{2,1,0:T(8,128)(2,1)S(1)} %get-tuple-element.35), channel_id=1, source_target_pairs={{0,32},{32,64},{64,96},{1,33},{33,65},{65,97},{2,34},{34,66},{66,9... | collective-permute-start | bytes 221192 | tf_op jit(solution)/shard_map/ppermute | solution.py:454
  28.8 5.2 %collective-permute-start.5 = (bf16[2,144,128]{2,1,0:T(8,128)(2,1)S(1)}, bf16[2,144,128]{2,1,0:T(8,128)(2,1)S(1)}, u32[]{:S(2)}, u32[]{:S(2)}) collective-permute-start(bf16[2,144,128]{2,1,0:T(8,128)(2,1)S(1)} %get-tuple-element.35), channel_id=1, source_target_pairs={{0,64},{32,96},{1,65},{33,97},{2,66},{34,98},{3,67},{35,99},{4,68}... | collective-permute-start | bytes 221192 | tf_op jit(solution)/shard_map/ppermute | solution.py:454
  34.0 3.2 %collective-permute-start.4 = (bf16[2,144,128]{2,1,0:T(8,128)(2,1)S(1)}, bf16[2,144,128]{2,1,0:T(8,128)(2,1)S(1)}, u32[]{:S(2)}, u32[]{:S(2)}) collective-permute-start(bf16[2,144,128]{2,1,0:T(8,128)(2,1)S(1)} %get-tuple-element.35), channel_id=1, source_target_pairs={{0,96},{1,97},{2,98},{3,99},{4,100},{5,101},{6,102},{7,103},{8,104... | collective-permute-start | bytes 221192 | tf_op jit(solution)/shard_map/ppermute | solution.py:454
  37.2 2.8 %shard_map.137.within = f32[1024,256]{1,0:T(8,128)S(1)} custom-call(f32[2,1024]{1,0:T(2,128)S(1)} %bitcast.19, bf16[1024,256]{1,0:T(8,128)(2,1)S(1)} %copy-done, bf16[1024,256]{1,0:T(8,128)(2,1)S(1)} %copy-done.1, bf16[1024,256]{1,0:T(8,128)(2,1)S(1)} %copy-done.2, f32[2,128,128]{2,1,0:T(8,128)S(1)} %get-tuple-element.28.first), custom_call_target="tpu_custom_call" | custom-call | tf_op jit(solution)/shard_map/pallas_call | solution.py:281
  40.1 2.7 %shard_map.140 = (bf16[256,256]{1,0:T(8,128)(2,1)S(1)}, bf16[256,256]{1,0:T(8,128)(2,1)S(1)}, bf16[256,256]{1,0:T(8,128)(2,1)S(1)}, bf16[256,256]{1,0:T(8,128)(2,1)S(1)}) custom-call(s32[4]{0:T(128)S(1)} %pad_add_fusion.coord, f32[2,1024]{1,0:T(2,128)S(1)} %bitcast.20, bf16[1024,256]{1,0:T(8,128)(2,1)S(1)} %copy-done, f32[1024,256]{1,0:T(8,128)S(1)} %shard_map.137.within, ...), custom_call_target="tpu_custom_call" | custom-call | tf_op jit(solution)/shard_map/pallas_call | solution.py:281
  44.1 3.8 %collective-permute-done.7.r1 = bf16[256,256]{1,0:T(8,128)(2,1)S(1)} collective-permute-done((bf16[256,256]{1,0:T(8,128)(2,1)S(1)}, bf16[256,256]{1,0:T(8,128)(2,1)S(1)}, u32[]{:S(2)}, u32[]{:S(2)}) %collective-permute-start.7) | collective-permute-done | bytes 131104 | tf_op jit(solution)/shard_map/ppermute | solution.py:464
  49.5 3.1 %collective-permute-start.18 = (bf16[2,3,64,1408]{3,2,1,0:T(8,128)(2,1)S(1)}, bf16[2,3,64,1408]{3,2,1,0:T(8,128)(2,1)S(1)}, u32[]{:S(2)}, u32[]{:S(2)}) collective-permute-start(bf16[2,3,64,1408]{3,2,1,0:T(8,128)(2,1)S(1)} %pad_maximum_fusion.1.refs_3_), channel_id=1, source_target_pairs={{0,96},{4,28},{8,104},{12,4},{16,112},{20,12},{24,120},{28,20},{32... | collective-permute-start | bytes 3244040 | tf_op jit(solution)/shard_map/ppermute | solution.py:50
  56.6 6.8 %collective-permute-done.9.r3 = bf16[256,256]{1,0:T(8,128)(2,1)S(1)} collective-permute-done((bf16[256,256]{1,0:T(8,128)(2,1)S(1)}, bf16[256,256]{1,0:T(8,128)(2,1)S(1)}, u32[]{:S(2)}, u32[]{:S(2)}) %collective-permute-start.9) | collective-permute-done | bytes 131104 | tf_op jit(solution)/shard_map/ppermute | solution.py:464
  63.5 4.4 %collective-permute-start.17 = (bf16[2,3,64,1408]{3,2,1,0:T(8,128)(2,1)S(1)}, bf16[2,3,64,1408]{3,2,1,0:T(8,128)(2,1)S(1)}, u32[]{:S(2)}, u32[]{:S(2)}) collective-permute-start(bf16[2,3,64,1408]{3,2,1,0:T(8,128)(2,1)S(1)} %pad_maximum_fusion.refs_2_), channel_id=1, source_target_pairs={{0,32},{4,12},{8,40},{12,20},{16,48},{20,28},{24,56},{28,4},{32,64... | collective-permute-start | bytes 3244040 | tf_op jit(solution)/shard_map/ppermute | solution.py:49
  67.8 8.1 %collective-permute-start.23 = (bf16[2,3,64,1408]{3,2,1,0:T(8,128)(2,1)S(1)}, bf16[2,3,64,1408]{3,2,1,0:T(8,128)(2,1)S(1)}, u32[]{:S(2)}, u32[]{:S(2)}) collective-permute-start(bf16[2,3,64,1408]{3,2,1,0:T(8,128)(2,1)S(1)} %pad_maximum_fusion.refs_2_), channel_id=1, source_target_pairs={{0,4},{4,0},{1,5},{5,1},{2,6},{6,2},{3,7},{7,3},{8,12},{12,8},{9,1... | collective-permute-start | bytes 3244040 | tf_op jit(solution)/shard_map/ppermute | solution.py:56
  75.9 3.3 %collective-permute-start.22 = (bf16[2,3,64,1408]{3,2,1,0:T(8,128)(2,1)S(1)}, bf16[2,3,64,1408]{3,2,1,0:T(8,128)(2,1)S(1)}, u32[]{:S(2)}, u32[]{:S(2)}) collective-permute-start(bf16[2,3,64,1408]{3,2,1,0:T(8,128)(2,1)S(1)} %pad_maximum_fusion.refs_2_), channel_id=1, source_target_pairs={{0,96},{4,28},{8,104},{12,4},{16,112},{20,12},{24,120},{28,20},{32... | collective-permute-start | bytes 3244040 | tf_op jit(solution)/shard_map/ppermute | solution.py:54
  79.9 7.7 %collective-permute-start.29 = (bf16[2,3,64,1408]{3,2,1,0:T(8,128)(2,1)}, bf16[2,3,64,1408]{3,2,1,0:T(8,128)(2,1)S(1)}, u32[]{:S(2)}, u32[]{:S(2)}) collective-permute-start(bf16[2,3,64,1408]{3,2,1,0:T(8,128)(2,1)} %collective-permute-done.21.refs_8_), channel_id=1, source_target_pairs={{0,4},{4,0},{1,5},{5,1},{2,6},{6,2},{3,7},{7,3},{8,12},{12,8},{9,1... | collective-permute-start | bytes 3244040 | tf_op jit(solution)/shard_map/ppermute | solution.py:56
  87.7 3.3 %collective-permute-start.20 = (bf16[2,3,64,1408]{3,2,1,0:T(8,128)(2,1)S(1)}, bf16[2,3,64,1408]{3,2,1,0:T(8,128)(2,1)S(1)}, u32[]{:S(2)}, u32[]{:S(2)}) collective-permute-start(bf16[2,3,64,1408]{3,2,1,0:T(8,128)(2,1)S(1)} %collective-permute-done.18.refs_5_), channel_id=1, source_target_pairs={{0,96},{4,28},{8,104},{12,4},{16,112},{20,12},{24,120},{28,20},{32... | collective-permute-start | bytes 3244040 | tf_op jit(solution)/shard_map/ppermute | solution.py:52
  91.0 3.1 %shard_map.141 = (bf16[256,2048]{1,0:T(8,128)(2,1)S(1)}, bf16[128,2048]{1,0:T(8,128)(2,1)S(1)}, bf16[128,2048]{1,0:T(8,128)(2,1)S(1)}) custom-call(s32[4]{0:T(128)S(1)} %pad_add_fusion.coord, bf16[256,256]{1,0:T(8,128)(2,1)S(1)} %get-tuple-element.36.r0, bf16[256,256]{1,0:T(8,128)(2,1)S(1)} %collective-permute-done.7.r1, ...), custom_call_target="tpu_custom_call" | custom-call | tf_op jit(solution)/shard_map/pallas_call | solution.py:281
  94.9 2.8 %collective-permute-start.35 = (bf16[128,2048]{1,0:T(8,128)(2,1)S(1)}, bf16[128,2048]{1,0:T(8,128)(2,1)S(1)}, u32[]{:S(2)}, u32[]{:S(2)}) collective-permute-start(bf16[128,2048]{1,0:T(8,128)(2,1)S(1)} %get-tuple-element.41.refs_1_), channel_id=1, source_target_pairs={{0,3},{1,0},{2,1},{3,2},{4,7},{5,4},{6,5},{7,6},{8,11},{9,8},{10,9... | collective-permute-start | bytes 1572872 | tf_op jit(solution)/shard_map/ppermute | solution.py:476
  97.6 11.0 %collective-permute-done.33.refs_0_ = bf16[128,2048]{1,0:T(8,128)(2,1)S(1)} collective-permute-done((bf16[128,2048]{1,0:T(8,128)(2,1)S(1)}, bf16[128,2048]{1,0:T(8,128)(2,1)S(1)}, u32[]{:S(2)}, u32[]{:S(2)}) %collective-permute-start.33) | collective-permute-done | bytes 524320 | tf_op jit(solution)/shard_map/ppermute | solution.py:475
  112.9 2.0 %collective-permute-start.36 = (bf16[128,2048]{1,0:T(8,128)(2,1)S(1)}, bf16[128,2048]{1,0:T(8,128)(2,1)S(1)}, u32[]{:S(2)}, u32[]{:S(2)}) collective-permute-start(bf16[128,2048]{1,0:T(8,128)(2,1)S(1)} %collective-permute-done.35.refs_1_), channel_id=1, source_target_pairs={{0,3},{1,0},{2,1},{3,2},{4,7},{5,4},{6,5},{7,6},{8,11},{9,8},{10,9... | collective-permute-start | bytes 1572872 | tf_op jit(solution)/shard_map/ppermute | solution.py:478
  116.5 9.4 %collective-permute-done.34.refs_0_ = bf16[128,2048]{1,0:T(8,128)(2,1)S(1)} collective-permute-done((bf16[128,2048]{1,0:T(8,128)(2,1)S(1)}, bf16[128,2048]{1,0:T(8,128)(2,1)S(1)}, u32[]{:S(2)}, u32[]{:S(2)}) %collective-permute-start.34) | collective-permute-done | bytes 524320 | tf_op jit(solution)/shard_map/ppermute | solution.py:477
  127.3 10.9 %ffn_rows.6 = (bf16[128,2048]{1,0:T(8,128)(2,1)S(1)}, bf16[128,2048]{1,0:T(8,128)(2,1)S(1)}) custom-call(s32[4]{0:T(128)S(1)} %pad_add_fusion.coord, bf16[128,2048]{1,0:T(8,128)(2,1)S(1)} %collective-permute-done.34.refs_0_, bf16[128,2048]{1,0:T(8,128)(2,1)S(1)} %collective-permute-done.36.refs_1_, bf16[2,3,64,1408]{3,2,1,0:T(8,128)(2,1)S(1)} %pad_maximum_fusion.refs_2_, ...), custom_call_target="tpu_custom_call" | custom-call | flops 4429185024 | bytes 17301504 | tf_op jit(solution)/shard_map/ffn_rows/pallas_call | solution.py:152
  138.3 3.3 %collective-permute-start.39 = (bf16[128,2048]{1,0:T(8,128)(2,1)S(1)}, bf16[128,2048]{1,0:T(8,128)(2,1)S(1)}, u32[]{:S(2)}, u32[]{:S(2)}) collective-permute-start(bf16[128,2048]{1,0:T(8,128)(2,1)S(1)} %get-tuple-element.47), channel_id=1, source_target_pairs={{0,3},{1,0},{2,1},{3,2},{4,7},{5,4},{6,5},{7,6},{8,11},{9,8},{10,9... | collective-permute-start | bytes 1572872 | tf_op jit(solution)/shard_map/ppermute | solution.py:492
  141.6 11.1 %ffn_rows.7 = (bf16[128,2048]{1,0:T(8,128)(2,1)S(1)}, bf16[128,2048]{1,0:T(8,128)(2,1)S(1)}) custom-call(s32[4]{0:T(128)S(1)} %pad_add_fusion.coord, bf16[128,2048]{1,0:T(8,128)(2,1)S(1)} %collective-permute-done.33.refs_0_, bf16[128,2048]{1,0:T(8,128)(2,1)S(1)} %collective-permute-done.35.refs_1_, bf16[2,3,64,1408]{3,2,1,0:T(8,128)(2,1)S(1)} %pad_maximum_fusion.refs_2_, ...), custom_call_target="tpu_custom_call" | custom-call | flops 4429185024 | bytes 17301504 | tf_op jit(solution)/shard_map/ffn_rows/pallas_call | solution.py:152
  154.2 10.9 %ffn_rows.5 = (bf16[128,2048]{1,0:T(8,128)(2,1)S(1)}, bf16[128,2048]{1,0:T(8,128)(2,1)S(1)}) custom-call(s32[4]{0:T(128)S(1)} %pad_add_fusion.coord, bf16[128,2048]{1,0:T(8,128)(2,1)S(1)} %collective-permute-done.31.refs_0_, bf16[128,2048]{1,0:T(8,128)(2,1)S(1)} %collective-permute-done.32.refs_1_, bf16[2,3,64,1408]{3,2,1,0:T(8,128)(2,1)S(1)} %pad_maximum_fusion.refs_2_, ...), custom_call_target="tpu_custom_call" | custom-call | flops 4429185024 | bytes 17301504 | tf_op jit(solution)/shard_map/ffn_rows/pallas_call | solution.py:152
  165.5 2.7 %collective-permute-start.40 = (bf16[128,2048]{1,0:T(8,128)(2,1)S(1)}, bf16[128,2048]{1,0:T(8,128)(2,1)S(1)}, u32[]{:S(2)}, u32[]{:S(2)}) collective-permute-start(bf16[128,2048]{1,0:T(8,128)(2,1)S(1)} %add_convert_fusion), channel_id=1, source_target_pairs={{0,3},{1,0},{2,1},{3,2},{4,7},{5,4},{6,5},{7,6},{8,11},{9,8},{10,9... | collective-permute-start | bytes 1572872 | tf_op jit(solution)/shard_map/ppermute | solution.py:495
  168.2 10.8 %ffn_rows.4 = (bf16[128,2048]{1,0:T(8,128)(2,1)S(1)}, bf16[128,2048]{1,0:T(8,128)(2,1)S(1)}) custom-call(s32[4]{0:T(128)S(1)} %pad_add_fusion.coord, bf16[128,2048]{1,0:T(8,128)(2,1)S(1)} %get-tuple-element.40.refs_0_, bf16[128,2048]{1,0:T(8,128)(2,1)S(1)} %get-tuple-element.41.refs_1_, bf16[2,3,64,1408]{3,2,1,0:T(8,128)(2,1)S(1)} %pad_maximum_fusion.refs_2_, ...), custom_call_target="tpu_custom_call" | custom-call | flops 4429185024 | bytes 17301504 | tf_op jit(solution)/shard_map/ffn_rows/pallas_call | solution.py:152
  179.1 1.9 %shard_map.142 = bf16[256,2048]{1,0:T(8,128)(2,1)} custom-call(bf16[128,2048]{1,0:T(8,128)(2,1)S(1)} %get-tuple-element.42.own_a, bf16[128,2048]{1,0:T(8,128)(2,1)S(1)} %get-tuple-element.43.own_b, bf16[128,2048]{1,0:T(8,128)(2,1)S(1)} %collective-permute-done.38.sum_a, bf16[128,2048]{1,0:T(8,128)(2,1)S(1)} %collective-permute-done.40.sum_b, ...), custom_call_target="tpu_custom_call" | custom-call | tf_op jit(solution)/shard_map/pallas_call | solution.py:281
  (118 shorter events, 23.4 us)
Async XLA Ops:
  2.3 17.0 %collective-permute-start.15 = (bf16[3,64,1408]{2,1,0:T(8,128)(2,1)}, bf16[3,64,1408]{2,1,0:T(8,128)(2,1)S(1)}, u32[]{:S(2)}, u32[]{:S(2)}) collective-permute-start(bf16[3,64,1408]{2,1,0:T(8,128)(2,1)} %get-tuple-element.52), channel_id=1, source_target_pairs={{0,24},{4,100},{8,0},{12,108},{16,8},{20,116},{24,16},{28,124},{32... | collective-permute-start | bytes 1622024 | tf_op jit(solution)/shard_map/ppermute | solution.py:45
  6.8 13.7 %collective-permute-start.16 = (bf16[3,64,1408]{2,1,0:T(8,128)(2,1)}, bf16[3,64,1408]{2,1,0:T(8,128)(2,1)}, u32[]{:S(2)}, u32[]{:S(2)}) collective-permute-start(bf16[3,64,1408]{2,1,0:T(8,128)(2,1)} %get-tuple-element.52), channel_id=1, source_target_pairs={{0,16},{4,68},{8,24},{12,76},{16,0},{20,84},{24,8},{28,92},{32,48}... | collective-permute-start | bytes 1622024 | tf_op jit(solution)/shard_map/ppermute | solution.py:46
  6.8 42.6 %collective-permute-start.10 = (bf16[256,2048]{1,0:T(8,128)(2,1)}, bf16[256,2048]{1,0:T(8,128)(2,1)S(1)}, u32[]{:S(2)}, u32[]{:S(2)}) collective-permute-start(bf16[256,2048]{1,0:T(8,128)(2,1)} %own.1), channel_id=1, source_target_pairs={{0,1},{1,2},{2,3},{3,0},{4,7},{5,4},{6,5},{7,6},{8,9},{9,10},{10,1... | collective-permute-start | bytes 3145736 | tf_op jit(solution)/shard_map/ppermute | solution.py:424
  13.0 11.3 %collective-permute-start.3 = (bf16[2,144,128]{2,1,0:T(8,128)(2,1)S(1)}, bf16[2,144,128]{2,1,0:T(8,128)(2,1)S(1)}, u32[]{:S(2)}, u32[]{:S(2)}) collective-permute-start(bf16[2,144,128]{2,1,0:T(8,128)(2,1)S(1)} %get-tuple-element.33), channel_id=1, source_target_pairs={{0,24},{8,0},{16,8},{24,16},{1,25},{9,1},{17,9},{25,17},{2,26},{10... | collective-permute-start | bytes 221192 | tf_op jit(solution)/shard_map/ppermute | solution.py:450
  21.9 54.0 %collective-permute-start.24 = (bf16[2,3,64,1408]{3,2,1,0:T(8,128)(2,1)S(1)}, bf16[2,3,64,1408]{3,2,1,0:T(8,128)(2,1)}, u32[]{:S(2)}, u32[]{:S(2)}) collective-permute-start(bf16[2,3,64,1408]{3,2,1,0:T(8,128)(2,1)S(1)} %pad_maximum_fusion.1.refs_3_), channel_id=1, source_target_pairs={{0,4},{4,0},{1,5},{5,1},{2,6},{6,2},{3,7},{7,3},{8,12},{12,8},{9,1... | collective-permute-start | bytes 3244040 | tf_op jit(solution)/shard_map/ppermute | solution.py:56
  24.3 54.9 %collective-permute-start.21 = (bf16[2,3,64,1408]{3,2,1,0:T(8,128)(2,1)S(1)}, bf16[2,3,64,1408]{3,2,1,0:T(8,128)(2,1)}, u32[]{:S(2)}, u32[]{:S(2)}) collective-permute-start(bf16[2,3,64,1408]{3,2,1,0:T(8,128)(2,1)S(1)} %pad_maximum_fusion.1.refs_3_), channel_id=1, source_target_pairs={{0,32},{4,12},{8,40},{12,20},{16,48},{20,28},{24,56},{28,4},{32,64... | collective-permute-start | bytes 3244040 | tf_op jit(solution)/shard_map/ppermute | solution.py:53
  28.8 11.3 %collective-permute-start.5 = (bf16[2,144,128]{2,1,0:T(8,128)(2,1)S(1)}, bf16[2,144,128]{2,1,0:T(8,128)(2,1)S(1)}, u32[]{:S(2)}, u32[]{:S(2)}) collective-permute-start(bf16[2,144,128]{2,1,0:T(8,128)(2,1)S(1)} %get-tuple-element.35), channel_id=1, source_target_pairs={{0,64},{32,96},{1,65},{33,97},{2,66},{34,98},{3,67},{35,99},{4,68}... | collective-permute-start | bytes 221192 | tf_op jit(solution)/shard_map/ppermute | solution.py:454
  44.1 10.4 %collective-permute-start.14 = (bf16[3,64,1408]{2,1,0:T(8,128)(2,1)}, bf16[3,64,1408]{2,1,0:T(8,128)(2,1)}, u32[]{:S(2)}, u32[]{:S(2)}) collective-permute-start(bf16[3,64,1408]{2,1,0:T(8,128)(2,1)} %get-tuple-element.52), channel_id=1, source_target_pairs={{0,8},{4,36},{8,16},{12,44},{16,24},{20,52},{24,0},{28,60},{32,40}... | collective-permute-start | bytes 1622024 | tf_op jit(solution)/shard_map/ppermute | solution.py:44
  49.5 29.8 %collective-permute-start.18 = (bf16[2,3,64,1408]{3,2,1,0:T(8,128)(2,1)S(1)}, bf16[2,3,64,1408]{3,2,1,0:T(8,128)(2,1)S(1)}, u32[]{:S(2)}, u32[]{:S(2)}) collective-permute-start(bf16[2,3,64,1408]{3,2,1,0:T(8,128)(2,1)S(1)} %pad_maximum_fusion.1.refs_3_), channel_id=1, source_target_pairs={{0,96},{4,28},{8,104},{12,4},{16,112},{20,12},{24,120},{28,20},{32... | collective-permute-start | bytes 3244040 | tf_op jit(solution)/shard_map/ppermute | solution.py:50
  53.2 14.6 %collective-permute-start.12 = (bf16[128,2048]{1,0:T(8,128)(2,1)S(1)}, bf16[128,2048]{1,0:T(8,128)(2,1)S(1)}, u32[]{:S(2)}, u32[]{:S(2)}) collective-permute-start(bf16[128,2048]{1,0:T(8,128)(2,1)S(1)} %constant_dynamic-slice_fusion), channel_id=1, source_target_pairs={{0,1},{1,2},{2,3},{3,0},{4,7},{5,4},{6,5},{7,6},{8,9},{9,10},{10,1... | collective-permute-start | bytes 1572872 | tf_op jit(solution)/shard_map/ppermute | solution.py:426
  54.5 8.9 %collective-permute-start.9 = (bf16[256,256]{1,0:T(8,128)(2,1)S(1)}, bf16[256,256]{1,0:T(8,128)(2,1)S(1)}, u32[]{:S(2)}, u32[]{:S(2)}) collective-permute-start(bf16[256,256]{1,0:T(8,128)(2,1)S(1)} %get-tuple-element.39), channel_id=1, source_target_pairs={{0,3},{1,0},{2,1},{3,2},{4,7},{5,4},{6,5},{7,6},{8,11},{9,8},{10,9... | collective-permute-start | bytes 393224 | tf_op jit(solution)/shard_map/ppermute | solution.py:464
  63.5 16.5 %collective-permute-start.17 = (bf16[2,3,64,1408]{3,2,1,0:T(8,128)(2,1)S(1)}, bf16[2,3,64,1408]{3,2,1,0:T(8,128)(2,1)S(1)}, u32[]{:S(2)}, u32[]{:S(2)}) collective-permute-start(bf16[2,3,64,1408]{3,2,1,0:T(8,128)(2,1)S(1)} %pad_maximum_fusion.refs_2_), channel_id=1, source_target_pairs={{0,32},{4,12},{8,40},{12,20},{16,48},{20,28},{24,56},{28,4},{32,64... | collective-permute-start | bytes 3244040 | tf_op jit(solution)/shard_map/ppermute | solution.py:49
  67.8 26.2 %collective-permute-start.23 = (bf16[2,3,64,1408]{3,2,1,0:T(8,128)(2,1)S(1)}, bf16[2,3,64,1408]{3,2,1,0:T(8,128)(2,1)S(1)}, u32[]{:S(2)}, u32[]{:S(2)}) collective-permute-start(bf16[2,3,64,1408]{3,2,1,0:T(8,128)(2,1)S(1)} %pad_maximum_fusion.refs_2_), channel_id=1, source_target_pairs={{0,4},{4,0},{1,5},{5,1},{2,6},{6,2},{3,7},{7,3},{8,12},{12,8},{9,1... | collective-permute-start | bytes 3244040 | tf_op jit(solution)/shard_map/ppermute | solution.py:56
  75.9 18.9 %collective-permute-start.22 = (bf16[2,3,64,1408]{3,2,1,0:T(8,128)(2,1)S(1)}, bf16[2,3,64,1408]{3,2,1,0:T(8,128)(2,1)S(1)}, u32[]{:S(2)}, u32[]{:S(2)}) collective-permute-start(bf16[2,3,64,1408]{3,2,1,0:T(8,128)(2,1)S(1)} %pad_maximum_fusion.refs_2_), channel_id=1, source_target_pairs={{0,96},{4,28},{8,104},{12,4},{16,112},{20,12},{24,120},{28,20},{32... | collective-permute-start | bytes 3244040 | tf_op jit(solution)/shard_map/ppermute | solution.py:54
  79.2 11.7 %collective-permute-start.11 = (bf16[256,2048]{1,0:T(8,128)(2,1)S(1)}, bf16[256,2048]{1,0:T(8,128)(2,1)S(1)}, u32[]{:S(2)}, u32[]{:S(2)}) collective-permute-start(bf16[256,2048]{1,0:T(8,128)(2,1)S(1)} %collective-permute-done.10.near), channel_id=1, source_target_pairs={{0,4},{4,0},{1,5},{5,1},{2,6},{6,2},{3,7},{7,3},{8,12},{12,8},{9,1... | collective-permute-start | bytes 3145736 | tf_op jit(solution)/shard_map/ppermute | solution.py:427
  79.9 29.2 %collective-permute-start.29 = (bf16[2,3,64,1408]{3,2,1,0:T(8,128)(2,1)}, bf16[2,3,64,1408]{3,2,1,0:T(8,128)(2,1)S(1)}, u32[]{:S(2)}, u32[]{:S(2)}) collective-permute-start(bf16[2,3,64,1408]{3,2,1,0:T(8,128)(2,1)} %collective-permute-done.21.refs_8_), channel_id=1, source_target_pairs={{0,4},{4,0},{1,5},{5,1},{2,6},{6,2},{3,7},{7,3},{8,12},{12,8},{9,1... | collective-permute-start | bytes 3244040 | tf_op jit(solution)/shard_map/ppermute | solution.py:56
  87.7 21.6 %collective-permute-start.20 = (bf16[2,3,64,1408]{3,2,1,0:T(8,128)(2,1)S(1)}, bf16[2,3,64,1408]{3,2,1,0:T(8,128)(2,1)S(1)}, u32[]{:S(2)}, u32[]{:S(2)}) collective-permute-start(bf16[2,3,64,1408]{3,2,1,0:T(8,128)(2,1)S(1)} %collective-permute-done.18.refs_5_), channel_id=1, source_target_pairs={{0,96},{4,28},{8,104},{12,4},{16,112},{20,12},{24,120},{28,20},{32... | collective-permute-start | bytes 3244040 | tf_op jit(solution)/shard_map/ppermute | solution.py:52
  90.9 18.7 %collective-permute-start.19 = (bf16[2,3,64,1408]{3,2,1,0:T(8,128)(2,1)S(1)}, bf16[2,3,64,1408]{3,2,1,0:T(8,128)(2,1)S(1)}, u32[]{:S(2)}, u32[]{:S(2)}) collective-permute-start(bf16[2,3,64,1408]{3,2,1,0:T(8,128)(2,1)S(1)} %collective-permute-done.17.refs_4_), channel_id=1, source_target_pairs={{0,32},{4,12},{8,40},{12,20},{16,48},{20,28},{24,56},{28,4},{32,64... | collective-permute-start | bytes 3244040 | tf_op jit(solution)/shard_map/ppermute | solution.py:51
  94.1 14.5 %collective-permute-start.33 = (bf16[128,2048]{1,0:T(8,128)(2,1)S(1)}, bf16[128,2048]{1,0:T(8,128)(2,1)S(1)}, u32[]{:S(2)}, u32[]{:S(2)}) collective-permute-start(bf16[128,2048]{1,0:T(8,128)(2,1)S(1)} %get-tuple-element.40.refs_0_), channel_id=1, source_target_pairs={{0,1},{1,2},{2,3},{3,0},{4,5},{5,6},{6,7},{7,4},{8,9},{9,10},{10,1... | collective-permute-start | bytes 1572872 | tf_op jit(solution)/shard_map/ppermute | solution.py:475
  94.9 13.8 %collective-permute-start.35 = (bf16[128,2048]{1,0:T(8,128)(2,1)S(1)}, bf16[128,2048]{1,0:T(8,128)(2,1)S(1)}, u32[]{:S(2)}, u32[]{:S(2)}) collective-permute-start(bf16[128,2048]{1,0:T(8,128)(2,1)S(1)} %get-tuple-element.41.refs_1_), channel_id=1, source_target_pairs={{0,3},{1,0},{2,1},{3,2},{4,7},{5,4},{6,5},{7,6},{8,11},{9,8},{10,9... | collective-permute-start | bytes 1572872 | tf_op jit(solution)/shard_map/ppermute | solution.py:476
  109.3 17.0 %collective-permute-start.28 = (bf16[2,3,64,1408]{3,2,1,0:T(8,128)(2,1)S(1)}, bf16[2,3,64,1408]{3,2,1,0:T(8,128)(2,1)S(1)}, u32[]{:S(2)}, u32[]{:S(2)}) collective-permute-start(bf16[2,3,64,1408]{3,2,1,0:T(8,128)(2,1)S(1)} %collective-permute-done.20.refs_7_), channel_id=1, source_target_pairs={{0,4},{4,0},{1,5},{5,1},{2,6},{6,2},{3,7},{7,3},{8,12},{12,8},{9,1... | collective-permute-start | bytes 3244040 | tf_op jit(solution)/shard_map/ppermute | solution.py:56
  109.7 17.6 %collective-permute-start.27 = (bf16[2,3,64,1408]{3,2,1,0:T(8,128)(2,1)S(1)}, bf16[2,3,64,1408]{3,2,1,0:T(8,128)(2,1)}, u32[]{:S(2)}, u32[]{:S(2)}) collective-permute-start(bf16[2,3,64,1408]{3,2,1,0:T(8,128)(2,1)S(1)} %collective-permute-done.19.refs_6_), channel_id=1, source_target_pairs={{0,4},{4,0},{1,5},{5,1},{2,6},{6,2},{3,7},{7,3},{8,12},{12,8},{9,1... | collective-permute-start | bytes 3244040 | tf_op jit(solution)/shard_map/ppermute | solution.py:56
  111.4 14.6 %collective-permute-start.34 = (bf16[128,2048]{1,0:T(8,128)(2,1)S(1)}, bf16[128,2048]{1,0:T(8,128)(2,1)S(1)}, u32[]{:S(2)}, u32[]{:S(2)}) collective-permute-start(bf16[128,2048]{1,0:T(8,128)(2,1)S(1)} %collective-permute-done.33.refs_0_), channel_id=1, source_target_pairs={{0,1},{1,2},{2,3},{3,0},{4,5},{5,6},{6,7},{7,4},{8,9},{9,10},{10,1... | collective-permute-start | bytes 1572872 | tf_op jit(solution)/shard_map/ppermute | solution.py:477
  112.9 13.3 %collective-permute-start.36 = (bf16[128,2048]{1,0:T(8,128)(2,1)S(1)}, bf16[128,2048]{1,0:T(8,128)(2,1)S(1)}, u32[]{:S(2)}, u32[]{:S(2)}) collective-permute-start(bf16[128,2048]{1,0:T(8,128)(2,1)S(1)} %collective-permute-done.35.refs_1_), channel_id=1, source_target_pairs={{0,3},{1,0},{2,1},{3,2},{4,7},{5,4},{6,5},{7,6},{8,11},{9,8},{10,9... | collective-permute-start | bytes 1572872 | tf_op jit(solution)/shard_map/ppermute | solution.py:478
  114.9 39.2 %collective-permute-start.32 = (bf16[128,2048]{1,0:T(8,128)(2,1)S(1)}, bf16[128,2048]{1,0:T(8,128)(2,1)S(1)}, u32[]{:S(2)}, u32[]{:S(2)}) collective-permute-start(bf16[128,2048]{1,0:T(8,128)(2,1)S(1)} %get-tuple-element.40.refs_0_), channel_id=1, source_target_pairs={{0,3},{1,0},{2,1},{3,2},{4,7},{5,4},{6,5},{7,6},{8,11},{9,8},{10,9... | collective-permute-start | bytes 1572872 | tf_op jit(solution)/shard_map/ppermute | solution.py:480
  125.9 28.3 %collective-permute-start.31 = (bf16[128,2048]{1,0:T(8,128)(2,1)S(1)}, bf16[128,2048]{1,0:T(8,128)(2,1)S(1)}, u32[]{:S(2)}, u32[]{:S(2)}) collective-permute-start(bf16[128,2048]{1,0:T(8,128)(2,1)S(1)} %get-tuple-element.41.refs_1_), channel_id=1, source_target_pairs={{0,1},{1,2},{2,3},{3,0},{4,5},{5,6},{6,7},{7,4},{8,9},{9,10},{10,1... | collective-permute-start | bytes 1572872 | tf_op jit(solution)/shard_map/ppermute | solution.py:479
  138.2 26.9 %collective-permute-start.37 = (bf16[128,2048]{1,0:T(8,128)(2,1)S(1)}, bf16[128,2048]{1,0:T(8,128)(2,1)S(1)}, u32[]{:S(2)}, u32[]{:S(2)}) collective-permute-start(bf16[128,2048]{1,0:T(8,128)(2,1)S(1)} %get-tuple-element.45), channel_id=1, source_target_pairs={{0,1},{1,2},{2,3},{3,0},{4,5},{5,6},{6,7},{7,4},{8,9},{9,10},{10,1... | collective-permute-start | bytes 1572872 | tf_op jit(solution)/shard_map/ppermute | solution.py:491
  138.3 27.0 %collective-permute-start.39 = (bf16[128,2048]{1,0:T(8,128)(2,1)S(1)}, bf16[128,2048]{1,0:T(8,128)(2,1)S(1)}, u32[]{:S(2)}, u32[]{:S(2)}) collective-permute-start(bf16[128,2048]{1,0:T(8,128)(2,1)S(1)} %get-tuple-element.47), channel_id=1, source_target_pairs={{0,3},{1,0},{2,1},{3,2},{4,7},{5,4},{6,5},{7,6},{8,11},{9,8},{10,9... | collective-permute-start | bytes 1572872 | tf_op jit(solution)/shard_map/ppermute | solution.py:492
  152.7 26.4 %collective-permute-start.41 = (bf16[128,2048]{1,0:T(8,128)(2,1)S(1)}, bf16[128,2048]{1,0:T(8,128)(2,1)S(1)}, u32[]{:S(2)}, u32[]{:S(2)}) collective-permute-start(bf16[128,2048]{1,0:T(8,128)(2,1)S(1)} %get-tuple-element.48), channel_id=1, source_target_pairs={{0,3},{1,0},{2,1},{3,2},{4,7},{5,4},{6,5},{7,6},{8,11},{9,8},{10,9... | collective-permute-start | bytes 1572872 | tf_op jit(solution)/shard_map/ppermute | solution.py:490
  154.1 24.9 %collective-permute-start.42 = (bf16[128,2048]{1,0:T(8,128)(2,1)S(1)}, bf16[128,2048]{1,0:T(8,128)(2,1)S(1)}, u32[]{:S(2)}, u32[]{:S(2)}) collective-permute-start(bf16[128,2048]{1,0:T(8,128)(2,1)S(1)} %get-tuple-element.49), channel_id=1, source_target_pairs={{0,1},{1,2},{2,3},{3,0},{4,5},{5,6},{6,7},{7,4},{8,9},{9,10},{10,1... | collective-permute-start | bytes 1572872 | tf_op jit(solution)/shard_map/ppermute | solution.py:489
  165.2 13.8 %collective-permute-start.38 = (bf16[128,2048]{1,0:T(8,128)(2,1)S(1)}, bf16[128,2048]{1,0:T(8,128)(2,1)S(1)}, u32[]{:S(2)}, u32[]{:S(2)}) collective-permute-start(bf16[128,2048]{1,0:T(8,128)(2,1)S(1)} %add_convert_fusion.1), channel_id=1, source_target_pairs={{0,1},{1,2},{2,3},{3,0},{4,5},{5,6},{6,7},{7,4},{8,9},{9,10},{10,1... | collective-permute-start | bytes 1572872 | tf_op jit(solution)/shard_map/ppermute | solution.py:494
  165.5 13.6 %collective-permute-start.40 = (bf16[128,2048]{1,0:T(8,128)(2,1)S(1)}, bf16[128,2048]{1,0:T(8,128)(2,1)S(1)}, u32[]{:S(2)}, u32[]{:S(2)}) collective-permute-start(bf16[128,2048]{1,0:T(8,128)(2,1)S(1)} %add_convert_fusion), channel_id=1, source_target_pairs={{0,3},{1,0},{2,1},{3,2},{4,7},{5,4},{6,5},{7,6},{8,11},{9,8},{10,9... | collective-permute-start | bytes 1572872 | tf_op jit(solution)/shard_map/ppermute | solution.py:495
  (34 other events, 470.7 us)
where the time goes:
time: 183 us; the launch traced here: 181 us
  starting transfers between devices  77.3 us (42%)
  Pallas kernels  57.1 us (31%)
  waiting for transfers between devices  39.7 us (22%)
  other arithmetic  5.26 us (3%)
    pallas_call x4, Pallas kernels, ffn(): pl.pallas_call(functools.partial(ffn_body, len(xs), n_out), out_shape=[ja...  43.6 us
    ppermute x8, starting transfers between devices, gather_weights(): return own + [lax.ppermute(v, 'sp_2', flipped(2, 1)) for v in own]  19.3 us
    pallas_call x7, Pallas kernels, vmem_call(): pl.pallas_call(body, out_shape=out_shape, in_specs=[pl.BlockSpec(memory_s...  13.5 us
    ppermute x3, starting transfers between devices, layer(): lax.ppermute(message, 'sp_0', [(i, i + k) for i in range(RING - k)])  11.9 us
    ppermute x3, waiting for transfers between devices, layer(): lax.ppermute(turned[k], 'tp', along(k))  11.2 us
    ppermute x1, waiting for transfers between devices, layer(): r_a = lax.ppermute(h_a, 'tp', up1)  11 us
    ppermute x1, waiting for transfers between devices, layer(): far_a = lax.ppermute(r_a, 'tp', up1)  9.43 us
    ppermute x1, starting transfers between devices, gather_weights(): left = lax.ppermute(mine, SP, near(-1))  4.58 us
  transfers between devices with their start and end apart: 43, of which 11 were waited for; matrix products, arithmetic and copies ran while one was open for 2% of the time, Pallas kernels for 31%

commit v1 on v0

--- a/solution.py
+++ b/solution.py
@@ -13,6 +13,7 @@
 SP = ("sp_0", "sp_1", "sp_2")
 SP_TP = ("sp_0", "sp_1", "sp_2", "tp")
 RING = 4
+LIMIT = 16 * 1024 * 1024
 EPSILON = 1e-06
 
 
@@ -59,116 +60,116 @@
 PIECES = ((0, 0), (2, 0), (0, 3), (2, 1), (0, 2), (2, 2), (2, 3), (0, 1))
 
 
-def ffn_body(n_in, n_out, coord, *refs):
-    xs = refs[:n_in]
-    count = 2 * len(PIECES)
-    pieces = refs[n_in : n_in + count]
-    outs = refs[n_in + count : n_in + count + n_out]
-    w, x, gate, up, hid, sem_gu, sem_d = refs[n_in + count + n_out :]
+def place_body(chosen, coord, *refs):
+    count = 2 * len(chosen)
+    pieces = refs[:count]
+    w, sem = refs[-2:]
     z, y, c = coord[0], coord[1], coord[2]
     offs = (0, RING - 1, 1, 2)
 
-    def plan(low):
-        items = []
+    def copies(low):
+        made = []
         for side in range(2):
             core = side if low else 1 - side
-            for i, (first, away) in enumerate(PIECES):
+            for i, index in enumerate(chosen):
+                first, away = PIECES[index]
                 for k in range(2):
                     near = offs[first + k]
                     dz, dy = (away, near) if core == 0 else (near, away)
                     chip = ((z + dz) % RING) * RING + (y + dy) % RING
-                    items.append((dz, pieces[side * len(PIECES) + i], k, core, chip))
-        return [item[1:] for item in sorted(items, key=lambda item: item[0])]
-
-    def gu_copy(src, k, core, chip):
-        return pltpu.make_async_copy(
-            src.at[k, pl.ds(0, 2)], w.at[pl.ds(0, 2), chip, core], sem_gu.at[core, chip]
-        )
-
-    def d_copy(src, k, core, chip):
-        return pltpu.make_async_copy(src.at[k, 2], w.at[2, chip, core], sem_d.at[core, chip])
+                    src = pieces[side * len(chosen) + i].at[k]
+                    made.append(
+                        pltpu.make_async_copy(src, w.at[:, chip, core], sem.at[len(made)])
+                    )
+        return made
 
     for low in (True, False):
 
         @pl.when((c == 0) == low)
         def _():
-            items = plan(low)
-            for item in items:
-                gu_copy(*item).start()
-            for item in items:
-                d_copy(*item).start()
-
-    rows = x.shape[0]
+            made = copies(low)
+            for one in made:
+                one.start()
+            for one in made:
+                one.wait()
+
+
+def place(coord, weights, chosen, w=None):
+    n = len(PIECES)
+    pieces = [weights[side * n + i] for side in range(2) for i in chosen]
+    width = weights[0].shape[-1]
+    hb = pl.BlockSpec(memory_space=pltpu.HBM)
+    vm = pl.BlockSpec(memory_space=pltpu.VMEM)
+    more = [] if w is None else [w]
+    return pl.pallas_call(
+        functools.partial(place_body, chosen),
+        out_shape=jax.ShapeDtypeStruct((3, 16, 2, 64, width), jnp.bfloat16),
+        in_specs=[pl.BlockSpec(memory_space=pltpu.SMEM)] + [hb] * len(pieces) + [vm] * len(more),
+        out_specs=vm,
+        scratch_shapes=[pltpu.SemaphoreType.DMA((2 * len(pieces),))],
+        input_output_aliases={} if w is None else {1 + len(pieces): 0},
+        compiler_params=pltpu.CompilerParams(vmem_limit_bytes=LIMIT),
+    )(coord, *pieces, *more)
+
+
+def ffn_body(n_in, n_out, *refs):
+    xs = refs[:n_in]
+    w = refs[n_in]
+    outs = refs[n_in + 1 : n_in + 1 + n_out]
+    x, both, hid = refs[n_in + 1 + n_out :]
+    rows, model = x.shape
+    width = both.shape[2]
     per = rows // n_in
     for i in range(n_in):
         x[i * per : (i + 1) * per, :] = xs[i][...]
-    gate[...] = jnp.zeros_like(gate)
-    up[...] = jnp.zeros_like(up)
-    depth = 512
-    width = gate.shape[1]
-
-    def load(which, k):
-        return w[which, pl.ds(4 * k, 4)].reshape(depth, width)
-
-    def enter(step, carry):
-        k = (z + step) % RING
-        for core in range(2):
-            for j in range(4):
-                gu_copy(pieces[0], 0, core, 4 * k + j).wait()
-        xk = x[:, pl.ds(pl.multiple_of(k * depth, depth), depth)]
-        gate[...] += jnp.dot(xk, load(0, k), preferred_element_type=jnp.float32)
-        up[...] += jnp.dot(xk, load(1, k), preferred_element_type=jnp.float32)
+
+    def enter(i, carry):
+        both[i] = jnp.dot(x[...], w[i].reshape(model, width), preferred_element_type=jnp.float32)
         return carry
 
-    lax.fori_loop(0, RING, enter, 0)
-    g = gate[...]
-    hid[...] = (g * (1.0 / (1.0 + jnp.exp(-g))) * up[...]).astype(jnp.bfloat16)
+    lax.fori_loop(0, 2, enter, 0)
+    g = both[0]
+    hid[...] = (g * (1.0 / (1.0 + jnp.exp(-g))) * both[1]).astype(jnp.bfloat16)
     per_out = rows // n_out
-
-    def leave(step, carry):
-        k = (z + step) % RING
-        for core in range(2):
-            for j in range(4):
-                d_copy(pieces[0], 0, core, 4 * k + j).wait()
-        part = lax.dot_general(
-            hid[...], load(2, k), (((1,), (1,)), ((), ())), preferred_element_type=jnp.float32
-        ).astype(jnp.bfloat16)
-        for i in range(n_out):
-            outs[i][:, pl.ds(pl.multiple_of(k * depth, depth), depth)] = part[
-                i * per_out : (i + 1) * per_out
-            ]
+    step = 256
+    turns = 2
+
+    def leave(turn, carry):
+        for j in range(model // step // turns):
+            k = turn * (model // step // turns) + j
+            part = lax.dot_general(
+                hid[...],
+                w[2, pl.ds(2 * k, 2)].reshape(step, width),
+                (((1,), (1,)), ((), ())),
+                preferred_element_type=jnp.float32,
+            ).astype(jnp.bfloat16)
+            for i in range(n_out):
+                outs[i][:, pl.ds(pl.multiple_of(k * step, step), step)] = part[
+                    i * per_out : (i + 1) * per_out
+                ]
         return carry
 
-    lax.fori_loop(0, RING, leave, 0)
-
-
-def ffn(coord, weights, xs, n_out):
+    lax.fori_loop(0, turns, leave, 0)
+
+
+def ffn(w, xs, n_out):
     rows = sum(v.shape[0] for v in xs)
     model = xs[0].shape[1]
-    width = weights[0].shape[-1]
+    width = w.shape[-1]
     vm = pl.BlockSpec(memory_space=pltpu.VMEM)
-    hb = pl.BlockSpec(memory_space=pltpu.HBM)
-    flops = 6 * rows * model * width
     return pl.pallas_call(
         functools.partial(ffn_body, len(xs), n_out),
         out_shape=[jax.ShapeDtypeStruct((rows // n_out, model), jnp.bfloat16)] * n_out,
-        in_specs=[pl.BlockSpec(memory_space=pltpu.SMEM)] + [vm] * len(xs) + [hb] * len(weights),
+        in_specs=[vm] * (len(xs) + 1),
         out_specs=[vm] * n_out,
         scratch_shapes=[
-            pltpu.VMEM((3, 16, 2, 64, width), jnp.bfloat16),
             pltpu.VMEM((rows, model), jnp.bfloat16),
-            pltpu.VMEM((rows, width), jnp.float32),
-            pltpu.VMEM((rows, width), jnp.float32),
+            pltpu.VMEM((2, rows, width), jnp.float32),
             pltpu.VMEM((rows, width), jnp.bfloat16),
-            pltpu.SemaphoreType.DMA((2, 16)),
-            pltpu.SemaphoreType.DMA((2, 16)),
         ],
-        compiler_params=pltpu.CompilerParams(vmem_limit_bytes=48 * 1024 * 1024),
-        cost_estimate=pl.CostEstimate(
-            flops=flops, bytes_accessed=6 * model * width, transcendentals=rows * width
-        ),
+        compiler_params=pltpu.CompilerParams(vmem_limit_bytes=LIMIT),
         name="ffn_rows",
-    )(coord, *xs, *weights)
+    )(*xs, w)
 
 
 def summed_decay(ld, scratch, span):
@@ -284,7 +285,7 @@
         in_specs=[pl.BlockSpec(memory_space=pltpu.SMEM)] * smem + [vm] * (len(args) - smem),
         out_specs=jax.tree.map(lambda _: vm, out_shape),
         scratch_shapes=list(scratch),
-        compiler_params=pltpu.CompilerParams(vmem_limit_bytes=40 * 1024 * 1024),
+        compiler_params=pltpu.CompilerParams(vmem_limit_bytes=LIMIT),
     )(*args)
 
 
@@ -479,8 +480,11 @@
     r_b = lax.ppermute(h_b, "tp", up1)
     l_a = lax.ppermute(h_a, "tp", down1)
 
+    w = place(coord, weights, (0, 1, 2, 3, 6, 7))
+    w = place(coord, weights, (4, 5), w)
+
     def feed(*xs):
-        return ffn(coord, weights, xs, 2)
+        return ffn(w, xs, 2)
 
     right_a, left_b = feed(r_a, l_b)
     opp_a, opp_b = feed(far_a, far_b)

time: 183 us -> 176 us (0.962)
  waiting for transfers between devices: 39.7 us -> 57 us
  starting transfers between devices: 77.3 us -> 64.2 us
  Pallas kernels: 57.1 us -> 44.2 us
    pallas_call x4, Pallas kernels: 43.6 us -> 24.4 us  [ffn(): pl.pallas_call(functools.partial(ffn_body, len(xs), n_out), out_shape=[ja...]
    ppermute x1, waiting for transfers between devices: 0.01 us -> 11.2 us  [layer(): lax.ppermute((wide(right_b) + wide(far_in_b)).astype(bf16), 'tp', down1)]
    ppermute x1, waiting for transfers between devices: 9.43 us -> 3.03 us  [layer(): far_a = lax.ppermute(r_a, 'tp', up1)]
    pallas_call x0 -> x2, Pallas kernels: none -> 5.42 us  [place(): pl.pallas_call(functools.partial(place_body, chosen), out_shape=jax.Shape...]
    ppermute x3, waiting for transfers between devices: 11.2 us -> 15.8 us  [layer(): lax.ppermute(turned[k], 'tp', along(k))]
    ppermute x1, waiting for transfers between devices: 0.01 us -> 3.92 us  [layer(): o_far2 = lax.ppermute(o_far, 'sp_2', flipped(2, 1))]
    ppermute x3, starting transfers between devices: 3.59 us -> 0.08 us  [layer(): lax.ppermute(turned[k], 'tp', along(k))]
    ppermute x1, starting transfers between devices: 4.39 us -> 1.01 us  [gather_weights(): ra = lax.ppermute(s0, SP, wide(1))]
  transfers between devices with their start and end apart: 43 -> 43, of which waited for: 11 -> 16; matrix products, arithmetic and copies ran while one was open for 2% -> 2% of each run, Pallas kernels for 31% -> 25%
where the time goes in v1:
time: 176 us; the launch traced here: 173 us
  starting transfers between devices  64.2 us (36%)
  waiting for transfers between devices  57 us (32%)
  Pallas kernels  44.2 us (25%)
  other arithmetic  5.28 us (3%)
    pallas_call x4, Pallas kernels, ffn(): pl.pallas_call(functools.partial(ffn_body, len(xs), n_out), out_shape=[ja...  24.4 us
    ppermute x8, starting transfers between devices, gather_weights(): return own + [lax.ppermute(v, 'sp_2', flipped(2, 1)) for v in own]  18.2 us
    ppermute x3, waiting for transfers between devices, layer(): lax.ppermute(turned[k], 'tp', along(k))  15.8 us
    pallas_call x7, Pallas kernels, vmem_call(): pl.pallas_call(body, out_shape=out_shape, in_specs=[pl.BlockSpec(memory_s...  14.4 us
    ppermute x1, waiting for transfers between devices, layer(): lax.ppermute((wide(right_b) + wide(far_in_b)).astype(bf16), 'tp', down1)  11.2 us
    ppermute x1, waiting for transfers between devices, layer(): r_a = lax.ppermute(h_a, 'tp', up1)  11.1 us
    ppermute x3, starting transfers between devices, layer(): lax.ppermute(message, 'sp_0', [(i, i + k) for i in range(RING - k)])  8.56 us
    pallas_call x2, Pallas kernels, place(): pl.pallas_call(functools.partial(place_body, chosen), out_shape=jax.Shape...  5.42 us
  transfers between devices with their start and end apart: 43, of which 16 were waited for; matrix products, arithmetic and copies ran while one was open for 2% of the time, Pallas kernels for 25%

profile of v1, /device:TPU:1, one launch (start us, length us, event | category | flops | bytes accessed | tf_op | source)
XLA Modules:
  0.0 172.7 jit_solution(1855388478320978682)
XLA Ops:
  0.0 2.2 %fusion = (bf16[1,3,64,1408]{3,2,1,0:T(8,128)(2,1)}, bf16[3,64,1408]{2,1,0:T(8,128)(2,1)}) fusion(bf16[1,64,1408]{2,1,0:T(8,128)(2,1)} %bitcast.25, bf16[1,64,1408]{2,1,0:T(8,128)(2,1)} %bitcast.26, bf16[1,64,1408]{2,1,0:T(8,128)(2,1)} %bitcast.27), kind=kLoop, calls=%fused_computation.7 | loop fusion | flops 540672 | bytes 1622016 | tf_op jit(solution)/shard_map/stack | solution.py:48
  2.3 4.6 %collective-permute-start.17 = (bf16[3,64,1408]{2,1,0:T(8,128)(2,1)}, bf16[3,64,1408]{2,1,0:T(8,128)(2,1)S(1)}, u32[]{:S(2)}, u32[]{:S(2)}) collective-permute-start(bf16[3,64,1408]{2,1,0:T(8,128)(2,1)} %get-tuple-element.52), channel_id=1, source_target_pairs={{0,24},{4,100},{8,0},{12,108},{16,8},{20,116},{24,16},{28,124},{32... | collective-permute-start | bytes 1622024 | tf_op jit(solution)/shard_map/ppermute | solution.py:46
  6.8 2.5 %collective-permute-start.10 = (bf16[256,2048]{1,0:T(8,128)(2,1)}, bf16[256,2048]{1,0:T(8,128)(2,1)S(1)}, u32[]{:S(2)}, u32[]{:S(2)}) collective-permute-start(bf16[256,2048]{1,0:T(8,128)(2,1)} %own.1), channel_id=1, source_target_pairs={{0,1},{1,2},{2,3},{3,0},{4,7},{5,4},{6,5},{7,6},{8,9},{9,10},{10,1... | collective-permute-start | bytes 3145736 | tf_op jit(solution)/shard_map/ppermute | solution.py:425
  15.7 3.6 %collective-permute-done.17 = bf16[3,64,1408]{2,1,0:T(8,128)(2,1)S(1)} collective-permute-done((bf16[3,64,1408]{2,1,0:T(8,128)(2,1)}, bf16[3,64,1408]{2,1,0:T(8,128)(2,1)S(1)}, u32[]{:S(2)}, u32[]{:S(2)}) %collective-permute-start.17) | collective-permute-done | bytes 540704 | tf_op jit(solution)/shard_map/ppermute | solution.py:46
  19.2 2.9 %collective-permute-start.2 = (bf16[2,144,128]{2,1,0:T(8,128)(2,1)}, bf16[2,144,128]{2,1,0:T(8,128)(2,1)S(1)}, u32[]{:S(2)}, u32[]{:S(2)}) collective-permute-start(bf16[2,144,128]{2,1,0:T(8,128)(2,1)} %get-tuple-element.33), channel_id=1, source_target_pairs={{0,16},{8,24},{16,0},{24,8},{1,17},{9,25},{17,1},{25,9},{2,18},{10... | collective-permute-start | bytes 221192 | tf_op jit(solution)/shard_map/ppermute | solution.py:451
  28.8 4.8 %collective-permute-start.4 = (bf16[2,144,128]{2,1,0:T(8,128)(2,1)S(1)}, bf16[2,144,128]{2,1,0:T(8,128)(2,1)S(1)}, u32[]{:S(2)}, u32[]{:S(2)}) collective-permute-start(bf16[2,144,128]{2,1,0:T(8,128)(2,1)S(1)} %get-tuple-element.35), channel_id=1, source_target_pairs={{0,96},{1,97},{2,98},{3,99},{4,100},{5,101},{6,102},{7,103},{8,104... | collective-permute-start | bytes 221192 | tf_op jit(solution)/shard_map/ppermute | solution.py:455
  37.4 2.4 %collective-permute-start.12 = (bf16[128,2048]{1,0:T(8,128)(2,1)S(1)}, bf16[128,2048]{1,0:T(8,128)(2,1)S(1)}, u32[]{:S(2)}, u32[]{:S(2)}) collective-permute-start(bf16[128,2048]{1,0:T(8,128)(2,1)S(1)} %constant_dynamic-slice_fusion), channel_id=1, source_target_pairs={{0,1},{1,2},{2,3},{3,0},{4,7},{5,4},{6,5},{7,6},{8,9},{9,10},{10,1... | collective-permute-start | bytes 1572872 | tf_op jit(solution)/shard_map/ppermute | solution.py:427
  39.8 2.5 %collective-permute-start.6 = (bf16[2,144,128]{2,1,0:T(8,128)(2,1)S(1)}, bf16[2,144,128]{2,1,0:T(8,128)(2,1)S(1)}, u32[]{:S(2)}, u32[]{:S(2)}) collective-permute-start(bf16[2,144,128]{2,1,0:T(8,128)(2,1)S(1)} %get-tuple-element.35), channel_id=1, source_target_pairs={{0,32},{32,64},{64,96},{1,33},{33,65},{65,97},{2,34},{34,66},{66,9... | collective-permute-start | bytes 221192 | tf_op jit(solution)/shard_map/ppermute | solution.py:455
  42.3 2.8 %shard_map.137.within = f32[1024,256]{1,0:T(8,128)S(1)} custom-call(f32[2,1024]{1,0:T(2,128)S(1)} %bitcast.19, bf16[1024,256]{1,0:T(8,128)(2,1)S(1)} %copy-done, bf16[1024,256]{1,0:T(8,128)(2,1)S(1)} %copy-done.1, bf16[1024,256]{1,0:T(8,128)(2,1)S(1)} %copy-done.2, f32[2,128,128]{2,1,0:T(8,128)S(1)} %copy-done.7), custom_call_target="tpu_custom_call" | custom-call | tf_op jit(solution)/shard_map/pallas_call | solution.py:282
  45.2 2.7 %shard_map.140 = (bf16[256,256]{1,0:T(8,128)(2,1)S(1)}, bf16[256,256]{1,0:T(8,128)(2,1)S(1)}, bf16[256,256]{1,0:T(8,128)(2,1)S(1)}, bf16[256,256]{1,0:T(8,128)(2,1)S(1)}) custom-call(s32[4]{0:T(128)S(1)} %pad_add_fusion.coord, f32[2,1024]{1,0:T(2,128)S(1)} %bitcast.20, bf16[1024,256]{1,0:T(8,128)(2,1)S(1)} %copy-done, f32[1024,256]{1,0:T(8,128)S(1)} %shard_map.137.within, ...), custom_call_target="tpu_custom_call" | custom-call | tf_op jit(solution)/shard_map/pallas_call | solution.py:282
  48.0 6.7 %collective-permute-done.7.r1 = bf16[256,256]{1,0:T(8,128)(2,1)S(1)} collective-permute-done((bf16[256,256]{1,0:T(8,128)(2,1)S(1)}, bf16[256,256]{1,0:T(8,128)(2,1)S(1)}, u32[]{:S(2)}, u32[]{:S(2)}) %collective-permute-start.7) | collective-permute-done | bytes 131104 | tf_op jit(solution)/shard_map/ppermute | solution.py:465
  54.7 5.3 %collective-permute-done.8.r2 = bf16[256,256]{1,0:T(8,128)(2,1)S(1)} collective-permute-done((bf16[256,256]{1,0:T(8,128)(2,1)S(1)}, bf16[256,256]{1,0:T(8,128)(2,1)S(1)}, u32[]{:S(2)}, u32[]{:S(2)}) %collective-permute-start.8) | collective-permute-done | bytes 131104 | tf_op jit(solution)/shard_map/ppermute | solution.py:465
  60.0 3.8 %collective-permute-done.9.r3 = bf16[256,256]{1,0:T(8,128)(2,1)S(1)} collective-permute-done((bf16[256,256]{1,0:T(8,128)(2,1)S(1)}, bf16[256,256]{1,0:T(8,128)(2,1)S(1)}, u32[]{:S(2)}, u32[]{:S(2)}) %collective-permute-start.9) | collective-permute-done | bytes 131104 | tf_op jit(solution)/shard_map/ppermute | solution.py:465
  63.9 14.7 %collective-permute-start.26 = (bf16[2,3,64,1408]{3,2,1,0:T(8,128)(2,1)S(1)}, bf16[2,3,64,1408]{3,2,1,0:T(8,128)(2,1)S(1)}, u32[]{:S(2)}, u32[]{:S(2)}) collective-permute-start(bf16[2,3,64,1408]{3,2,1,0:T(8,128)(2,1)S(1)} %pad_maximum_fusion.1.refs_1_), channel_id=1, source_target_pairs={{0,4},{4,0},{1,5},{5,1},{2,6},{6,2},{3,7},{7,3},{8,12},{12,8},{9,1... | collective-permute-start | bytes 3244040 | tf_op jit(solution)/shard_map/ppermute | solution.py:57
  78.5 2.6 %collective-permute-start.24 = (bf16[2,3,64,1408]{3,2,1,0:T(8,128)(2,1)S(1)}, bf16[2,3,64,1408]{3,2,1,0:T(8,128)(2,1)S(1)}, u32[]{:S(2)}, u32[]{:S(2)}) collective-permute-start(bf16[2,3,64,1408]{3,2,1,0:T(8,128)(2,1)S(1)} %pad_maximum_fusion.refs_0_), channel_id=1, source_target_pairs={{0,96},{4,28},{8,104},{12,4},{16,112},{20,12},{24,120},{28,20},{32... | collective-permute-start | bytes 3244040 | tf_op jit(solution)/shard_map/ppermute | solution.py:55
  82.1 3.9 %collective-permute-done.13.far2 = bf16[128,2048]{1,0:T(8,128)(2,1)S(1)} collective-permute-done((bf16[128,2048]{1,0:T(8,128)(2,1)S(1)}, bf16[128,2048]{1,0:T(8,128)(2,1)S(1)}, u32[]{:S(2)}, u32[]{:S(2)}) %collective-permute-start.13) | collective-permute-done | bytes 524320 | tf_op jit(solution)/shard_map/ppermute | solution.py:429
  86.1 2.0 %collective-permute-start.20 = (bf16[2,3,64,1408]{3,2,1,0:T(8,128)(2,1)}, bf16[2,3,64,1408]{3,2,1,0:T(8,128)(2,1)S(1)}, u32[]{:S(2)}, u32[]{:S(2)}) collective-permute-start(bf16[2,3,64,1408]{3,2,1,0:T(8,128)(2,1)} %collective-permute-done.19.refs_3_), channel_id=1, source_target_pairs={{0,96},{4,28},{8,104},{12,4},{16,112},{20,12},{24,120},{28,20},{32... | collective-permute-start | bytes 3244040 | tf_op jit(solution)/shard_map/ppermute | solution.py:53
  88.1 3.0 %shard_map.141 = (bf16[256,2048]{1,0:T(8,128)(2,1)S(1)}, bf16[128,2048]{1,0:T(8,128)(2,1)S(1)}, bf16[128,2048]{1,0:T(8,128)(2,1)S(1)}) custom-call(s32[4]{0:T(128)S(1)} %pad_add_fusion.coord, bf16[256,256]{1,0:T(8,128)(2,1)S(1)} %get-tuple-element.36.r0, bf16[256,256]{1,0:T(8,128)(2,1)S(1)} %collective-permute-done.7.r1, ...), custom_call_target="tpu_custom_call" | custom-call | tf_op jit(solution)/shard_map/pallas_call | solution.py:282
  91.2 2.0 %collective-permute-done.24.refs_5_ = bf16[2,3,64,1408]{3,2,1,0:T(8,128)(2,1)S(1)} collective-permute-done((bf16[2,3,64,1408]{3,2,1,0:T(8,128)(2,1)S(1)}, bf16[2,3,64,1408]{3,2,1,0:T(8,128)(2,1)S(1)}, u32[]{:S(2)}, u32[]{:S(2)}) %collective-permute-start.24) | collective-permute-done | bytes 1081376 | tf_op jit(solution)/shard_map/ppermute | solution.py:55
  93.2 2.7 %collective-permute-start.35 = (bf16[128,2048]{1,0:T(8,128)(2,1)S(1)}, bf16[128,2048]{1,0:T(8,128)(2,1)S(1)}, u32[]{:S(2)}, u32[]{:S(2)}) collective-permute-start(bf16[128,2048]{1,0:T(8,128)(2,1)S(1)} %get-tuple-element.41.refs_1_), channel_id=1, source_target_pairs={{0,3},{1,0},{2,1},{3,2},{4,7},{5,4},{6,5},{7,6},{8,11},{9,8},{10,9... | collective-permute-start | bytes 1572872 | tf_op jit(solution)/shard_map/ppermute | solution.py:477
  95.9 11.1 %collective-permute-done.33.refs_0_ = bf16[128,2048]{1,0:T(8,128)(2,1)S(1)} collective-permute-done((bf16[128,2048]{1,0:T(8,128)(2,1)S(1)}, bf16[128,2048]{1,0:T(8,128)(2,1)S(1)}, u32[]{:S(2)}, u32[]{:S(2)}) %collective-permute-start.33) | collective-permute-done | bytes 524320 | tf_op jit(solution)/shard_map/ppermute | solution.py:476
  114.4 3.8 %shard_map.142.refs_4_ = bf16[3,16,2,64,1408]{4,3,2,1,0:T(8,128)(2,1)S(1)} custom-call(s32[4]{0:T(128)S(1)} %pad_add_fusion.coord, bf16[2,3,64,1408]{3,2,1,0:T(8,128)(2,1)S(1)} %pad_maximum_fusion.refs_0_, bf16[2,3,64,1408]{3,2,1,0:T(8,128)(2,1)S(1)} %pad_maximum_fusion.1.refs_1_, bf16[2,3,64,1408]{3,2,1,0:T(8,128)(2,1)S(1)} %collective-permute-done.15.refs_2_, ...), custom_call_target="tpu_custom_call" | custom-call | tf_op jit(solution)/shard_map/pallas_call | solution.py:104
  118.2 2.7 %collective-permute-start.32 = (bf16[128,2048]{1,0:T(8,128)(2,1)S(1)}, bf16[128,2048]{1,0:T(8,128)(2,1)S(1)}, u32[]{:S(2)}, u32[]{:S(2)}) collective-permute-start(bf16[128,2048]{1,0:T(8,128)(2,1)S(1)} %get-tuple-element.40.refs_0_), channel_id=1, source_target_pairs={{0,3},{1,0},{2,1},{3,2},{4,7},{5,4},{6,5},{7,6},{8,11},{9,8},{10,9... | collective-permute-start | bytes 1572872 | tf_op jit(solution)/shard_map/ppermute | solution.py:481
  122.6 3.0 %collective-permute-done.34.refs_0_ = bf16[128,2048]{1,0:T(8,128)(2,1)S(1)} collective-permute-done((bf16[128,2048]{1,0:T(8,128)(2,1)S(1)}, bf16[128,2048]{1,0:T(8,128)(2,1)S(1)}, u32[]{:S(2)}, u32[]{:S(2)}) %collective-permute-start.34) | collective-permute-done | bytes 524320 | tf_op jit(solution)/shard_map/ppermute | solution.py:478
  125.9 6.1 %ffn_rows.6 = (bf16[128,2048]{1,0:T(8,128)(2,1)S(1)}, bf16[128,2048]{1,0:T(8,128)(2,1)S(1)}) custom-call(bf16[128,2048]{1,0:T(8,128)(2,1)S(1)} %collective-permute-done.34.refs_0_, bf16[128,2048]{1,0:T(8,128)(2,1)S(1)} %collective-permute-done.36.refs_1_, bf16[3,16,2,64,1408]{4,3,2,1,0:T(8,128)(2,1)S(1)} %shard_map.143.refs_2_), custom_call_target="tpu_custom_call" | custom-call | tf_op jit(solution)/shard_map/ffn_rows/pallas_call | solution.py:160
  132.0 2.6 %collective-permute-start.39 = (bf16[128,2048]{1,0:T(8,128)(2,1)S(1)}, bf16[128,2048]{1,0:T(8,128)(2,1)S(1)}, u32[]{:S(2)}, u32[]{:S(2)}) collective-permute-start(bf16[128,2048]{1,0:T(8,128)(2,1)S(1)} %get-tuple-element.47), channel_id=1, source_target_pairs={{0,3},{1,0},{2,1},{3,2},{4,7},{5,4},{6,5},{7,6},{8,11},{9,8},{10,9... | collective-permute-start | bytes 1572872 | tf_op jit(solution)/shard_map/ppermute | solution.py:496
  134.7 6.1 %ffn_rows.7 = (bf16[128,2048]{1,0:T(8,128)(2,1)S(1)}, bf16[128,2048]{1,0:T(8,128)(2,1)S(1)}) custom-call(bf16[128,2048]{1,0:T(8,128)(2,1)S(1)} %collective-permute-done.33.refs_0_, bf16[128,2048]{1,0:T(8,128)(2,1)S(1)} %collective-permute-done.35.refs_1_, bf16[3,16,2,64,1408]{4,3,2,1,0:T(8,128)(2,1)S(1)} %shard_map.143.refs_2_), custom_call_target="tpu_custom_call" | custom-call | tf_op jit(solution)/shard_map/ffn_rows/pallas_call | solution.py:160
  140.8 2.7 %collective-permute-start.41 = (bf16[128,2048]{1,0:T(8,128)(2,1)S(1)}, bf16[128,2048]{1,0:T(8,128)(2,1)S(1)}, u32[]{:S(2)}, u32[]{:S(2)}) collective-permute-start(bf16[128,2048]{1,0:T(8,128)(2,1)S(1)} %get-tuple-element.48), channel_id=1, source_target_pairs={{0,3},{1,0},{2,1},{3,2},{4,7},{5,4},{6,5},{7,6},{8,11},{9,8},{10,9... | collective-permute-start | bytes 1572872 | tf_op jit(solution)/shard_map/ppermute | solution.py:494
  143.5 6.1 %ffn_rows.5 = (bf16[128,2048]{1,0:T(8,128)(2,1)S(1)}, bf16[128,2048]{1,0:T(8,128)(2,1)S(1)}) custom-call(bf16[128,2048]{1,0:T(8,128)(2,1)S(1)} %collective-permute-done.31.refs_0_, bf16[128,2048]{1,0:T(8,128)(2,1)S(1)} %collective-permute-done.32.refs_1_, bf16[3,16,2,64,1408]{4,3,2,1,0:T(8,128)(2,1)S(1)} %shard_map.143.refs_2_), custom_call_target="tpu_custom_call" | custom-call | tf_op jit(solution)/shard_map/ffn_rows/pallas_call | solution.py:160
  149.8 2.7 %collective-permute-start.40 = (bf16[128,2048]{1,0:T(8,128)(2,1)S(1)}, bf16[128,2048]{1,0:T(8,128)(2,1)S(1)}, u32[]{:S(2)}, u32[]{:S(2)}) collective-permute-start(bf16[128,2048]{1,0:T(8,128)(2,1)S(1)} %add_convert_fusion), channel_id=1, source_target_pairs={{0,3},{1,0},{2,1},{3,2},{4,7},{5,4},{6,5},{7,6},{8,11},{9,8},{10,9... | collective-permute-start | bytes 1572872 | tf_op jit(solution)/shard_map/ppermute | solution.py:499
  152.7 6.1 %ffn_rows.4 = (bf16[128,2048]{1,0:T(8,128)(2,1)S(1)}, bf16[128,2048]{1,0:T(8,128)(2,1)S(1)}) custom-call(bf16[128,2048]{1,0:T(8,128)(2,1)S(1)} %get-tuple-element.40.refs_0_, bf16[128,2048]{1,0:T(8,128)(2,1)S(1)} %get-tuple-element.41.refs_1_, bf16[3,16,2,64,1408]{4,3,2,1,0:T(8,128)(2,1)S(1)} %shard_map.143.refs_2_), custom_call_target="tpu_custom_call" | custom-call | tf_op jit(solution)/shard_map/ffn_rows/pallas_call | solution.py:160
  159.7 11.2 %collective-permute-done.40.sum_b = bf16[128,2048]{1,0:T(8,128)(2,1)S(1)} collective-permute-done((bf16[128,2048]{1,0:T(8,128)(2,1)S(1)}, bf16[128,2048]{1,0:T(8,128)(2,1)S(1)}, u32[]{:S(2)}, u32[]{:S(2)}) %collective-permute-start.40) | collective-permute-done | bytes 524320 | tf_op jit(solution)/shard_map/ppermute | solution.py:499
  (106 shorter events, 30.3 us)
Async XLA Ops:
  2.3 17.0 %collective-permute-start.17 = (bf16[3,64,1408]{2,1,0:T(8,128)(2,1)}, bf16[3,64,1408]{2,1,0:T(8,128)(2,1)S(1)}, u32[]{:S(2)}, u32[]{:S(2)}) collective-permute-start(bf16[3,64,1408]{2,1,0:T(8,128)(2,1)} %get-tuple-element.52), channel_id=1, source_target_pairs={{0,24},{4,100},{8,0},{12,108},{16,8},{20,116},{24,16},{28,124},{32... | collective-permute-start | bytes 1622024 | tf_op jit(solution)/shard_map/ppermute | solution.py:46
  6.8 15.3 %collective-permute-start.18 = (bf16[3,64,1408]{2,1,0:T(8,128)(2,1)}, bf16[3,64,1408]{2,1,0:T(8,128)(2,1)}, u32[]{:S(2)}, u32[]{:S(2)}) collective-permute-start(bf16[3,64,1408]{2,1,0:T(8,128)(2,1)} %get-tuple-element.52), channel_id=1, source_target_pairs={{0,16},{4,68},{8,24},{12,76},{16,0},{20,84},{24,8},{28,92},{32,48}... | collective-permute-start | bytes 1622024 | tf_op jit(solution)/shard_map/ppermute | solution.py:47
  6.8 29.5 %collective-permute-start.10 = (bf16[256,2048]{1,0:T(8,128)(2,1)}, bf16[256,2048]{1,0:T(8,128)(2,1)S(1)}, u32[]{:S(2)}, u32[]{:S(2)}) collective-permute-start(bf16[256,2048]{1,0:T(8,128)(2,1)} %own.1), channel_id=1, source_target_pairs={{0,1},{1,2},{2,3},{3,0},{4,7},{5,4},{6,5},{7,6},{8,9},{9,10},{10,1... | collective-permute-start | bytes 3145736 | tf_op jit(solution)/shard_map/ppermute | solution.py:425
  9.3 24.3 %collective-permute-start.14 = (bf16[3,64,1408]{2,1,0:T(8,128)(2,1)}, bf16[3,64,1408]{2,1,0:T(8,128)(2,1)}, u32[]{:S(2)}, u32[]{:S(2)}) collective-permute-start(bf16[3,64,1408]{2,1,0:T(8,128)(2,1)} %get-tuple-element.52), channel_id=1, source_target_pairs={{0,8},{4,36},{8,16},{12,44},{16,24},{20,52},{24,0},{28,60},{32,40}... | collective-permute-start | bytes 1622024 | tf_op jit(solution)/shard_map/ppermute | solution.py:45
  14.4 9.9 %collective-permute-start.1 = (bf16[2,144,128]{2,1,0:T(8,128)(2,1)}, bf16[2,144,128]{2,1,0:T(8,128)(2,1)S(1)}, u32[]{:S(2)}, u32[]{:S(2)}) collective-permute-start(bf16[2,144,128]{2,1,0:T(8,128)(2,1)} %get-tuple-element.33), channel_id=1, source_target_pairs={{0,8},{8,16},{16,24},{24,0},{1,9},{9,17},{17,25},{25,1},{2,10},{10... | collective-permute-start | bytes 221192 | tf_op jit(solution)/shard_map/ppermute | solution.py:451
  24.3 56.8 %collective-permute-start.19 = (bf16[2,3,64,1408]{3,2,1,0:T(8,128)(2,1)S(1)}, bf16[2,3,64,1408]{3,2,1,0:T(8,128)(2,1)}, u32[]{:S(2)}, u32[]{:S(2)}) collective-permute-start(bf16[2,3,64,1408]{3,2,1,0:T(8,128)(2,1)S(1)} %pad_maximum_fusion.1.refs_1_), channel_id=1, source_target_pairs={{0,96},{4,28},{8,104},{12,4},{16,112},{20,12},{24,120},{28,20},{32... | collective-permute-start | bytes 3244040 | tf_op jit(solution)/shard_map/ppermute | solution.py:51
  25.6 55.5 %collective-permute-start.23 = (bf16[2,3,64,1408]{3,2,1,0:T(8,128)(2,1)S(1)}, bf16[2,3,64,1408]{3,2,1,0:T(8,128)(2,1)}, u32[]{:S(2)}, u32[]{:S(2)}) collective-permute-start(bf16[2,3,64,1408]{3,2,1,0:T(8,128)(2,1)S(1)} %pad_maximum_fusion.1.refs_1_), channel_id=1, source_target_pairs={{0,32},{4,12},{8,40},{12,20},{16,48},{20,28},{24,56},{28,4},{32,64... | collective-permute-start | bytes 3244040 | tf_op jit(solution)/shard_map/ppermute | solution.py:54
  28.8 8.6 %collective-permute-start.4 = (bf16[2,144,128]{2,1,0:T(8,128)(2,1)S(1)}, bf16[2,144,128]{2,1,0:T(8,128)(2,1)S(1)}, u32[]{:S(2)}, u32[]{:S(2)}) collective-permute-start(bf16[2,144,128]{2,1,0:T(8,128)(2,1)S(1)} %get-tuple-element.35), channel_id=1, source_target_pairs={{0,96},{1,97},{2,98},{3,99},{4,100},{5,101},{6,102},{7,103},{8,104... | collective-permute-start | bytes 221192 | tf_op jit(solution)/shard_map/ppermute | solution.py:455
  36.3 45.3 %collective-permute-start.15 = (bf16[2,3,64,1408]{3,2,1,0:T(8,128)(2,1)S(1)}, bf16[2,3,64,1408]{3,2,1,0:T(8,128)(2,1)S(1)}, u32[]{:S(2)}, u32[]{:S(2)}) collective-permute-start(bf16[2,3,64,1408]{3,2,1,0:T(8,128)(2,1)S(1)} %pad_maximum_fusion.refs_0_), channel_id=1, source_target_pairs={{0,32},{4,12},{8,40},{12,20},{16,48},{20,28},{24,56},{28,4},{32,64... | collective-permute-start | bytes 3244040 | tf_op jit(solution)/shard_map/ppermute | solution.py:50
  37.4 41.1 %collective-permute-start.12 = (bf16[128,2048]{1,0:T(8,128)(2,1)S(1)}, bf16[128,2048]{1,0:T(8,128)(2,1)S(1)}, u32[]{:S(2)}, u32[]{:S(2)}) collective-permute-start(bf16[128,2048]{1,0:T(8,128)(2,1)S(1)} %constant_dynamic-slice_fusion), channel_id=1, source_target_pairs={{0,1},{1,2},{2,3},{3,0},{4,7},{5,4},{6,5},{7,6},{8,9},{9,10},{10,1... | collective-permute-start | bytes 1572872 | tf_op jit(solution)/shard_map/ppermute | solution.py:427
  47.9 6.8 %collective-permute-start.7 = (bf16[256,256]{1,0:T(8,128)(2,1)S(1)}, bf16[256,256]{1,0:T(8,128)(2,1)S(1)}, u32[]{:S(2)}, u32[]{:S(2)}) collective-permute-start(bf16[256,256]{1,0:T(8,128)(2,1)S(1)} %get-tuple-element.37), channel_id=1, source_target_pairs={{0,1},{1,2},{2,3},{3,0},{4,5},{5,6},{6,7},{7,4},{8,9},{9,10},{10,1... | collective-permute-start | bytes 393224 | tf_op jit(solution)/shard_map/ppermute | solution.py:465
  63.9 18.0 %collective-permute-start.26 = (bf16[2,3,64,1408]{3,2,1,0:T(8,128)(2,1)S(1)}, bf16[2,3,64,1408]{3,2,1,0:T(8,128)(2,1)S(1)}, u32[]{:S(2)}, u32[]{:S(2)}) collective-permute-start(bf16[2,3,64,1408]{3,2,1,0:T(8,128)(2,1)S(1)} %pad_maximum_fusion.1.refs_1_), channel_id=1, source_target_pairs={{0,4},{4,0},{1,5},{5,1},{2,6},{6,2},{3,7},{7,3},{8,12},{12,8},{9,1... | collective-permute-start | bytes 3244040 | tf_op jit(solution)/shard_map/ppermute | solution.py:57
  78.5 14.7 %collective-permute-start.24 = (bf16[2,3,64,1408]{3,2,1,0:T(8,128)(2,1)S(1)}, bf16[2,3,64,1408]{3,2,1,0:T(8,128)(2,1)S(1)}, u32[]{:S(2)}, u32[]{:S(2)}) collective-permute-start(bf16[2,3,64,1408]{3,2,1,0:T(8,128)(2,1)S(1)} %pad_maximum_fusion.refs_0_), channel_id=1, source_target_pairs={{0,96},{4,28},{8,104},{12,4},{16,112},{20,12},{24,120},{28,20},{32... | collective-permute-start | bytes 3244040 | tf_op jit(solution)/shard_map/ppermute | solution.py:55
  81.1 7.0 %collective-permute-start.11 = (bf16[256,2048]{1,0:T(8,128)(2,1)S(1)}, bf16[256,2048]{1,0:T(8,128)(2,1)S(1)}, u32[]{:S(2)}, u32[]{:S(2)}) collective-permute-start(bf16[256,2048]{1,0:T(8,128)(2,1)S(1)} %collective-permute-done.10.near), channel_id=1, source_target_pairs={{0,4},{4,0},{1,5},{5,1},{2,6},{6,2},{3,7},{7,3},{8,12},{12,8},{9,1... | collective-permute-start | bytes 3145736 | tf_op jit(solution)/shard_map/ppermute | solution.py:428
  81.1 12.1 %collective-permute-start.25 = (bf16[2,3,64,1408]{3,2,1,0:T(8,128)(2,1)S(1)}, bf16[2,3,64,1408]{3,2,1,0:T(8,128)(2,1)S(1)}, u32[]{:S(2)}, u32[]{:S(2)}) collective-permute-start(bf16[2,3,64,1408]{3,2,1,0:T(8,128)(2,1)S(1)} %pad_maximum_fusion.refs_0_), channel_id=1, source_target_pairs={{0,4},{4,0},{1,5},{5,1},{2,6},{6,2},{3,7},{7,3},{8,12},{12,8},{9,1... | collective-permute-start | bytes 3244040 | tf_op jit(solution)/shard_map/ppermute | solution.py:57
  81.9 26.9 %collective-permute-start.28 = (bf16[2,3,64,1408]{3,2,1,0:T(8,128)(2,1)}, bf16[2,3,64,1408]{3,2,1,0:T(8,128)(2,1)S(1)}, u32[]{:S(2)}, u32[]{:S(2)}) collective-permute-start(bf16[2,3,64,1408]{3,2,1,0:T(8,128)(2,1)} %collective-permute-done.19.refs_3_), channel_id=1, source_target_pairs={{0,4},{4,0},{1,5},{5,1},{2,6},{6,2},{3,7},{7,3},{8,12},{12,8},{9,1... | collective-permute-start | bytes 3244040 | tf_op jit(solution)/shard_map/ppermute | solution.py:57
  86.1 23.2 %collective-permute-start.20 = (bf16[2,3,64,1408]{3,2,1,0:T(8,128)(2,1)}, bf16[2,3,64,1408]{3,2,1,0:T(8,128)(2,1)S(1)}, u32[]{:S(2)}, u32[]{:S(2)}) collective-permute-start(bf16[2,3,64,1408]{3,2,1,0:T(8,128)(2,1)} %collective-permute-done.19.refs_3_), channel_id=1, source_target_pairs={{0,96},{4,28},{8,104},{12,4},{16,112},{20,12},{24,120},{28,20},{32... | collective-permute-start | bytes 3244040 | tf_op jit(solution)/shard_map/ppermute | solution.py:53
  88.1 21.3 %collective-permute-start.16 = (bf16[2,3,64,1408]{3,2,1,0:T(8,128)(2,1)S(1)}, bf16[2,3,64,1408]{3,2,1,0:T(8,128)(2,1)S(1)}, u32[]{:S(2)}, u32[]{:S(2)}) collective-permute-start(bf16[2,3,64,1408]{3,2,1,0:T(8,128)(2,1)S(1)} %collective-permute-done.15.refs_2_), channel_id=1, source_target_pairs={{0,32},{4,12},{8,40},{12,20},{16,48},{20,28},{24,56},{28,4},{32,64... | collective-permute-start | bytes 3244040 | tf_op jit(solution)/shard_map/ppermute | solution.py:52
  93.2 13.8 %collective-permute-start.33 = (bf16[128,2048]{1,0:T(8,128)(2,1)S(1)}, bf16[128,2048]{1,0:T(8,128)(2,1)S(1)}, u32[]{:S(2)}, u32[]{:S(2)}) collective-permute-start(bf16[128,2048]{1,0:T(8,128)(2,1)S(1)} %get-tuple-element.40.refs_0_), channel_id=1, source_target_pairs={{0,1},{1,2},{2,3},{3,0},{4,5},{5,6},{6,7},{7,4},{8,9},{9,10},{10,1... | collective-permute-start | bytes 1572872 | tf_op jit(solution)/shard_map/ppermute | solution.py:476
  93.2 15.5 %collective-permute-start.35 = (bf16[128,2048]{1,0:T(8,128)(2,1)S(1)}, bf16[128,2048]{1,0:T(8,128)(2,1)S(1)}, u32[]{:S(2)}, u32[]{:S(2)}) collective-permute-start(bf16[128,2048]{1,0:T(8,128)(2,1)S(1)} %get-tuple-element.41.refs_1_), channel_id=1, source_target_pairs={{0,3},{1,0},{2,1},{3,2},{4,7},{5,4},{6,5},{7,6},{8,11},{9,8},{10,9... | collective-permute-start | bytes 1572872 | tf_op jit(solution)/shard_map/ppermute | solution.py:477
  109.3 8.9 %collective-permute-start.22 = (bf16[2,3,64,1408]{3,2,1,0:T(8,128)(2,1)S(1)}, bf16[2,3,64,1408]{3,2,1,0:T(8,128)(2,1)S(1)}, u32[]{:S(2)}, u32[]{:S(2)}) collective-permute-start(bf16[2,3,64,1408]{3,2,1,0:T(8,128)(2,1)S(1)} %collective-permute-done.20.refs_1_), channel_id=1, source_target_pairs={{0,4},{4,0},{1,5},{5,1},{2,6},{6,2},{3,7},{7,3},{8,12},{12,8},{9,1... | collective-permute-start | bytes 3244040 | tf_op jit(solution)/shard_map/ppermute | solution.py:57
  109.3 11.5 %collective-permute-start.21 = (bf16[2,3,64,1408]{3,2,1,0:T(8,128)(2,1)S(1)}, bf16[2,3,64,1408]{3,2,1,0:T(8,128)(2,1)S(1)}, u32[]{:S(2)}, u32[]{:S(2)}) collective-permute-start(bf16[2,3,64,1408]{3,2,1,0:T(8,128)(2,1)S(1)} %collective-permute-done.16.refs_0_), channel_id=1, source_target_pairs={{0,4},{4,0},{1,5},{5,1},{2,6},{6,2},{3,7},{7,3},{8,12},{12,8},{9,1... | collective-permute-start | bytes 3244040 | tf_op jit(solution)/shard_map/ppermute | solution.py:57
  111.3 14.3 %collective-permute-start.34 = (bf16[128,2048]{1,0:T(8,128)(2,1)S(1)}, bf16[128,2048]{1,0:T(8,128)(2,1)S(1)}, u32[]{:S(2)}, u32[]{:S(2)}) collective-permute-start(bf16[128,2048]{1,0:T(8,128)(2,1)S(1)} %collective-permute-done.33.refs_0_), channel_id=1, source_target_pairs={{0,1},{1,2},{2,3},{3,0},{4,5},{5,6},{6,7},{7,4},{8,9},{9,10},{10,1... | collective-permute-start | bytes 1572872 | tf_op jit(solution)/shard_map/ppermute | solution.py:478
  112.8 13.1 %collective-permute-start.36 = (bf16[128,2048]{1,0:T(8,128)(2,1)S(1)}, bf16[128,2048]{1,0:T(8,128)(2,1)S(1)}, u32[]{:S(2)}, u32[]{:S(2)}) collective-permute-start(bf16[128,2048]{1,0:T(8,128)(2,1)S(1)} %collective-permute-done.35.refs_1_), channel_id=1, source_target_pairs={{0,3},{1,0},{2,1},{3,2},{4,7},{5,4},{6,5},{7,6},{8,11},{9,8},{10,9... | collective-permute-start | bytes 1572872 | tf_op jit(solution)/shard_map/ppermute | solution.py:479
  114.4 29.1 %collective-permute-start.31 = (bf16[128,2048]{1,0:T(8,128)(2,1)S(1)}, bf16[128,2048]{1,0:T(8,128)(2,1)S(1)}, u32[]{:S(2)}, u32[]{:S(2)}) collective-permute-start(bf16[128,2048]{1,0:T(8,128)(2,1)S(1)} %get-tuple-element.41.refs_1_), channel_id=1, source_target_pairs={{0,1},{1,2},{2,3},{3,0},{4,5},{5,6},{6,7},{7,4},{8,9},{9,10},{10,1... | collective-permute-start | bytes 1572872 | tf_op jit(solution)/shard_map/ppermute | solution.py:480
  118.2 25.4 %collective-permute-start.32 = (bf16[128,2048]{1,0:T(8,128)(2,1)S(1)}, bf16[128,2048]{1,0:T(8,128)(2,1)S(1)}, u32[]{:S(2)}, u32[]{:S(2)}) collective-permute-start(bf16[128,2048]{1,0:T(8,128)(2,1)S(1)} %get-tuple-element.40.refs_0_), channel_id=1, source_target_pairs={{0,3},{1,0},{2,1},{3,2},{4,7},{5,4},{6,5},{7,6},{8,11},{9,8},{10,9... | collective-permute-start | bytes 1572872 | tf_op jit(solution)/shard_map/ppermute | solution.py:481
  132.0 17.6 %collective-permute-start.39 = (bf16[128,2048]{1,0:T(8,128)(2,1)S(1)}, bf16[128,2048]{1,0:T(8,128)(2,1)S(1)}, u32[]{:S(2)}, u32[]{:S(2)}) collective-permute-start(bf16[128,2048]{1,0:T(8,128)(2,1)S(1)} %get-tuple-element.47), channel_id=1, source_target_pairs={{0,3},{1,0},{2,1},{3,2},{4,7},{5,4},{6,5},{7,6},{8,11},{9,8},{10,9... | collective-permute-start | bytes 1572872 | tf_op jit(solution)/shard_map/ppermute | solution.py:496
  134.7 17.9 %collective-permute-start.37 = (bf16[128,2048]{1,0:T(8,128)(2,1)S(1)}, bf16[128,2048]{1,0:T(8,128)(2,1)S(1)}, u32[]{:S(2)}, u32[]{:S(2)}) collective-permute-start(bf16[128,2048]{1,0:T(8,128)(2,1)S(1)} %get-tuple-element.45), channel_id=1, source_target_pairs={{0,1},{1,2},{2,3},{3,0},{4,5},{5,6},{6,7},{7,4},{8,9},{9,10},{10,1... | collective-permute-start | bytes 1572872 | tf_op jit(solution)/shard_map/ppermute | solution.py:495
  140.8 18.9 %collective-permute-start.41 = (bf16[128,2048]{1,0:T(8,128)(2,1)S(1)}, bf16[128,2048]{1,0:T(8,128)(2,1)S(1)}, u32[]{:S(2)}, u32[]{:S(2)}) collective-permute-start(bf16[128,2048]{1,0:T(8,128)(2,1)S(1)} %get-tuple-element.48), channel_id=1, source_target_pairs={{0,3},{1,0},{2,1},{3,2},{4,7},{5,4},{6,5},{7,6},{8,11},{9,8},{10,9... | collective-permute-start | bytes 1572872 | tf_op jit(solution)/shard_map/ppermute | solution.py:494
  143.5 16.1 %collective-permute-start.42 = (bf16[128,2048]{1,0:T(8,128)(2,1)S(1)}, bf16[128,2048]{1,0:T(8,128)(2,1)S(1)}, u32[]{:S(2)}, u32[]{:S(2)}) collective-permute-start(bf16[128,2048]{1,0:T(8,128)(2,1)S(1)} %get-tuple-element.49), channel_id=1, source_target_pairs={{0,1},{1,2},{2,3},{3,0},{4,5},{5,6},{6,7},{7,4},{8,9},{9,10},{10,1... | collective-permute-start | bytes 1572872 | tf_op jit(solution)/shard_map/ppermute | solution.py:493
  149.8 21.1 %collective-permute-start.40 = (bf16[128,2048]{1,0:T(8,128)(2,1)S(1)}, bf16[128,2048]{1,0:T(8,128)(2,1)S(1)}, u32[]{:S(2)}, u32[]{:S(2)}) collective-permute-start(bf16[128,2048]{1,0:T(8,128)(2,1)S(1)} %add_convert_fusion), channel_id=1, source_target_pairs={{0,3},{1,0},{2,1},{3,2},{4,7},{5,4},{6,5},{7,6},{8,11},{9,8},{10,9... | collective-permute-start | bytes 1572872 | tf_op jit(solution)/shard_map/ppermute | solution.py:499
  152.7 18.2 %collective-permute-start.38 = (bf16[128,2048]{1,0:T(8,128)(2,1)S(1)}, bf16[128,2048]{1,0:T(8,128)(2,1)S(1)}, u32[]{:S(2)}, u32[]{:S(2)}) collective-permute-start(bf16[128,2048]{1,0:T(8,128)(2,1)S(1)} %add_convert_fusion.1), channel_id=1, source_target_pairs={{0,1},{1,2},{2,3},{3,0},{4,5},{5,6},{6,7},{7,4},{8,9},{9,10},{10,1... | collective-permute-start | bytes 1572872 | tf_op jit(solution)/shard_map/ppermute | solution.py:498
  (27 other events, 307.6 us)

commit v2 on v1

--- a/solution.py
+++ b/solution.py
@@ -38,15 +38,17 @@
     return [(i, i ^ bit) for i in range(size)]
 
 
-def gather_weights(w_gate, w_up, w_down):
-    mine = jnp.stack([w_gate, w_up, w_down.T])
+def near_shards(mine):
     near = functools.partial(role_shift, True)
+    return (
+        lax.ppermute(mine, SP, near(1)),
+        lax.ppermute(mine, SP, near(-1)),
+        lax.ppermute(mine, SP, near(2)),
+    )
+
+
+def far_shards(s0, s1):
     wide = functools.partial(role_shift, False)
-    right = lax.ppermute(mine, SP, near(1))
-    left = lax.ppermute(mine, SP, near(-1))
-    far = lax.ppermute(mine, SP, near(2))
-    s0 = jnp.stack([mine, right])
-    s1 = jnp.stack([left, far])
     ra = lax.ppermute(s0, SP, wide(1))
     lb = lax.ppermute(s1, SP, wide(-1))
     fa = lax.ppermute(ra, SP, wide(1))
@@ -193,40 +195,47 @@
     )
 
 
-def state_body(ld, k, v, whole, message, first, scratch):
-    rows, heads, depth = k.shape[0], ld.shape[0], first.shape[1]
+def block_state(row, col, k, v, h, b, depth):
+    lanes = slice(h * depth, (h + 1) * depth)
+    here = slice(b * BLOCK, (b + 1) * BLOCK)
+    last = row[h : h + 1, (b + 1) * BLOCK - 1 : (b + 1) * BLOCK]
+    to_end = jnp.exp(last - col[here, h : h + 1]) * depth ** (-0.5)
+    scaled = (k[here, lanes].astype(jnp.float32) * to_end).astype(jnp.bfloat16)
+    added = lax.dot_general(
+        scaled, v[here, lanes], (((0,), (0,)), ((), ())), preferred_element_type=jnp.float32
+    )
+    return added, last
+
+
+def state_body(ld, k, v, message, scratch):
+    rows, heads, depth = k.shape[0], ld.shape[0], message.shape[2]
     row, col = summed_decay(ld, scratch, BLOCK)
-    scale = depth ** (-0.5)
     for h in range(heads):
-        lanes = slice(h * depth, (h + 1) * depth)
-        state = None
-        total = 0.0
-        for b in range(rows // BLOCK):
-            here = slice(b * BLOCK, (b + 1) * BLOCK)
-            last = row[h : h + 1, (b + 1) * BLOCK - 1 : (b + 1) * BLOCK]
-            to_end = jnp.exp(last - col[here, h : h + 1]) * scale
-            scaled = (k[here, lanes].astype(jnp.float32) * to_end).astype(jnp.bfloat16)
-            added = lax.dot_general(
-                scaled, v[here, lanes], (((0,), (0,)), ((), ())), preferred_element_type=jnp.float32
-            )
+        state, total = block_state(row, col, k, v, h, 0, depth)
+        for b in range(1, rows // BLOCK):
+            added, last = block_state(row, col, k, v, h, b, depth)
+            state = jnp.exp(last) * state + added
             total = total + last
-            if b == 0:
-                first[h] = added
-                state = added
-            else:
-                state = jnp.exp(last) * state + added
-        decay = jnp.broadcast_to(jnp.exp(total), (1, depth))
-        write_state(whole, h, decay, state)
-        write_state(message, h, decay, state)
-
-
-def within_body(ld, q, k, v, first, out, scratch):
-    rows, heads, depth = q.shape[0], ld.shape[0], first.shape[1]
+        write_state(message, h, jnp.broadcast_to(jnp.exp(total), (1, depth)), state)
+
+
+def joining(one, other, out, sem):
+    made = [pltpu.make_async_copy(r, out.at[i], sem.at[i]) for i, r in enumerate((one, other))]
+    for copy in made:
+        copy.start()
+    return made
+
+
+def within_body(ld, q, k, v, near, far, out, both, scratch, sem):
+    rows, heads = q.shape[0], ld.shape[0]
+    depth = q.shape[1] // heads
+    copies = joining(near, far, both, sem)
     row, col = summed_decay(ld, scratch, BLOCK)
     scale = depth ** (-0.5)
     tile = BLOCK // 2
     for h in range(heads):
         lanes = slice(h * depth, (h + 1) * depth)
+        state = None
         for b in range(rows // BLOCK):
             for i in range(2):
                 t0 = b * BLOCK + i * tile
@@ -246,14 +255,20 @@
                 scores = (products * scale * weight).astype(jnp.bfloat16)
                 result = jnp.dot(scores, v[seen, lanes], preferred_element_type=jnp.float32)
                 if b > 0:
-                    result = result + times_wide(q[here, lanes], first[h]) * jnp.exp(
+                    result = result + times_wide(q[here, lanes], state) * jnp.exp(
                         col[here, h : h + 1]
                     )
                 out[here, lanes] = result
-
-
-def finish_body(coord, ld, q, within, gates, before, far3, far2, far1, gain, o0, o1, o2, o3, scratch, sums):
+            if b + 1 < rows // BLOCK:
+                added, last = block_state(row, col, k, v, h, b, depth)
+                state = added if b == 0 else jnp.exp(last) * state + added
+    for copy in copies:
+        copy.wait()
+
+
+def finish_body(coord, ld, q, within, gates, before, far3, far2, far1, gain, w_near, w_far, o0, o1, o2, o3, both, scratch, sums, sem):
     rows, heads, depth = q.shape[0], ld.shape[0], before.shape[2]
+    copies = joining(w_near, w_far, both, sem)
     _, sums[...] = summed_decay(ld, scratch, rows)
     states = []
     for h in range(heads):
@@ -275,40 +290,52 @@
             normed = centered * lax.rsqrt(variance + EPSILON) * gain[h : h + 1, :]
             g = gates[here, lanes].astype(jnp.float32)
             out[:, lanes] = (g * (1.0 / (1.0 + jnp.exp(-g))) * normed).astype(jnp.bfloat16)
-
-
-def vmem_call(body, out_shape, *args, scratch=(), smem=0):
+    for copy in copies:
+        copy.wait()
+
+
+def vmem_call(body, out_shape, *args, scratch=(), smem=0, hbm=(), hbm_out=()):
     vm = pl.BlockSpec(memory_space=pltpu.VMEM)
+    hb = pl.BlockSpec(memory_space=pltpu.HBM)
+    sm = pl.BlockSpec(memory_space=pltpu.SMEM)
+    specs = [sm if i < smem else hb if i in hbm else vm for i in range(len(args))]
+    if isinstance(out_shape, tuple):
+        out_specs = tuple(hb if i in hbm_out else vm for i in range(len(out_shape)))
+    else:
+        out_specs = vm
     return pl.pallas_call(
         body,
         out_shape=out_shape,
-        in_specs=[pl.BlockSpec(memory_space=pltpu.SMEM)] * smem + [vm] * (len(args) - smem),
-        out_specs=jax.tree.map(lambda _: vm, out_shape),
+        in_specs=specs,
+        out_specs=out_specs,
         scratch_shapes=list(scratch),
         compiler_params=pltpu.CompilerParams(vmem_limit_bytes=LIMIT),
     )(*args)
 
 
-def mix_body(coord, r0, r1, r2, r3, own, near, near2, far, far2, resid, gain1, gain2, middle, out_a, out_b, acc):
+def mix_body(coord, r0, r1, r2, r3, own, near, near2, far, far2, resid, gain1, gain2, middle, out_a, out_b):
     half = own.shape[0] // 2
     low = coord[2] == 0
 
-    def part(cols, piece):
-        return jnp.dot(cols, piece[...], preferred_element_type=jnp.float32)
-
-    def rounded(v):
-        return v.astype(jnp.bfloat16).astype(jnp.float32)
-
     def chosen(one, other):
         return jnp.where(low, one.astype(jnp.float32), other.astype(jnp.float32)).astype(jnp.bfloat16)
 
     left, right = r1[...], r3[...]
     far_a, far_b = r2[:, 0:half], r2[:, half:]
-    acc[...] = rounded(part(r0[...], own))
-    acc[...] += rounded(part(chosen(left, right), near))
-    acc[...] += rounded(part(chosen(right, left), near2))
-    far = part(chosen(far_a, far_b), far) + part(chosen(far_b, far_a), far2)
-    mixed = rounded(acc[...] + rounded(far))
+    columns = [
+        r0[...],
+        chosen(left, right),
+        chosen(right, left),
+        chosen(far_a, far_b),
+        chosen(far_b, far_a),
+    ]
+    rows = [v[...] for v in (own, near, near2, far, far2)]
+    mixed = jnp.dot(
+        jnp.concatenate(columns, axis=1),
+        jnp.concatenate(rows, axis=0),
+        preferred_element_type=jnp.float32,
+    )
+    mixed = mixed.astype(jnp.bfloat16).astype(jnp.float32)
     mean = jnp.mean(mixed * mixed, axis=-1, keepdims=True)
     mid = resid[...].astype(jnp.float32) + mixed * lax.rsqrt(mean + EPSILON) * gain1[...]
     mid = mid.astype(jnp.bfloat16)
@@ -362,21 +389,20 @@
     return tuple(jnp.where(flag, a, b) for a, b in zip(one, other))
 
 
-def pair_body(coord, total, got, new_total, before, message):
+def pair_body(coord, own, got, before, message):
     upper = coord[2] == 1
-    for h in range(total.shape[0]):
-        mine, other = read_state(total, h), read_state(got, h)
+    for h in range(own.shape[0]):
+        mine, other = read_state(own, h), read_state(got, h)
         nothing = (jnp.ones_like(mine[0]), jnp.zeros_like(mine[1]))
         both = either(upper, joined(other, mine), joined(mine, other))
-        write_state(new_total, h, *both)
         write_state(message, h, *both)
         write_state(before, h, *either(upper, other, nothing))
 
 
-def plane_body(coord, total, inner, b1, b2, b3, before, message):
+def plane_body(coord, own, inner, b1, b2, b3, before, message):
     y = coord[1]
-    for h in range(total.shape[0]):
-        mine = read_state(total, h)
+    for h in range(own.shape[0]):
+        mine = read_state(own, h)
         nothing = (jnp.ones_like(mine[0]), jnp.zeros_like(mine[1]))
         back = [read_state(r, h) for r in (b1, b2, b3)]
         past = nothing
@@ -418,7 +444,6 @@
     x = lax.axis_index("tp")
     coord = jnp.stack([z, y, c, x]).astype(jnp.int32)
     up1, down1 = along(1), along(-1)
-    weights = gather_weights(w_gate, w_up, w_down)
     o_half = out_weight.shape[0] // 2
     turn = [(i, (i + 1) % RING) for i in range(RING)]
     turn += [(RING + i, RING + (i - 1) % RING) for i in range(RING)]
@@ -435,33 +460,38 @@
     sums = pltpu.VMEM((128, rows), f32)
     total_shape = shaped(f32, heads, depth + 8, depth)
     message_shape = shaped(bf16, heads, depth + 16, depth)
-    total, message, first = kernel(
-        state_body,
-        (total_shape, message_shape, shaped(f32, heads, depth, depth)),
-        ld, keys, values,
-        scratch=(sums,),
-    )
-    within = kernel(
-        within_body, shaped(f32, rows, width), ld, queries, keys, values, first, scratch=(sums,)
+    block = w_gate.shape
+    mine = jnp.stack([w_gate, w_up, w_down.T])
+    message = kernel(state_body, message_shape, ld, keys, values, scratch=(sums,))
+    w_right, w_left, w_far = near_shards(mine)
+    pair = pltpu.SemaphoreType.DMA((2,))
+    within, s0 = kernel(
+        within_body,
+        (shaped(f32, rows, width), shaped(bf16, 2, 3, *block)),
+        ld, queries, keys, values, mine, w_right,
+        scratch=(sums, pair),
+        hbm=(4, 5),
+        hbm_out=(1,),
     )
     got = lax.ppermute(message, "sp_2", flipped(2, 1))
-    total, inner, message = kernel(
-        pair_body, (total_shape, total_shape, message_shape), coord, total, got, smem=1
-    )
+    inner, message = kernel(pair_body, (total_shape, message_shape), coord, message, got, smem=1)
     back = [lax.ppermute(message, "sp_1", along(k)) for k in (1, 2, 3)]
     before, message = kernel(
-        plane_body, (total_shape, message_shape), coord, total, inner, *back, smem=1
+        plane_body, (total_shape, message_shape), coord, message, inner, *back, smem=1
     )
     back = [lax.ppermute(message, "sp_0", [(i, i + k) for i in range(RING - k)]) for k in (3, 2, 1)]
     quarter, model = resid.shape
     piece = shaped(bf16, quarter, width)
-    turned = kernel(
+    *turned, s1 = kernel(
         finish_body,
-        (piece,) * RING,
-        coord, ld, queries, within, gates, before, *back, norm_gain,
-        scratch=(sums, pltpu.VMEM((rows, 128), f32)),
+        (piece,) * RING + (shaped(bf16, 2, 3, *block),),
+        coord, ld, queries, within, gates, before, *back, norm_gain, w_left, w_far,
+        scratch=(sums, pltpu.VMEM((rows, 128), f32), pair),
         smem=1,
-    )
+        hbm=(10, 11),
+        hbm_out=(4,),
+    )
+    weights = far_shards(s0, s1)
     turned = (turned[0], *(lax.ppermute(turned[k], "tp", along(k)) for k in (1, 2, 3)))
     half = quarter // 2
     middle, h_a, h_b = kernel(
@@ -469,7 +499,6 @@
         (shaped(bf16, quarter, model), shaped(bf16, half, model), shaped(bf16, half, model)),
         coord, *turned, out_weight, o_near, o_near2, o_far, o_far2, resid,
         post_mix_gain.reshape(1, -1), pre_ffn_gain.reshape(1, -1),
-        scratch=(pltpu.VMEM((quarter, model), f32),),
         smem=1,
     )
 

time: 176 us -> 220 us (1.25); the launches traced: 173 us -> 219 us
  Pallas kernels: 44.2 us -> 75.1 us
  waiting for transfers between devices: 57 us -> 71.7 us
  other arithmetic: 5.28 us -> 1.5 us
  starting transfers between devices: 64.2 us -> 67.1 us
    pallas_call x7, Pallas kernels: 14.4 us -> 45 us  [vmem_call(): pl.pallas_call(body, out_shape=out_shape, in_specs=specs, out_specs=out_s...]
    ppermute x3, waiting for transfers between devices: 0.59 us -> 16 us  [layer(): back = [lax.ppermute(message, 'sp_1', along(k)) for k in (1, 2, 3)]]
    ppermute x1, starting transfers between devices: 0.01 us -> 6.66 us  [layer(): o_near2 = lax.ppermute(o_near, 'sp_2', flipped(2, 1))]
    ppermute x17, starting transfers between devices: 30.5 us -> 25.8 us  [the longest x8 15 us: far_shards(): return own + [lax.ppermute(v, 'sp_2', flipped(2, 1)) for v in own]]
    ppermute x3, starting transfers between devices: 8.56 us -> 13.2 us  [layer(): lax.ppermute(message, 'sp_0', [(i, i + k) for i in range(RING - k)])]
    ppermute x1, waiting for transfers between devices: 3.92 us -> 0.01 us  [layer(): o_far2 = lax.ppermute(o_far, 'sp_2', flipped(2, 1))]
    another operation x3 -> x1, other arithmetic: 4.96 us -> 1.17 us  [layer(): mine = jnp.stack([w_gate, w_up, w_down.T])]
    ppermute x3, starting transfers between devices: 4.99 us -> 1.58 us  [layer(): back = [lax.ppermute(message, 'sp_1', along(k)) for k in (1, 2, 3)]]
  transfers between devices with their start and end apart: 43 -> 43, of which waited for: 16 -> 17; matrix products, arithmetic and copies ran while one was open for 2% -> 1% of each run, Pallas kernels for 25% -> 33%
where the time goes in v2:
time: 220 us; the launch traced here: 219 us
  Pallas kernels  75.1 us (34%)
  waiting for transfers between devices  71.7 us (33%)
  starting transfers between devices  67.1 us (30%)
  local copies, waits for them, and re-layouts  3.62 us (2%)
    pallas_call x7, Pallas kernels, vmem_call(): pl.pallas_call(body, out_shape=out_shape, in_specs=specs, out_specs=out_s...  45 us
    pallas_call x4, Pallas kernels, ffn(): pl.pallas_call(functools.partial(ffn_body, len(xs), n_out), out_shape=[ja...  24.6 us
    ppermute x3, waiting for transfers between devices, layer(): lax.ppermute(turned[k], 'tp', along(k))  16.9 us
    ppermute x3, waiting for transfers between devices, layer(): back = [lax.ppermute(message, 'sp_1', along(k)) for k in (1, 2, 3)]  16 us
    ppermute x8, starting transfers between devices, far_shards(): return own + [lax.ppermute(v, 'sp_2', flipped(2, 1)) for v in own]  15 us
    ppermute x3, starting transfers between devices, layer(): lax.ppermute(message, 'sp_0', [(i, i + k) for i in range(RING - k)])  13.2 us
    ppermute x1, waiting for transfers between devices, layer(): r_a = lax.ppermute(h_a, 'tp', up1)  11.4 us
    ppermute x1, waiting for transfers between devices, layer(): lax.ppermute((wide(right_b) + wide(far_in_b)).astype(bf16), 'tp', down1)  11.2 us
  transfers between devices with their start and end apart: 43, of which 17 were waited for; matrix products, arithmetic and copies ran while one was open for 1% of the time, Pallas kernels for 33%

profile of v2, /device:TPU:1, one launch (start us, length us, event | category | flops | bytes accessed | tf_op | source)
XLA Modules:
  0.0 219.4 jit_solution(9583199816438599408)
XLA Ops:
  0.0 3.4 %collective-permute-start.13 = (bf16[256,2048]{1,0:T(8,128)(2,1)}, bf16[256,2048]{1,0:T(8,128)(2,1)S(1)}, u32[]{:S(2)}, u32[]{:S(2)}) collective-permute-start(bf16[256,2048]{1,0:T(8,128)(2,1)} %own.1), channel_id=1, source_target_pairs={{0,1},{1,2},{2,3},{3,0},{4,7},{5,4},{6,5},{7,6},{8,9},{9,10},{10,1... | collective-permute-start | bytes 3145736 | tf_op jit(solution)/shard_map/ppermute | solution.py:450
  6.3 2.2 %collective-permute-start.8 = (bf16[3,64,1408]{2,1,0:T(8,128)(2,1)S(1)}, bf16[3,64,1408]{2,1,0:T(8,128)(2,1)}, u32[]{:S(2)}, u32[]{:S(2)}) collective-permute-start(bf16[3,64,1408]{2,1,0:T(8,128)(2,1)S(1)} %pad_maximum_fusion.near), channel_id=1, source_target_pairs={{0,24},{4,100},{8,0},{12,108},{16,8},{20,116},{24,16},{28,124},{32... | collective-permute-start | bytes 1622024 | tf_op jit(solution)/shard_map/ppermute | solution.py:45
  9.7 1.8 shard_map.137.own
  14.8 8.3 %collective-permute-done.2.b1 = bf16[2,144,128]{2,1,0:T(8,128)(2,1)S(1)} collective-permute-done((bf16[2,144,128]{2,1,0:T(8,128)(2,1)S(1)}, bf16[2,144,128]{2,1,0:T(8,128)(2,1)S(1)}, u32[]{:S(2)}, u32[]{:S(2)}) %collective-permute-start.2) | collective-permute-done | bytes 73760 | tf_op jit(solution)/shard_map/ppermute | solution.py:478
  23.3 4.5 %collective-permute-done.3.b2 = bf16[2,144,128]{2,1,0:T(8,128)(2,1)S(1)} collective-permute-done((bf16[2,144,128]{2,1,0:T(8,128)(2,1)S(1)}, bf16[2,144,128]{2,1,0:T(8,128)(2,1)S(1)}, u32[]{:S(2)}, u32[]{:S(2)}) %collective-permute-start.3) | collective-permute-done | bytes 73760 | tf_op jit(solution)/shard_map/ppermute | solution.py:478
  27.8 3.2 %collective-permute-done.4.b3 = bf16[2,144,128]{2,1,0:T(8,128)(2,1)S(1)} collective-permute-done((bf16[2,144,128]{2,1,0:T(8,128)(2,1)S(1)}, bf16[2,144,128]{2,1,0:T(8,128)(2,1)S(1)}, u32[]{:S(2)}, u32[]{:S(2)}) %collective-permute-start.4) | collective-permute-done | bytes 73760 | tf_op jit(solution)/shard_map/ppermute | solution.py:478
  31.7 5.8 %collective-permute-start.5 = (bf16[2,144,128]{2,1,0:T(8,128)(2,1)S(1)}, bf16[2,144,128]{2,1,0:T(8,128)(2,1)S(1)}, u32[]{:S(2)}, u32[]{:S(2)}) collective-permute-start(bf16[2,144,128]{2,1,0:T(8,128)(2,1)S(1)} %get-tuple-element.31), channel_id=1, source_target_pairs={{0,96},{1,97},{2,98},{3,99},{4,100},{5,101},{6,102},{7,103},{8,104... | collective-permute-start | bytes 221192 | tf_op jit(solution)/shard_map/ppermute | solution.py:482
  40.2 6.1 %collective-permute-start.7 = (bf16[2,144,128]{2,1,0:T(8,128)(2,1)S(1)}, bf16[2,144,128]{2,1,0:T(8,128)(2,1)S(1)}, u32[]{:S(2)}, u32[]{:S(2)}) collective-permute-start(bf16[2,144,128]{2,1,0:T(8,128)(2,1)S(1)} %get-tuple-element.31), channel_id=1, source_target_pairs={{0,32},{32,64},{64,96},{1,33},{33,65},{65,97},{2,34},{34,66},{66,9... | collective-permute-start | bytes 221192 | tf_op jit(solution)/shard_map/ppermute | solution.py:482
  46.3 3.1 %shard_map.136 = (f32[1024,256]{1,0:T(8,128)S(1)}, bf16[2,3,64,1408]{3,2,1,0:T(8,128)(2,1)S(1)}) custom-call(f32[2,1024]{1,0:T(2,128)S(1)} %bitcast.14, bf16[1024,256]{1,0:T(8,128)(2,1)S(1)} %copy-done.2, bf16[1024,256]{1,0:T(8,128)(2,1)S(1)} %copy-done, bf16[1024,256]{1,0:T(8,128)(2,1)S(1)} %copy-done.1, bf16[3,64,1408]{2,1,0:T(8,128)(2,1)S(1)} %pad_maximum_fusion.near, ...), custom_call_target="tpu_custom_call" | custom-call | tf_op jit(solution)/shard_map/pallas_call | solution.py:306
  50.5 34.4 %shard_map.140 = (bf16[256,256]{1,0:T(8,128)(2,1)S(1)}, bf16[256,256]{1,0:T(8,128)(2,1)S(1)}, bf16[256,256]{1,0:T(8,128)(2,1)S(1)}, bf16[256,256]{1,0:T(8,128)(2,1)S(1)}, bf16[2,3,64,1408]{3,2,1,0:T(8,128)(2,1)}) custom-call(s32[4]{0:T(128)S(1)} %pad_add_fusion.coord, f32[2,1024]{1,0:T(2,128)S(1)} %bitcast.15, bf16[1024,256]{1,0:T(8,128)(2,1)S(1)} %copy-done.2, ...), custom_call_target="tpu_custom_call" | custom-call | tf_op jit(solution)/shard_map/pallas_call | solution.py:306
  87.7 5.4 %collective-permute-start.26 = (bf16[2,3,64,1408]{3,2,1,0:T(8,128)(2,1)}, bf16[2,3,64,1408]{3,2,1,0:T(8,128)(2,1)S(1)}, u32[]{:S(2)}, u32[]{:S(2)}) collective-permute-start(bf16[2,3,64,1408]{3,2,1,0:T(8,128)(2,1)} %get-tuple-element.39.refs_1_), channel_id=1, source_target_pairs={{0,4},{4,0},{1,5},{5,1},{2,6},{6,2},{3,7},{7,3},{8,12},{12,8},{9,1... | collective-permute-start | bytes 3244040 | tf_op jit(solution)/shard_map/ppermute | solution.py:59
  94.6 7.0 %collective-permute-done.10.r1 = bf16[256,256]{1,0:T(8,128)(2,1)S(1)} collective-permute-done((bf16[256,256]{1,0:T(8,128)(2,1)}, bf16[256,256]{1,0:T(8,128)(2,1)S(1)}, u32[]{:S(2)}, u32[]{:S(2)}) %collective-permute-start.10) | collective-permute-done | bytes 131104 | tf_op jit(solution)/shard_map/ppermute | solution.py:495
  102.0 5.2 %collective-permute-done.11.r2 = bf16[256,256]{1,0:T(8,128)(2,1)S(1)} collective-permute-done((bf16[256,256]{1,0:T(8,128)(2,1)}, bf16[256,256]{1,0:T(8,128)(2,1)S(1)}, u32[]{:S(2)}, u32[]{:S(2)}) %collective-permute-start.11) | collective-permute-done | bytes 131104 | tf_op jit(solution)/shard_map/ppermute | solution.py:495
  107.3 4.7 %collective-permute-done.12.r3 = bf16[256,256]{1,0:T(8,128)(2,1)S(1)} collective-permute-done((bf16[256,256]{1,0:T(8,128)(2,1)S(1)}, bf16[256,256]{1,0:T(8,128)(2,1)S(1)}, u32[]{:S(2)}, u32[]{:S(2)}) %collective-permute-start.12) | collective-permute-done | bytes 131104 | tf_op jit(solution)/shard_map/ppermute | solution.py:495
  112.0 2.7 %collective-permute-start.24 = (bf16[2,3,64,1408]{3,2,1,0:T(8,128)(2,1)S(1)}, bf16[2,3,64,1408]{3,2,1,0:T(8,128)(2,1)S(1)}, u32[]{:S(2)}, u32[]{:S(2)}) collective-permute-start(bf16[2,3,64,1408]{3,2,1,0:T(8,128)(2,1)S(1)} %copy-done.4), channel_id=1, source_target_pairs={{0,96},{4,28},{8,104},{12,4},{16,112},{20,12},{24,120},{28,20},{32... | collective-permute-start | bytes 3244040 | tf_op jit(solution)/shard_map/ppermute | solution.py:57
  114.6 6.7 %collective-permute-start.14 = (bf16[256,2048]{1,0:T(8,128)(2,1)S(1)}, bf16[256,2048]{1,0:T(8,128)(2,1)S(1)}, u32[]{:S(2)}, u32[]{:S(2)}) collective-permute-start(bf16[256,2048]{1,0:T(8,128)(2,1)S(1)} %collective-permute-done.13.near), channel_id=1, source_target_pairs={{0,4},{4,0},{1,5},{5,1},{2,6},{6,2},{3,7},{7,3},{8,12},{12,8},{9,1... | collective-permute-start | bytes 3145736 | tf_op jit(solution)/shard_map/ppermute | solution.py:453
  121.8 5.6 %collective-permute-done.17.refs_2_ = bf16[2,3,64,1408]{3,2,1,0:T(8,128)(2,1)S(1)} collective-permute-done((bf16[2,3,64,1408]{3,2,1,0:T(8,128)(2,1)S(1)}, bf16[2,3,64,1408]{3,2,1,0:T(8,128)(2,1)S(1)}, u32[]{:S(2)}, u32[]{:S(2)}) %collective-permute-start.17) | collective-permute-done | bytes 1081376 | tf_op jit(solution)/shard_map/ppermute | solution.py:52
  127.4 7.0 %collective-permute-start.28 = (bf16[2,3,64,1408]{3,2,1,0:T(8,128)(2,1)S(1)}, bf16[2,3,64,1408]{3,2,1,0:T(8,128)(2,1)S(1)}, u32[]{:S(2)}, u32[]{:S(2)}) collective-permute-start(bf16[2,3,64,1408]{3,2,1,0:T(8,128)(2,1)S(1)} %collective-permute-done.19.refs_3_), channel_id=1, source_target_pairs={{0,4},{4,0},{1,5},{5,1},{2,6},{6,2},{3,7},{7,3},{8,12},{12,8},{9,1... | collective-permute-start | bytes 3244040 | tf_op jit(solution)/shard_map/ppermute | solution.py:59
  137.1 2.6 %shard_map.141 = (bf16[256,2048]{1,0:T(8,128)(2,1)S(1)}, bf16[128,2048]{1,0:T(8,128)(2,1)S(1)}, bf16[128,2048]{1,0:T(8,128)(2,1)S(1)}) custom-call(s32[4]{0:T(128)S(1)} %pad_add_fusion.coord, bf16[256,256]{1,0:T(8,128)(2,1)S(1)} %get-tuple-element.32.r0, bf16[256,256]{1,0:T(8,128)(2,1)S(1)} %collective-permute-done.10.r1, ...), custom_call_target="tpu_custom_call" | custom-call | tf_op jit(solution)/shard_map/pallas_call | solution.py:306
  142.5 11.4 %collective-permute-done.33.refs_0_ = bf16[128,2048]{1,0:T(8,128)(2,1)S(1)} collective-permute-done((bf16[128,2048]{1,0:T(8,128)(2,1)S(1)}, bf16[128,2048]{1,0:T(8,128)(2,1)S(1)}, u32[]{:S(2)}, u32[]{:S(2)}) %collective-permute-start.33) | collective-permute-done | bytes 524320 | tf_op jit(solution)/shard_map/ppermute | solution.py:505
  161.0 3.8 %shard_map.142.refs_4_ = bf16[3,16,2,64,1408]{4,3,2,1,0:T(8,128)(2,1)S(1)} custom-call(s32[4]{0:T(128)S(1)} %pad_add_fusion.coord, bf16[2,3,64,1408]{3,2,1,0:T(8,128)(2,1)S(1)} %copy-done.4, bf16[2,3,64,1408]{3,2,1,0:T(8,128)(2,1)} %get-tuple-element.39.refs_1_, bf16[2,3,64,1408]{3,2,1,0:T(8,128)(2,1)S(1)} %collective-permute-done.17.refs_2_, ...), custom_call_target="tpu_custom_call" | custom-call | tf_op jit(solution)/shard_map/pallas_call | solution.py:106
  164.8 2.7 %collective-permute-start.32 = (bf16[128,2048]{1,0:T(8,128)(2,1)S(1)}, bf16[128,2048]{1,0:T(8,128)(2,1)S(1)}, u32[]{:S(2)}, u32[]{:S(2)}) collective-permute-start(bf16[128,2048]{1,0:T(8,128)(2,1)S(1)} %get-tuple-element.36.refs_0_), channel_id=1, source_target_pairs={{0,3},{1,0},{2,1},{3,2},{4,7},{5,4},{6,5},{7,6},{8,11},{9,8},{10,9... | collective-permute-start | bytes 1572872 | tf_op jit(solution)/shard_map/ppermute | solution.py:510
  169.2 3.0 %collective-permute-done.34.refs_0_ = bf16[128,2048]{1,0:T(8,128)(2,1)S(1)} collective-permute-done((bf16[128,2048]{1,0:T(8,128)(2,1)S(1)}, bf16[128,2048]{1,0:T(8,128)(2,1)S(1)}, u32[]{:S(2)}, u32[]{:S(2)}) %collective-permute-start.34) | collective-permute-done | bytes 524320 | tf_op jit(solution)/shard_map/ppermute | solution.py:507
  172.6 6.2 %ffn_rows.6 = (bf16[128,2048]{1,0:T(8,128)(2,1)S(1)}, bf16[128,2048]{1,0:T(8,128)(2,1)S(1)}) custom-call(bf16[128,2048]{1,0:T(8,128)(2,1)S(1)} %collective-permute-done.34.refs_0_, bf16[128,2048]{1,0:T(8,128)(2,1)S(1)} %collective-permute-done.36.refs_1_, bf16[3,16,2,64,1408]{4,3,2,1,0:T(8,128)(2,1)S(1)} %shard_map.143.refs_2_), custom_call_target="tpu_custom_call" | custom-call | tf_op jit(solution)/shard_map/ffn_rows/pallas_call | solution.py:162
  178.7 2.1 collective-permute-start.39
  180.9 6.2 %ffn_rows.7 = (bf16[128,2048]{1,0:T(8,128)(2,1)S(1)}, bf16[128,2048]{1,0:T(8,128)(2,1)S(1)}) custom-call(bf16[128,2048]{1,0:T(8,128)(2,1)S(1)} %collective-permute-done.33.refs_0_, bf16[128,2048]{1,0:T(8,128)(2,1)S(1)} %collective-permute-done.35.refs_1_, bf16[3,16,2,64,1408]{4,3,2,1,0:T(8,128)(2,1)S(1)} %shard_map.143.refs_2_), custom_call_target="tpu_custom_call" | custom-call | tf_op jit(solution)/shard_map/ffn_rows/pallas_call | solution.py:162
  187.0 2.7 %collective-permute-start.41 = (bf16[128,2048]{1,0:T(8,128)(2,1)S(1)}, bf16[128,2048]{1,0:T(8,128)(2,1)S(1)}, u32[]{:S(2)}, u32[]{:S(2)}) collective-permute-start(bf16[128,2048]{1,0:T(8,128)(2,1)S(1)} %get-tuple-element.46), channel_id=1, source_target_pairs={{0,3},{1,0},{2,1},{3,2},{4,7},{5,4},{6,5},{7,6},{8,11},{9,8},{10,9... | collective-permute-start | bytes 1572872 | tf_op jit(solution)/shard_map/ppermute | solution.py:523
  189.8 6.2 %ffn_rows.5 = (bf16[128,2048]{1,0:T(8,128)(2,1)S(1)}, bf16[128,2048]{1,0:T(8,128)(2,1)S(1)}) custom-call(bf16[128,2048]{1,0:T(8,128)(2,1)S(1)} %collective-permute-done.31.refs_0_, bf16[128,2048]{1,0:T(8,128)(2,1)S(1)} %collective-permute-done.32.refs_1_, bf16[3,16,2,64,1408]{4,3,2,1,0:T(8,128)(2,1)S(1)} %shard_map.143.refs_2_), custom_call_target="tpu_custom_call" | custom-call | tf_op jit(solution)/shard_map/ffn_rows/pallas_call | solution.py:162
  196.1 2.7 %collective-permute-start.40 = (bf16[128,2048]{1,0:T(8,128)(2,1)S(1)}, bf16[128,2048]{1,0:T(8,128)(2,1)S(1)}, u32[]{:S(2)}, u32[]{:S(2)}) collective-permute-start(bf16[128,2048]{1,0:T(8,128)(2,1)S(1)} %add_convert_fusion), channel_id=1, source_target_pairs={{0,3},{1,0},{2,1},{3,2},{4,7},{5,4},{6,5},{7,6},{8,11},{9,8},{10,9... | collective-permute-start | bytes 1572872 | tf_op jit(solution)/shard_map/ppermute | solution.py:528
  199.1 6.2 %ffn_rows.4 = (bf16[128,2048]{1,0:T(8,128)(2,1)S(1)}, bf16[128,2048]{1,0:T(8,128)(2,1)S(1)}) custom-call(bf16[128,2048]{1,0:T(8,128)(2,1)S(1)} %get-tuple-element.36.refs_0_, bf16[128,2048]{1,0:T(8,128)(2,1)S(1)} %get-tuple-element.37.refs_1_, bf16[3,16,2,64,1408]{4,3,2,1,0:T(8,128)(2,1)S(1)} %shard_map.143.refs_2_), custom_call_target="tpu_custom_call" | custom-call | tf_op jit(solution)/shard_map/ffn_rows/pallas_call | solution.py:162
  206.3 11.2 %collective-permute-done.40.sum_b = bf16[128,2048]{1,0:T(8,128)(2,1)S(1)} collective-permute-done((bf16[128,2048]{1,0:T(8,128)(2,1)S(1)}, bf16[128,2048]{1,0:T(8,128)(2,1)S(1)}, u32[]{:S(2)}, u32[]{:S(2)}) %collective-permute-start.40) | collective-permute-done | bytes 524320 | tf_op jit(solution)/shard_map/ppermute | solution.py:528
  217.5 1.8 shard_map.144
  (102 shorter events, 33.2 us)
Async XLA Ops:
  0.0 93.0 %collective-permute-start.13 = (bf16[256,2048]{1,0:T(8,128)(2,1)}, bf16[256,2048]{1,0:T(8,128)(2,1)S(1)}, u32[]{:S(2)}, u32[]{:S(2)}) collective-permute-start(bf16[256,2048]{1,0:T(8,128)(2,1)} %own.1), channel_id=1, source_target_pairs={{0,1},{1,2},{2,3},{3,0},{4,7},{5,4},{6,5},{7,6},{8,9},{9,10},{10,1... | collective-permute-start | bytes 3145736 | tf_op jit(solution)/shard_map/ppermute | solution.py:450
  4.6 35.6 %collective-permute-start = (bf16[3,64,1408]{2,1,0:T(8,128)(2,1)S(1)}, bf16[3,64,1408]{2,1,0:T(8,128)(2,1)}, u32[]{:S(2)}, u32[]{:S(2)}) collective-permute-start(bf16[3,64,1408]{2,1,0:T(8,128)(2,1)S(1)} %pad_maximum_fusion.near), channel_id=1, source_target_pairs={{0,8},{4,36},{8,16},{12,44},{16,24},{20,52},{24,0},{28,60},{32,40}... | collective-permute-start | bytes 1622024 | tf_op jit(solution)/shard_map/ppermute | solution.py:44
  6.3 44.1 %collective-permute-start.8 = (bf16[3,64,1408]{2,1,0:T(8,128)(2,1)S(1)}, bf16[3,64,1408]{2,1,0:T(8,128)(2,1)}, u32[]{:S(2)}, u32[]{:S(2)}) collective-permute-start(bf16[3,64,1408]{2,1,0:T(8,128)(2,1)S(1)} %pad_maximum_fusion.near), channel_id=1, source_target_pairs={{0,24},{4,100},{8,0},{12,108},{16,8},{20,116},{24,16},{28,124},{32... | collective-permute-start | bytes 1622024 | tf_op jit(solution)/shard_map/ppermute | solution.py:45
  8.5 41.9 %collective-permute-start.9 = (bf16[3,64,1408]{2,1,0:T(8,128)(2,1)S(1)}, bf16[3,64,1408]{2,1,0:T(8,128)(2,1)}, u32[]{:S(2)}, u32[]{:S(2)}) collective-permute-start(bf16[3,64,1408]{2,1,0:T(8,128)(2,1)S(1)} %pad_maximum_fusion.near), channel_id=1, source_target_pairs={{0,16},{4,68},{8,24},{12,76},{16,0},{20,84},{24,8},{28,92},{32,48}... | collective-permute-start | bytes 1622024 | tf_op jit(solution)/shard_map/ppermute | solution.py:46
  13.4 9.6 %collective-permute-start.2 = (bf16[2,144,128]{2,1,0:T(8,128)(2,1)S(1)}, bf16[2,144,128]{2,1,0:T(8,128)(2,1)S(1)}, u32[]{:S(2)}, u32[]{:S(2)}) collective-permute-start(bf16[2,144,128]{2,1,0:T(8,128)(2,1)S(1)} %get-tuple-element.28.own), channel_id=1, source_target_pairs={{0,8},{8,16},{16,24},{24,0},{1,9},{9,17},{17,25},{25,1},{2,10},{10... | collective-permute-start | bytes 221192 | tf_op jit(solution)/shard_map/ppermute | solution.py:478
  38.9 11.5 %collective-permute-start.6 = (bf16[2,144,128]{2,1,0:T(8,128)(2,1)S(1)}, bf16[2,144,128]{2,1,0:T(8,128)(2,1)S(1)}, u32[]{:S(2)}, u32[]{:S(2)}) collective-permute-start(bf16[2,144,128]{2,1,0:T(8,128)(2,1)S(1)} %get-tuple-element.31), channel_id=1, source_target_pairs={{0,64},{32,96},{1,65},{33,97},{2,66},{34,98},{3,67},{35,99},{4,68}... | collective-permute-start | bytes 221192 | tf_op jit(solution)/shard_map/ppermute | solution.py:482
  40.2 10.2 %collective-permute-start.7 = (bf16[2,144,128]{2,1,0:T(8,128)(2,1)S(1)}, bf16[2,144,128]{2,1,0:T(8,128)(2,1)S(1)}, u32[]{:S(2)}, u32[]{:S(2)}) collective-permute-start(bf16[2,144,128]{2,1,0:T(8,128)(2,1)S(1)} %get-tuple-element.31), channel_id=1, source_target_pairs={{0,32},{32,64},{64,96},{1,33},{33,65},{65,97},{2,34},{34,66},{66,9... | collective-permute-start | bytes 221192 | tf_op jit(solution)/shard_map/ppermute | solution.py:482
  86.2 28.4 %collective-permute-start.19 = (bf16[2,3,64,1408]{3,2,1,0:T(8,128)(2,1)}, bf16[2,3,64,1408]{3,2,1,0:T(8,128)(2,1)S(1)}, u32[]{:S(2)}, u32[]{:S(2)}) collective-permute-start(bf16[2,3,64,1408]{3,2,1,0:T(8,128)(2,1)} %get-tuple-element.39.refs_1_), channel_id=1, source_target_pairs={{0,96},{4,28},{8,104},{12,4},{16,112},{20,12},{24,120},{28,20},{32... | collective-permute-start | bytes 3244040 | tf_op jit(solution)/shard_map/ppermute | solution.py:53
  87.4 33.9 %collective-permute-start.23 = (bf16[2,3,64,1408]{3,2,1,0:T(8,128)(2,1)}, bf16[2,3,64,1408]{3,2,1,0:T(8,128)(2,1)}, u32[]{:S(2)}, u32[]{:S(2)}) collective-permute-start(bf16[2,3,64,1408]{3,2,1,0:T(8,128)(2,1)} %get-tuple-element.39.refs_1_), channel_id=1, source_target_pairs={{0,32},{4,12},{8,40},{12,20},{16,48},{20,28},{24,56},{28,4},{32,64... | collective-permute-start | bytes 3244040 | tf_op jit(solution)/shard_map/ppermute | solution.py:56
  87.7 33.9 %collective-permute-start.26 = (bf16[2,3,64,1408]{3,2,1,0:T(8,128)(2,1)}, bf16[2,3,64,1408]{3,2,1,0:T(8,128)(2,1)S(1)}, u32[]{:S(2)}, u32[]{:S(2)}) collective-permute-start(bf16[2,3,64,1408]{3,2,1,0:T(8,128)(2,1)} %get-tuple-element.39.refs_1_), channel_id=1, source_target_pairs={{0,4},{4,0},{1,5},{5,1},{2,6},{6,2},{3,7},{7,3},{8,12},{12,8},{9,1... | collective-permute-start | bytes 3244040 | tf_op jit(solution)/shard_map/ppermute | solution.py:59
  93.1 18.8 %collective-permute-start.15 = (bf16[128,2048]{1,0:T(8,128)(2,1)S(1)}, bf16[128,2048]{1,0:T(8,128)(2,1)S(1)}, u32[]{:S(2)}, u32[]{:S(2)}) collective-permute-start(bf16[128,2048]{1,0:T(8,128)(2,1)S(1)} %constant_dynamic-slice_fusion), channel_id=1, source_target_pairs={{0,1},{1,2},{2,3},{3,0},{4,7},{5,4},{6,5},{7,6},{8,9},{9,10},{10,1... | collective-permute-start | bytes 1572872 | tf_op jit(solution)/shard_map/ppermute | solution.py:452
  111.9 15.5 %collective-permute-start.17 = (bf16[2,3,64,1408]{3,2,1,0:T(8,128)(2,1)S(1)}, bf16[2,3,64,1408]{3,2,1,0:T(8,128)(2,1)S(1)}, u32[]{:S(2)}, u32[]{:S(2)}) collective-permute-start(bf16[2,3,64,1408]{3,2,1,0:T(8,128)(2,1)S(1)} %copy-done.4), channel_id=1, source_target_pairs={{0,32},{4,12},{8,40},{12,20},{16,48},{20,28},{24,56},{28,4},{32,64... | collective-permute-start | bytes 3244040 | tf_op jit(solution)/shard_map/ppermute | solution.py:52
  112.0 27.8 %collective-permute-start.24 = (bf16[2,3,64,1408]{3,2,1,0:T(8,128)(2,1)S(1)}, bf16[2,3,64,1408]{3,2,1,0:T(8,128)(2,1)S(1)}, u32[]{:S(2)}, u32[]{:S(2)}) collective-permute-start(bf16[2,3,64,1408]{3,2,1,0:T(8,128)(2,1)S(1)} %copy-done.4), channel_id=1, source_target_pairs={{0,96},{4,28},{8,104},{12,4},{16,112},{20,12},{24,120},{28,20},{32... | collective-permute-start | bytes 3244040 | tf_op jit(solution)/shard_map/ppermute | solution.py:57
  114.6 21.0 %collective-permute-start.14 = (bf16[256,2048]{1,0:T(8,128)(2,1)S(1)}, bf16[256,2048]{1,0:T(8,128)(2,1)S(1)}, u32[]{:S(2)}, u32[]{:S(2)}) collective-permute-start(bf16[256,2048]{1,0:T(8,128)(2,1)S(1)} %collective-permute-done.13.near), channel_id=1, source_target_pairs={{0,4},{4,0},{1,5},{5,1},{2,6},{6,2},{3,7},{7,3},{8,12},{12,8},{9,1... | collective-permute-start | bytes 3145736 | tf_op jit(solution)/shard_map/ppermute | solution.py:453
  121.3 19.8 %collective-permute-start.25 = (bf16[2,3,64,1408]{3,2,1,0:T(8,128)(2,1)S(1)}, bf16[2,3,64,1408]{3,2,1,0:T(8,128)(2,1)S(1)}, u32[]{:S(2)}, u32[]{:S(2)}) collective-permute-start(bf16[2,3,64,1408]{3,2,1,0:T(8,128)(2,1)S(1)} %copy-done.4), channel_id=1, source_target_pairs={{0,4},{4,0},{1,5},{5,1},{2,6},{6,2},{3,7},{7,3},{8,12},{12,8},{9,1... | collective-permute-start | bytes 3244040 | tf_op jit(solution)/shard_map/ppermute | solution.py:59
  121.6 12.8 %collective-permute-start.16 = (bf16[128,2048]{1,0:T(8,128)(2,1)S(1)}, bf16[128,2048]{1,0:T(8,128)(2,1)S(1)}, u32[]{:S(2)}, u32[]{:S(2)}) collective-permute-start(bf16[128,2048]{1,0:T(8,128)(2,1)S(1)} %collective-permute-done.15.far), channel_id=1, source_target_pairs={{0,4},{4,0},{1,5},{5,1},{2,6},{6,2},{3,7},{7,3},{8,12},{12,8},{9,1... | collective-permute-start | bytes 1572872 | tf_op jit(solution)/shard_map/ppermute | solution.py:454
  127.4 28.0 %collective-permute-start.28 = (bf16[2,3,64,1408]{3,2,1,0:T(8,128)(2,1)S(1)}, bf16[2,3,64,1408]{3,2,1,0:T(8,128)(2,1)S(1)}, u32[]{:S(2)}, u32[]{:S(2)}) collective-permute-start(bf16[2,3,64,1408]{3,2,1,0:T(8,128)(2,1)S(1)} %collective-permute-done.19.refs_3_), channel_id=1, source_target_pairs={{0,4},{4,0},{1,5},{5,1},{2,6},{6,2},{3,7},{7,3},{8,12},{12,8},{9,1... | collective-permute-start | bytes 3244040 | tf_op jit(solution)/shard_map/ppermute | solution.py:59
  134.4 21.5 %collective-permute-start.20 = (bf16[2,3,64,1408]{3,2,1,0:T(8,128)(2,1)S(1)}, bf16[2,3,64,1408]{3,2,1,0:T(8,128)(2,1)S(1)}, u32[]{:S(2)}, u32[]{:S(2)}) collective-permute-start(bf16[2,3,64,1408]{3,2,1,0:T(8,128)(2,1)S(1)} %collective-permute-done.19.refs_3_), channel_id=1, source_target_pairs={{0,96},{4,28},{8,104},{12,4},{16,112},{20,12},{24,120},{28,20},{32... | collective-permute-start | bytes 3244040 | tf_op jit(solution)/shard_map/ppermute | solution.py:55
  135.6 20.4 %collective-permute-start.18 = (bf16[2,3,64,1408]{3,2,1,0:T(8,128)(2,1)S(1)}, bf16[2,3,64,1408]{3,2,1,0:T(8,128)(2,1)S(1)}, u32[]{:S(2)}, u32[]{:S(2)}) collective-permute-start(bf16[2,3,64,1408]{3,2,1,0:T(8,128)(2,1)S(1)} %collective-permute-done.17.refs_2_), channel_id=1, source_target_pairs={{0,32},{4,12},{8,40},{12,20},{16,48},{20,28},{24,56},{28,4},{32,64... | collective-permute-start | bytes 3244040 | tf_op jit(solution)/shard_map/ppermute | solution.py:54
  139.8 14.2 %collective-permute-start.33 = (bf16[128,2048]{1,0:T(8,128)(2,1)S(1)}, bf16[128,2048]{1,0:T(8,128)(2,1)S(1)}, u32[]{:S(2)}, u32[]{:S(2)}) collective-permute-start(bf16[128,2048]{1,0:T(8,128)(2,1)S(1)} %get-tuple-element.36.refs_0_), channel_id=1, source_target_pairs={{0,1},{1,2},{2,3},{3,0},{4,5},{5,6},{6,7},{7,4},{8,9},{9,10},{10,1... | collective-permute-start | bytes 1572872 | tf_op jit(solution)/shard_map/ppermute | solution.py:505
  141.1 14.3 %collective-permute-start.35 = (bf16[128,2048]{1,0:T(8,128)(2,1)S(1)}, bf16[128,2048]{1,0:T(8,128)(2,1)S(1)}, u32[]{:S(2)}, u32[]{:S(2)}) collective-permute-start(bf16[128,2048]{1,0:T(8,128)(2,1)S(1)} %get-tuple-element.37.refs_1_), channel_id=1, source_target_pairs={{0,3},{1,0},{2,1},{3,2},{4,7},{5,4},{6,5},{7,6},{8,11},{9,8},{10,9... | collective-permute-start | bytes 1572872 | tf_op jit(solution)/shard_map/ppermute | solution.py:506
  156.0 11.5 %collective-permute-start.21 = (bf16[2,3,64,1408]{3,2,1,0:T(8,128)(2,1)S(1)}, bf16[2,3,64,1408]{3,2,1,0:T(8,128)(2,1)S(1)}, u32[]{:S(2)}, u32[]{:S(2)}) collective-permute-start(bf16[2,3,64,1408]{3,2,1,0:T(8,128)(2,1)S(1)} %collective-permute-done.18.refs_0_), channel_id=1, source_target_pairs={{0,4},{4,0},{1,5},{5,1},{2,6},{6,2},{3,7},{7,3},{8,12},{12,8},{9,1... | collective-permute-start | bytes 3244040 | tf_op jit(solution)/shard_map/ppermute | solution.py:59
  157.9 14.3 %collective-permute-start.34 = (bf16[128,2048]{1,0:T(8,128)(2,1)S(1)}, bf16[128,2048]{1,0:T(8,128)(2,1)S(1)}, u32[]{:S(2)}, u32[]{:S(2)}) collective-permute-start(bf16[128,2048]{1,0:T(8,128)(2,1)S(1)} %collective-permute-done.33.refs_0_), channel_id=1, source_target_pairs={{0,1},{1,2},{2,3},{3,0},{4,5},{5,6},{6,7},{7,4},{8,9},{9,10},{10,1... | collective-permute-start | bytes 1572872 | tf_op jit(solution)/shard_map/ppermute | solution.py:507
  159.5 13.1 %collective-permute-start.36 = (bf16[128,2048]{1,0:T(8,128)(2,1)S(1)}, bf16[128,2048]{1,0:T(8,128)(2,1)S(1)}, u32[]{:S(2)}, u32[]{:S(2)}) collective-permute-start(bf16[128,2048]{1,0:T(8,128)(2,1)S(1)} %collective-permute-done.35.refs_1_), channel_id=1, source_target_pairs={{0,3},{1,0},{2,1},{3,2},{4,7},{5,4},{6,5},{7,6},{8,11},{9,8},{10,9... | collective-permute-start | bytes 1572872 | tf_op jit(solution)/shard_map/ppermute | solution.py:508
  161.0 28.8 %collective-permute-start.31 = (bf16[128,2048]{1,0:T(8,128)(2,1)S(1)}, bf16[128,2048]{1,0:T(8,128)(2,1)S(1)}, u32[]{:S(2)}, u32[]{:S(2)}) collective-permute-start(bf16[128,2048]{1,0:T(8,128)(2,1)S(1)} %get-tuple-element.37.refs_1_), channel_id=1, source_target_pairs={{0,1},{1,2},{2,3},{3,0},{4,5},{5,6},{6,7},{7,4},{8,9},{9,10},{10,1... | collective-permute-start | bytes 1572872 | tf_op jit(solution)/shard_map/ppermute | solution.py:509
  164.8 25.0 %collective-permute-start.32 = (bf16[128,2048]{1,0:T(8,128)(2,1)S(1)}, bf16[128,2048]{1,0:T(8,128)(2,1)S(1)}, u32[]{:S(2)}, u32[]{:S(2)}) collective-permute-start(bf16[128,2048]{1,0:T(8,128)(2,1)S(1)} %get-tuple-element.36.refs_0_), channel_id=1, source_target_pairs={{0,3},{1,0},{2,1},{3,2},{4,7},{5,4},{6,5},{7,6},{8,11},{9,8},{10,9... | collective-permute-start | bytes 1572872 | tf_op jit(solution)/shard_map/ppermute | solution.py:510
  178.7 17.2 %collective-permute-start.39 = (bf16[128,2048]{1,0:T(8,128)(2,1)S(1)}, bf16[128,2048]{1,0:T(8,128)(2,1)S(1)}, u32[]{:S(2)}, u32[]{:S(2)}) collective-permute-start(bf16[128,2048]{1,0:T(8,128)(2,1)S(1)} %get-tuple-element.45), channel_id=1, source_target_pairs={{0,3},{1,0},{2,1},{3,2},{4,7},{5,4},{6,5},{7,6},{8,11},{9,8},{10,9... | collective-permute-start | bytes 1572872 | tf_op jit(solution)/shard_map/ppermute | solution.py:525
  180.9 18.0 %collective-permute-start.37 = (bf16[128,2048]{1,0:T(8,128)(2,1)S(1)}, bf16[128,2048]{1,0:T(8,128)(2,1)S(1)}, u32[]{:S(2)}, u32[]{:S(2)}) collective-permute-start(bf16[128,2048]{1,0:T(8,128)(2,1)S(1)} %get-tuple-element.43), channel_id=1, source_target_pairs={{0,1},{1,2},{2,3},{3,0},{4,5},{5,6},{6,7},{7,4},{8,9},{9,10},{10,1... | collective-permute-start | bytes 1572872 | tf_op jit(solution)/shard_map/ppermute | solution.py:524
  187.0 19.2 %collective-permute-start.41 = (bf16[128,2048]{1,0:T(8,128)(2,1)S(1)}, bf16[128,2048]{1,0:T(8,128)(2,1)S(1)}, u32[]{:S(2)}, u32[]{:S(2)}) collective-permute-start(bf16[128,2048]{1,0:T(8,128)(2,1)S(1)} %get-tuple-element.46), channel_id=1, source_target_pairs={{0,3},{1,0},{2,1},{3,2},{4,7},{5,4},{6,5},{7,6},{8,11},{9,8},{10,9... | collective-permute-start | bytes 1572872 | tf_op jit(solution)/shard_map/ppermute | solution.py:523
  189.8 16.5 %collective-permute-start.42 = (bf16[128,2048]{1,0:T(8,128)(2,1)S(1)}, bf16[128,2048]{1,0:T(8,128)(2,1)S(1)}, u32[]{:S(2)}, u32[]{:S(2)}) collective-permute-start(bf16[128,2048]{1,0:T(8,128)(2,1)S(1)} %get-tuple-element.47), channel_id=1, source_target_pairs={{0,1},{1,2},{2,3},{3,0},{4,5},{5,6},{6,7},{7,4},{8,9},{9,10},{10,1... | collective-permute-start | bytes 1572872 | tf_op jit(solution)/shard_map/ppermute | solution.py:522
  196.1 21.4 %collective-permute-start.40 = (bf16[128,2048]{1,0:T(8,128)(2,1)S(1)}, bf16[128,2048]{1,0:T(8,128)(2,1)S(1)}, u32[]{:S(2)}, u32[]{:S(2)}) collective-permute-start(bf16[128,2048]{1,0:T(8,128)(2,1)S(1)} %add_convert_fusion), channel_id=1, source_target_pairs={{0,3},{1,0},{2,1},{3,2},{4,7},{5,4},{6,5},{7,6},{8,11},{9,8},{10,9... | collective-permute-start | bytes 1572872 | tf_op jit(solution)/shard_map/ppermute | solution.py:528
  199.0 18.5 %collective-permute-start.38 = (bf16[128,2048]{1,0:T(8,128)(2,1)S(1)}, bf16[128,2048]{1,0:T(8,128)(2,1)S(1)}, u32[]{:S(2)}, u32[]{:S(2)}) collective-permute-start(bf16[128,2048]{1,0:T(8,128)(2,1)S(1)} %add_convert_fusion.1), channel_id=1, source_target_pairs={{0,1},{1,2},{2,3},{3,0},{4,5},{5,6},{6,7},{7,4},{8,9},{9,10},{10,1... | collective-permute-start | bytes 1572872 | tf_op jit(solution)/shard_map/ppermute | solution.py:527
  (26 other events, 467.3 us)

commit v3 on v2

--- a/solution.py
+++ b/solution.py
@@ -1,4 +1,5 @@
 import functools
+import math
 
 import jax
 import jax.numpy as jnp
@@ -233,6 +234,9 @@
     row, col = summed_decay(ld, scratch, BLOCK)
     scale = depth ** (-0.5)
     tile = BLOCK // 2
+    causal = lax.broadcasted_iota(jnp.int32, (tile, tile), 0) >= lax.broadcasted_iota(
+        jnp.int32, (tile, tile), 1
+    )
     for h in range(heads):
         lanes = slice(h * depth, (h + 1) * depth)
         state = None
@@ -248,11 +252,10 @@
                     (((1,), (1,)), ((), ())),
                     preferred_element_type=jnp.float32,
                 )
-                gap = col[here, h : h + 1] - row[h : h + 1, seen]
-                at = lax.broadcasted_iota(jnp.int32, (tile, span), 0) + i * tile
-                causal = at >= lax.broadcasted_iota(jnp.int32, (tile, span), 1)
-                weight = jnp.where(causal, jnp.exp(jnp.minimum(gap, 0.0)), 0.0)
-                scores = (products * scale * weight).astype(jnp.bfloat16)
+                gap = (col[here, h : h + 1] + math.log(scale)) - row[h : h + 1, seen]
+                edge = jnp.where(causal, gap[:, span - tile :], -jnp.inf)
+                gap = edge if i == 0 else jnp.concatenate([gap[:, : span - tile], edge], axis=1)
+                scores = (products * jnp.exp(gap)).astype(jnp.bfloat16)
                 result = jnp.dot(scores, v[seen, lanes], preferred_element_type=jnp.float32)
                 if b > 0:
                     result = result + times_wide(q[here, lanes], state) * jnp.exp(
@@ -347,15 +350,25 @@
     out_b[...] = h[h.shape[0] // 2 :]
 
 
-def final_body(own_a, own_b, sum_a, sum_b, near_a, near_b, middle, gain, out):
+def final_body(own_a, own_b, sum_a, sum_b, near_a, near_b, middle, gain, out, rows, sem):
     half = own_a.shape[0]
+    step = half // 2
+    copies = []
     for i, refs in enumerate(((own_a, sum_a, near_a), (own_b, sum_b, near_b))):
-        here = slice(i * half, (i + 1) * half)
-        total = sum(r[...].astype(jnp.float32) for r in refs)
-        total = total.astype(jnp.bfloat16).astype(jnp.float32)
-        mean = jnp.mean(total * total, axis=-1, keepdims=True)
-        mid = middle[here, :].astype(jnp.float32)
-        out[here, :] = (mid + total * lax.rsqrt(mean + EPSILON) * gain[...]).astype(jnp.bfloat16)
+        for j in range(2):
+            part = slice(j * step, (j + 1) * step)
+            here = slice(i * half + j * step, i * half + (j + 1) * step)
+            total = sum(r[part, :].astype(jnp.float32) for r in refs)
+            total = total.astype(jnp.bfloat16).astype(jnp.float32)
+            mean = jnp.mean(total * total, axis=-1, keepdims=True)
+            mid = middle[here, :].astype(jnp.float32)
+            done = mid + total * lax.rsqrt(mean + EPSILON) * gain[...]
+            rows[here, :] = done.astype(jnp.bfloat16)
+            copy = pltpu.make_async_copy(rows.at[here], out.at[here], sem.at[2 * i + j])
+            copy.start()
+            copies.append(copy)
+    for copy in copies:
+        copy.wait()
 
 
 def read_state(ref, h):
@@ -526,11 +539,14 @@
     wide = lambda v: v.astype(f32)
     sum_a = lax.ppermute((wide(left_a) + wide(far_in_a)).astype(bf16), "tp", up1)
     sum_b = lax.ppermute((wide(right_b) + wide(far_in_b)).astype(bf16), "tp", down1)
-    return kernel(
+    (updated,) = kernel(
         final_body,
-        shaped(bf16, quarter, model),
+        (shaped(bf16, quarter, model),),
         own_a, own_b, sum_a, sum_b, near_a, near_b, middle, post_ffn_gain.reshape(1, -1),
-    )
+        scratch=(pltpu.VMEM((quarter, model), bf16), pltpu.SemaphoreType.DMA((4,))),
+        hbm_out=(0,),
+    )
+    return updated
 
 
 def solution(mesh):

time: 220 us -> 219 us (level)
  no operation moved by 1% of the time
where the time goes in v3:
time: 219 us
  Pallas kernels  74.7 us (34%)
  waiting for transfers between devices  71.7 us (33%)
  starting transfers between devices  67.1 us (31%)
  local copies, waits for them, and re-layouts  3.62 us (2%)
    pallas_call x7, Pallas kernels, vmem_call(): pl.pallas_call(body, out_shape=out_shape, in_specs=specs, out_specs=out_s...  44.7 us
    pallas_call x4, Pallas kernels, ffn(): pl.pallas_call(functools.partial(ffn_body, len(xs), n_out), out_shape=[ja...  24.6 us
    ppermute x3, waiting for transfers between devices, layer(): lax.ppermute(turned[k], 'tp', along(k))  16.9 us
    ppermute x3, waiting for transfers between devices, layer(): back = [lax.ppermute(message, 'sp_1', along(k)) for k in (1, 2, 3)]  16 us
    ppermute x8, starting transfers between devices, far_shards(): return own + [lax.ppermute(v, 'sp_2', flipped(2, 1)) for v in own]  15 us
    ppermute x3, starting transfers between devices, layer(): lax.ppermute(message, 'sp_0', [(i, i + k) for i in range(RING - k)])  13.2 us
    ppermute x1, waiting for transfers between devices, layer(): r_a = lax.ppermute(h_a, 'tp', up1)  11.4 us
    ppermute x1, waiting for transfers between devices, layer(): lax.ppermute((wide(right_b) + wide(far_in_b)).astype(bf16), 'tp', down1)  11.2 us
  transfers between devices with their start and end apart: 43, of which 17 were waited for; matrix products, arithmetic and copies ran while one was open for 1% of the time, Pallas kernels for 33%

profile of v3, /device:TPU:1, one launch (start us, length us, event | category | flops | bytes accessed | tf_op | source)
XLA Modules:
  0.0 219.2 jit_solution(1674539011778232987)
XLA Ops:
  0.0 3.4 %collective-permute-start.13 = (bf16[256,2048]{1,0:T(8,128)(2,1)}, bf16[256,2048]{1,0:T(8,128)(2,1)S(1)}, u32[]{:S(2)}, u32[]{:S(2)}) collective-permute-start(bf16[256,2048]{1,0:T(8,128)(2,1)} %own.1), channel_id=1, source_target_pairs={{0,1},{1,2},{2,3},{3,0},{4,7},{5,4},{6,5},{7,6},{8,9},{9,10},{10,1... | collective-permute-start | bytes 3145736 | tf_op jit(solution)/shard_map/ppermute | solution.py:463
  4.6 1.7 collective-permute-start
  6.3 2.2 %collective-permute-start.8 = (bf16[3,64,1408]{2,1,0:T(8,128)(2,1)S(1)}, bf16[3,64,1408]{2,1,0:T(8,128)(2,1)}, u32[]{:S(2)}, u32[]{:S(2)}) collective-permute-start(bf16[3,64,1408]{2,1,0:T(8,128)(2,1)S(1)} %pad_maximum_fusion.near), channel_id=1, source_target_pairs={{0,24},{4,100},{8,0},{12,108},{16,8},{20,116},{24,16},{28,124},{32... | collective-permute-start | bytes 1622024 | tf_op jit(solution)/shard_map/ppermute | solution.py:46
  9.7 1.8 shard_map.137.own
  14.8 8.3 %collective-permute-done.2.b1 = bf16[2,144,128]{2,1,0:T(8,128)(2,1)S(1)} collective-permute-done((bf16[2,144,128]{2,1,0:T(8,128)(2,1)S(1)}, bf16[2,144,128]{2,1,0:T(8,128)(2,1)S(1)}, u32[]{:S(2)}, u32[]{:S(2)}) %collective-permute-start.2) | collective-permute-done | bytes 73760 | tf_op jit(solution)/shard_map/ppermute | solution.py:491
  23.3 4.5 %collective-permute-done.3.b2 = bf16[2,144,128]{2,1,0:T(8,128)(2,1)S(1)} collective-permute-done((bf16[2,144,128]{2,1,0:T(8,128)(2,1)S(1)}, bf16[2,144,128]{2,1,0:T(8,128)(2,1)S(1)}, u32[]{:S(2)}, u32[]{:S(2)}) %collective-permute-start.3) | collective-permute-done | bytes 73760 | tf_op jit(solution)/shard_map/ppermute | solution.py:491
  27.8 3.2 %collective-permute-done.4.b3 = bf16[2,144,128]{2,1,0:T(8,128)(2,1)S(1)} collective-permute-done((bf16[2,144,128]{2,1,0:T(8,128)(2,1)S(1)}, bf16[2,144,128]{2,1,0:T(8,128)(2,1)S(1)}, u32[]{:S(2)}, u32[]{:S(2)}) %collective-permute-start.4) | collective-permute-done | bytes 73760 | tf_op jit(solution)/shard_map/ppermute | solution.py:491
  31.7 5.8 %collective-permute-start.5 = (bf16[2,144,128]{2,1,0:T(8,128)(2,1)S(1)}, bf16[2,144,128]{2,1,0:T(8,128)(2,1)S(1)}, u32[]{:S(2)}, u32[]{:S(2)}) collective-permute-start(bf16[2,144,128]{2,1,0:T(8,128)(2,1)S(1)} %get-tuple-element.31), channel_id=1, source_target_pairs={{0,96},{1,97},{2,98},{3,99},{4,100},{5,101},{6,102},{7,103},{8,104... | collective-permute-start | bytes 221192 | tf_op jit(solution)/shard_map/ppermute | solution.py:495
  40.2 6.1 %collective-permute-start.7 = (bf16[2,144,128]{2,1,0:T(8,128)(2,1)S(1)}, bf16[2,144,128]{2,1,0:T(8,128)(2,1)S(1)}, u32[]{:S(2)}, u32[]{:S(2)}) collective-permute-start(bf16[2,144,128]{2,1,0:T(8,128)(2,1)S(1)} %get-tuple-element.31), channel_id=1, source_target_pairs={{0,32},{32,64},{64,96},{1,33},{33,65},{65,97},{2,34},{34,66},{66,9... | collective-permute-start | bytes 221192 | tf_op jit(solution)/shard_map/ppermute | solution.py:495
  46.3 3.0 %shard_map.136 = (f32[1024,256]{1,0:T(8,128)S(1)}, bf16[2,3,64,1408]{3,2,1,0:T(8,128)(2,1)S(1)}) custom-call(f32[2,1024]{1,0:T(2,128)S(1)} %bitcast.14, bf16[1024,256]{1,0:T(8,128)(2,1)S(1)} %copy-done.2, bf16[1024,256]{1,0:T(8,128)(2,1)S(1)} %copy-done, bf16[1024,256]{1,0:T(8,128)(2,1)S(1)} %copy-done.1, bf16[3,64,1408]{2,1,0:T(8,128)(2,1)S(1)} %pad_maximum_fusion.near, ...), custom_call_target="tpu_custom_call" | custom-call | tf_op jit(solution)/shard_map/pallas_call | solution.py:309
  50.4 34.4 %shard_map.140 = (bf16[256,256]{1,0:T(8,128)(2,1)S(1)}, bf16[256,256]{1,0:T(8,128)(2,1)S(1)}, bf16[256,256]{1,0:T(8,128)(2,1)S(1)}, bf16[256,256]{1,0:T(8,128)(2,1)S(1)}, bf16[2,3,64,1408]{3,2,1,0:T(8,128)(2,1)}) custom-call(s32[4]{0:T(128)S(1)} %pad_add_fusion.coord, f32[2,1024]{1,0:T(2,128)S(1)} %bitcast.15, bf16[1024,256]{1,0:T(8,128)(2,1)S(1)} %copy-done.2, ...), custom_call_target="tpu_custom_call" | custom-call | tf_op jit(solution)/shard_map/pallas_call | solution.py:309
  87.6 5.4 %collective-permute-start.26 = (bf16[2,3,64,1408]{3,2,1,0:T(8,128)(2,1)}, bf16[2,3,64,1408]{3,2,1,0:T(8,128)(2,1)S(1)}, u32[]{:S(2)}, u32[]{:S(2)}) collective-permute-start(bf16[2,3,64,1408]{3,2,1,0:T(8,128)(2,1)} %get-tuple-element.39.refs_1_), channel_id=1, source_target_pairs={{0,4},{4,0},{1,5},{5,1},{2,6},{6,2},{3,7},{7,3},{8,12},{12,8},{9,1... | collective-permute-start | bytes 3244040 | tf_op jit(solution)/shard_map/ppermute | solution.py:60
  94.5 7.0 %collective-permute-done.10.r1 = bf16[256,256]{1,0:T(8,128)(2,1)S(1)} collective-permute-done((bf16[256,256]{1,0:T(8,128)(2,1)}, bf16[256,256]{1,0:T(8,128)(2,1)S(1)}, u32[]{:S(2)}, u32[]{:S(2)}) %collective-permute-start.10) | collective-permute-done | bytes 131104 | tf_op jit(solution)/shard_map/ppermute | solution.py:508
  101.9 5.2 %collective-permute-done.11.r2 = bf16[256,256]{1,0:T(8,128)(2,1)S(1)} collective-permute-done((bf16[256,256]{1,0:T(8,128)(2,1)}, bf16[256,256]{1,0:T(8,128)(2,1)S(1)}, u32[]{:S(2)}, u32[]{:S(2)}) %collective-permute-start.11) | collective-permute-done | bytes 131104 | tf_op jit(solution)/shard_map/ppermute | solution.py:508
  107.2 4.7 %collective-permute-done.12.r3 = bf16[256,256]{1,0:T(8,128)(2,1)S(1)} collective-permute-done((bf16[256,256]{1,0:T(8,128)(2,1)S(1)}, bf16[256,256]{1,0:T(8,128)(2,1)S(1)}, u32[]{:S(2)}, u32[]{:S(2)}) %collective-permute-start.12) | collective-permute-done | bytes 131104 | tf_op jit(solution)/shard_map/ppermute | solution.py:508
  111.8 2.7 %collective-permute-start.24 = (bf16[2,3,64,1408]{3,2,1,0:T(8,128)(2,1)S(1)}, bf16[2,3,64,1408]{3,2,1,0:T(8,128)(2,1)S(1)}, u32[]{:S(2)}, u32[]{:S(2)}) collective-permute-start(bf16[2,3,64,1408]{3,2,1,0:T(8,128)(2,1)S(1)} %copy-done.4), channel_id=1, source_target_pairs={{0,96},{4,28},{8,104},{12,4},{16,112},{20,12},{24,120},{28,20},{32... | collective-permute-start | bytes 3244040 | tf_op jit(solution)/shard_map/ppermute | solution.py:58
  114.5 6.7 %collective-permute-start.14 = (bf16[256,2048]{1,0:T(8,128)(2,1)S(1)}, bf16[256,2048]{1,0:T(8,128)(2,1)S(1)}, u32[]{:S(2)}, u32[]{:S(2)}) collective-permute-start(bf16[256,2048]{1,0:T(8,128)(2,1)S(1)} %collective-permute-done.13.near), channel_id=1, source_target_pairs={{0,4},{4,0},{1,5},{5,1},{2,6},{6,2},{3,7},{7,3},{8,12},{12,8},{9,1... | collective-permute-start | bytes 3145736 | tf_op jit(solution)/shard_map/ppermute | solution.py:466
  121.7 5.6 %collective-permute-done.17.refs_2_ = bf16[2,3,64,1408]{3,2,1,0:T(8,128)(2,1)S(1)} collective-permute-done((bf16[2,3,64,1408]{3,2,1,0:T(8,128)(2,1)S(1)}, bf16[2,3,64,1408]{3,2,1,0:T(8,128)(2,1)S(1)}, u32[]{:S(2)}, u32[]{:S(2)}) %collective-permute-start.17) | collective-permute-done | bytes 1081376 | tf_op jit(solution)/shard_map/ppermute | solution.py:53
  127.3 6.9 %collective-permute-start.28 = (bf16[2,3,64,1408]{3,2,1,0:T(8,128)(2,1)S(1)}, bf16[2,3,64,1408]{3,2,1,0:T(8,128)(2,1)S(1)}, u32[]{:S(2)}, u32[]{:S(2)}) collective-permute-start(bf16[2,3,64,1408]{3,2,1,0:T(8,128)(2,1)S(1)} %collective-permute-done.19.refs_3_), channel_id=1, source_target_pairs={{0,4},{4,0},{1,5},{5,1},{2,6},{6,2},{3,7},{7,3},{8,12},{12,8},{9,1... | collective-permute-start | bytes 3244040 | tf_op jit(solution)/shard_map/ppermute | solution.py:60
  137.0 2.6 %shard_map.141 = (bf16[256,2048]{1,0:T(8,128)(2,1)S(1)}, bf16[128,2048]{1,0:T(8,128)(2,1)S(1)}, bf16[128,2048]{1,0:T(8,128)(2,1)S(1)}) custom-call(s32[4]{0:T(128)S(1)} %pad_add_fusion.coord, bf16[256,256]{1,0:T(8,128)(2,1)S(1)} %get-tuple-element.32.r0, bf16[256,256]{1,0:T(8,128)(2,1)S(1)} %collective-permute-done.10.r1, ...), custom_call_target="tpu_custom_call" | custom-call | tf_op jit(solution)/shard_map/pallas_call | solution.py:309
  142.4 11.4 %collective-permute-done.33.refs_0_ = bf16[128,2048]{1,0:T(8,128)(2,1)S(1)} collective-permute-done((bf16[128,2048]{1,0:T(8,128)(2,1)S(1)}, bf16[128,2048]{1,0:T(8,128)(2,1)S(1)}, u32[]{:S(2)}, u32[]{:S(2)}) %collective-permute-start.33) | collective-permute-done | bytes 524320 | tf_op jit(solution)/shard_map/ppermute | solution.py:518
  160.9 3.8 %shard_map.142.refs_4_ = bf16[3,16,2,64,1408]{4,3,2,1,0:T(8,128)(2,1)S(1)} custom-call(s32[4]{0:T(128)S(1)} %pad_add_fusion.coord, bf16[2,3,64,1408]{3,2,1,0:T(8,128)(2,1)S(1)} %copy-done.4, bf16[2,3,64,1408]{3,2,1,0:T(8,128)(2,1)} %get-tuple-element.39.refs_1_, bf16[2,3,64,1408]{3,2,1,0:T(8,128)(2,1)S(1)} %collective-permute-done.17.refs_2_, ...), custom_call_target="tpu_custom_call" | custom-call | tf_op jit(solution)/shard_map/pallas_call | solution.py:107
  164.7 2.7 %collective-permute-start.32 = (bf16[128,2048]{1,0:T(8,128)(2,1)S(1)}, bf16[128,2048]{1,0:T(8,128)(2,1)S(1)}, u32[]{:S(2)}, u32[]{:S(2)}) collective-permute-start(bf16[128,2048]{1,0:T(8,128)(2,1)S(1)} %get-tuple-element.36.refs_0_), channel_id=1, source_target_pairs={{0,3},{1,0},{2,1},{3,2},{4,7},{5,4},{6,5},{7,6},{8,11},{9,8},{10,9... | collective-permute-start | bytes 1572872 | tf_op jit(solution)/shard_map/ppermute | solution.py:523
  169.1 3.0 %collective-permute-done.34.refs_0_ = bf16[128,2048]{1,0:T(8,128)(2,1)S(1)} collective-permute-done((bf16[128,2048]{1,0:T(8,128)(2,1)S(1)}, bf16[128,2048]{1,0:T(8,128)(2,1)S(1)}, u32[]{:S(2)}, u32[]{:S(2)}) %collective-permute-start.34) | collective-permute-done | bytes 524320 | tf_op jit(solution)/shard_map/ppermute | solution.py:520
  172.5 6.2 %ffn_rows.6 = (bf16[128,2048]{1,0:T(8,128)(2,1)S(1)}, bf16[128,2048]{1,0:T(8,128)(2,1)S(1)}) custom-call(bf16[128,2048]{1,0:T(8,128)(2,1)S(1)} %collective-permute-done.34.refs_0_, bf16[128,2048]{1,0:T(8,128)(2,1)S(1)} %collective-permute-done.36.refs_1_, bf16[3,16,2,64,1408]{4,3,2,1,0:T(8,128)(2,1)S(1)} %shard_map.143.refs_2_), custom_call_target="tpu_custom_call" | custom-call | tf_op jit(solution)/shard_map/ffn_rows/pallas_call | solution.py:163
  178.6 2.1 collective-permute-start.39
  180.8 6.2 %ffn_rows.7 = (bf16[128,2048]{1,0:T(8,128)(2,1)S(1)}, bf16[128,2048]{1,0:T(8,128)(2,1)S(1)}) custom-call(bf16[128,2048]{1,0:T(8,128)(2,1)S(1)} %collective-permute-done.33.refs_0_, bf16[128,2048]{1,0:T(8,128)(2,1)S(1)} %collective-permute-done.35.refs_1_, bf16[3,16,2,64,1408]{4,3,2,1,0:T(8,128)(2,1)S(1)} %shard_map.143.refs_2_), custom_call_target="tpu_custom_call" | custom-call | tf_op jit(solution)/shard_map/ffn_rows/pallas_call | solution.py:163
  186.9 2.7 %collective-permute-start.41 = (bf16[128,2048]{1,0:T(8,128)(2,1)S(1)}, bf16[128,2048]{1,0:T(8,128)(2,1)S(1)}, u32[]{:S(2)}, u32[]{:S(2)}) collective-permute-start(bf16[128,2048]{1,0:T(8,128)(2,1)S(1)} %get-tuple-element.46), channel_id=1, source_target_pairs={{0,3},{1,0},{2,1},{3,2},{4,7},{5,4},{6,5},{7,6},{8,11},{9,8},{10,9... | collective-permute-start | bytes 1572872 | tf_op jit(solution)/shard_map/ppermute | solution.py:536
  189.7 6.2 %ffn_rows.5 = (bf16[128,2048]{1,0:T(8,128)(2,1)S(1)}, bf16[128,2048]{1,0:T(8,128)(2,1)S(1)}) custom-call(bf16[128,2048]{1,0:T(8,128)(2,1)S(1)} %collective-permute-done.31.refs_0_, bf16[128,2048]{1,0:T(8,128)(2,1)S(1)} %collective-permute-done.32.refs_1_, bf16[3,16,2,64,1408]{4,3,2,1,0:T(8,128)(2,1)S(1)} %shard_map.143.refs_2_), custom_call_target="tpu_custom_call" | custom-call | tf_op jit(solution)/shard_map/ffn_rows/pallas_call | solution.py:163
  196.0 2.7 %collective-permute-start.40 = (bf16[128,2048]{1,0:T(8,128)(2,1)S(1)}, bf16[128,2048]{1,0:T(8,128)(2,1)S(1)}, u32[]{:S(2)}, u32[]{:S(2)}) collective-permute-start(bf16[128,2048]{1,0:T(8,128)(2,1)S(1)} %add_convert_fusion), channel_id=1, source_target_pairs={{0,3},{1,0},{2,1},{3,2},{4,7},{5,4},{6,5},{7,6},{8,11},{9,8},{10,9... | collective-permute-start | bytes 1572872 | tf_op jit(solution)/shard_map/ppermute | solution.py:541
  199.0 6.2 %ffn_rows.4 = (bf16[128,2048]{1,0:T(8,128)(2,1)S(1)}, bf16[128,2048]{1,0:T(8,128)(2,1)S(1)}) custom-call(bf16[128,2048]{1,0:T(8,128)(2,1)S(1)} %get-tuple-element.36.refs_0_, bf16[128,2048]{1,0:T(8,128)(2,1)S(1)} %get-tuple-element.37.refs_1_, bf16[3,16,2,64,1408]{4,3,2,1,0:T(8,128)(2,1)S(1)} %shard_map.143.refs_2_), custom_call_target="tpu_custom_call" | custom-call | tf_op jit(solution)/shard_map/ffn_rows/pallas_call | solution.py:163
  206.2 11.2 %collective-permute-done.40.sum_b = bf16[128,2048]{1,0:T(8,128)(2,1)S(1)} collective-permute-done((bf16[128,2048]{1,0:T(8,128)(2,1)S(1)}, bf16[128,2048]{1,0:T(8,128)(2,1)S(1)}, u32[]{:S(2)}, u32[]{:S(2)}) %collective-permute-start.40) | collective-permute-done | bytes 524320 | tf_op jit(solution)/shard_map/ppermute | solution.py:541
  (102 shorter events, 33.1 us)
Async XLA Ops:
  0.0 92.9 %collective-permute-start.13 = (bf16[256,2048]{1,0:T(8,128)(2,1)}, bf16[256,2048]{1,0:T(8,128)(2,1)S(1)}, u32[]{:S(2)}, u32[]{:S(2)}) collective-permute-start(bf16[256,2048]{1,0:T(8,128)(2,1)} %own.1), channel_id=1, source_target_pairs={{0,1},{1,2},{2,3},{3,0},{4,7},{5,4},{6,5},{7,6},{8,9},{9,10},{10,1... | collective-permute-start | bytes 3145736 | tf_op jit(solution)/shard_map/ppermute | solution.py:463
  4.6 35.6 %collective-permute-start = (bf16[3,64,1408]{2,1,0:T(8,128)(2,1)S(1)}, bf16[3,64,1408]{2,1,0:T(8,128)(2,1)}, u32[]{:S(2)}, u32[]{:S(2)}) collective-permute-start(bf16[3,64,1408]{2,1,0:T(8,128)(2,1)S(1)} %pad_maximum_fusion.near), channel_id=1, source_target_pairs={{0,8},{4,36},{8,16},{12,44},{16,24},{20,52},{24,0},{28,60},{32,40}... | collective-permute-start | bytes 1622024 | tf_op jit(solution)/shard_map/ppermute | solution.py:45
  6.3 44.0 %collective-permute-start.8 = (bf16[3,64,1408]{2,1,0:T(8,128)(2,1)S(1)}, bf16[3,64,1408]{2,1,0:T(8,128)(2,1)}, u32[]{:S(2)}, u32[]{:S(2)}) collective-permute-start(bf16[3,64,1408]{2,1,0:T(8,128)(2,1)S(1)} %pad_maximum_fusion.near), channel_id=1, source_target_pairs={{0,24},{4,100},{8,0},{12,108},{16,8},{20,116},{24,16},{28,124},{32... | collective-permute-start | bytes 1622024 | tf_op jit(solution)/shard_map/ppermute | solution.py:46
  8.5 41.8 %collective-permute-start.9 = (bf16[3,64,1408]{2,1,0:T(8,128)(2,1)S(1)}, bf16[3,64,1408]{2,1,0:T(8,128)(2,1)}, u32[]{:S(2)}, u32[]{:S(2)}) collective-permute-start(bf16[3,64,1408]{2,1,0:T(8,128)(2,1)S(1)} %pad_maximum_fusion.near), channel_id=1, source_target_pairs={{0,16},{4,68},{8,24},{12,76},{16,0},{20,84},{24,8},{28,92},{32,48}... | collective-permute-start | bytes 1622024 | tf_op jit(solution)/shard_map/ppermute | solution.py:47
  13.4 9.6 %collective-permute-start.2 = (bf16[2,144,128]{2,1,0:T(8,128)(2,1)S(1)}, bf16[2,144,128]{2,1,0:T(8,128)(2,1)S(1)}, u32[]{:S(2)}, u32[]{:S(2)}) collective-permute-start(bf16[2,144,128]{2,1,0:T(8,128)(2,1)S(1)} %get-tuple-element.28.own), channel_id=1, source_target_pairs={{0,8},{8,16},{16,24},{24,0},{1,9},{9,17},{17,25},{25,1},{2,10},{10... | collective-permute-start | bytes 221192 | tf_op jit(solution)/shard_map/ppermute | solution.py:491
  38.9 11.4 %collective-permute-start.6 = (bf16[2,144,128]{2,1,0:T(8,128)(2,1)S(1)}, bf16[2,144,128]{2,1,0:T(8,128)(2,1)S(1)}, u32[]{:S(2)}, u32[]{:S(2)}) collective-permute-start(bf16[2,144,128]{2,1,0:T(8,128)(2,1)S(1)} %get-tuple-element.31), channel_id=1, source_target_pairs={{0,64},{32,96},{1,65},{33,97},{2,66},{34,98},{3,67},{35,99},{4,68}... | collective-permute-start | bytes 221192 | tf_op jit(solution)/shard_map/ppermute | solution.py:495
  40.2 10.1 %collective-permute-start.7 = (bf16[2,144,128]{2,1,0:T(8,128)(2,1)S(1)}, bf16[2,144,128]{2,1,0:T(8,128)(2,1)S(1)}, u32[]{:S(2)}, u32[]{:S(2)}) collective-permute-start(bf16[2,144,128]{2,1,0:T(8,128)(2,1)S(1)} %get-tuple-element.31), channel_id=1, source_target_pairs={{0,32},{32,64},{64,96},{1,33},{33,65},{65,97},{2,34},{34,66},{66,9... | collective-permute-start | bytes 221192 | tf_op jit(solution)/shard_map/ppermute | solution.py:495
  86.1 28.4 %collective-permute-start.19 = (bf16[2,3,64,1408]{3,2,1,0:T(8,128)(2,1)}, bf16[2,3,64,1408]{3,2,1,0:T(8,128)(2,1)S(1)}, u32[]{:S(2)}, u32[]{:S(2)}) collective-permute-start(bf16[2,3,64,1408]{3,2,1,0:T(8,128)(2,1)} %get-tuple-element.39.refs_1_), channel_id=1, source_target_pairs={{0,96},{4,28},{8,104},{12,4},{16,112},{20,12},{24,120},{28,20},{32... | collective-permute-start | bytes 3244040 | tf_op jit(solution)/shard_map/ppermute | solution.py:54
  87.3 33.9 %collective-permute-start.23 = (bf16[2,3,64,1408]{3,2,1,0:T(8,128)(2,1)}, bf16[2,3,64,1408]{3,2,1,0:T(8,128)(2,1)}, u32[]{:S(2)}, u32[]{:S(2)}) collective-permute-start(bf16[2,3,64,1408]{3,2,1,0:T(8,128)(2,1)} %get-tuple-element.39.refs_1_), channel_id=1, source_target_pairs={{0,32},{4,12},{8,40},{12,20},{16,48},{20,28},{24,56},{28,4},{32,64... | collective-permute-start | bytes 3244040 | tf_op jit(solution)/shard_map/ppermute | solution.py:57
  87.6 33.9 %collective-permute-start.26 = (bf16[2,3,64,1408]{3,2,1,0:T(8,128)(2,1)}, bf16[2,3,64,1408]{3,2,1,0:T(8,128)(2,1)S(1)}, u32[]{:S(2)}, u32[]{:S(2)}) collective-permute-start(bf16[2,3,64,1408]{3,2,1,0:T(8,128)(2,1)} %get-tuple-element.39.refs_1_), channel_id=1, source_target_pairs={{0,4},{4,0},{1,5},{5,1},{2,6},{6,2},{3,7},{7,3},{8,12},{12,8},{9,1... | collective-permute-start | bytes 3244040 | tf_op jit(solution)/shard_map/ppermute | solution.py:60
  93.0 18.8 %collective-permute-start.15 = (bf16[128,2048]{1,0:T(8,128)(2,1)S(1)}, bf16[128,2048]{1,0:T(8,128)(2,1)S(1)}, u32[]{:S(2)}, u32[]{:S(2)}) collective-permute-start(bf16[128,2048]{1,0:T(8,128)(2,1)S(1)} %constant_dynamic-slice_fusion), channel_id=1, source_target_pairs={{0,1},{1,2},{2,3},{3,0},{4,7},{5,4},{6,5},{7,6},{8,9},{9,10},{10,1... | collective-permute-start | bytes 1572872 | tf_op jit(solution)/shard_map/ppermute | solution.py:465
  111.8 15.5 %collective-permute-start.17 = (bf16[2,3,64,1408]{3,2,1,0:T(8,128)(2,1)S(1)}, bf16[2,3,64,1408]{3,2,1,0:T(8,128)(2,1)S(1)}, u32[]{:S(2)}, u32[]{:S(2)}) collective-permute-start(bf16[2,3,64,1408]{3,2,1,0:T(8,128)(2,1)S(1)} %copy-done.4), channel_id=1, source_target_pairs={{0,32},{4,12},{8,40},{12,20},{16,48},{20,28},{24,56},{28,4},{32,64... | collective-permute-start | bytes 3244040 | tf_op jit(solution)/shard_map/ppermute | solution.py:53
  111.8 27.8 %collective-permute-start.24 = (bf16[2,3,64,1408]{3,2,1,0:T(8,128)(2,1)S(1)}, bf16[2,3,64,1408]{3,2,1,0:T(8,128)(2,1)S(1)}, u32[]{:S(2)}, u32[]{:S(2)}) collective-permute-start(bf16[2,3,64,1408]{3,2,1,0:T(8,128)(2,1)S(1)} %copy-done.4), channel_id=1, source_target_pairs={{0,96},{4,28},{8,104},{12,4},{16,112},{20,12},{24,120},{28,20},{32... | collective-permute-start | bytes 3244040 | tf_op jit(solution)/shard_map/ppermute | solution.py:58
  114.5 21.0 %collective-permute-start.14 = (bf16[256,2048]{1,0:T(8,128)(2,1)S(1)}, bf16[256,2048]{1,0:T(8,128)(2,1)S(1)}, u32[]{:S(2)}, u32[]{:S(2)}) collective-permute-start(bf16[256,2048]{1,0:T(8,128)(2,1)S(1)} %collective-permute-done.13.near), channel_id=1, source_target_pairs={{0,4},{4,0},{1,5},{5,1},{2,6},{6,2},{3,7},{7,3},{8,12},{12,8},{9,1... | collective-permute-start | bytes 3145736 | tf_op jit(solution)/shard_map/ppermute | solution.py:466
  121.2 19.8 %collective-permute-start.25 = (bf16[2,3,64,1408]{3,2,1,0:T(8,128)(2,1)S(1)}, bf16[2,3,64,1408]{3,2,1,0:T(8,128)(2,1)S(1)}, u32[]{:S(2)}, u32[]{:S(2)}) collective-permute-start(bf16[2,3,64,1408]{3,2,1,0:T(8,128)(2,1)S(1)} %copy-done.4), channel_id=1, source_target_pairs={{0,4},{4,0},{1,5},{5,1},{2,6},{6,2},{3,7},{7,3},{8,12},{12,8},{9,1... | collective-permute-start | bytes 3244040 | tf_op jit(solution)/shard_map/ppermute | solution.py:60
  121.5 12.8 %collective-permute-start.16 = (bf16[128,2048]{1,0:T(8,128)(2,1)S(1)}, bf16[128,2048]{1,0:T(8,128)(2,1)S(1)}, u32[]{:S(2)}, u32[]{:S(2)}) collective-permute-start(bf16[128,2048]{1,0:T(8,128)(2,1)S(1)} %collective-permute-done.15.far), channel_id=1, source_target_pairs={{0,4},{4,0},{1,5},{5,1},{2,6},{6,2},{3,7},{7,3},{8,12},{12,8},{9,1... | collective-permute-start | bytes 1572872 | tf_op jit(solution)/shard_map/ppermute | solution.py:467
  127.3 28.0 %collective-permute-start.28 = (bf16[2,3,64,1408]{3,2,1,0:T(8,128)(2,1)S(1)}, bf16[2,3,64,1408]{3,2,1,0:T(8,128)(2,1)S(1)}, u32[]{:S(2)}, u32[]{:S(2)}) collective-permute-start(bf16[2,3,64,1408]{3,2,1,0:T(8,128)(2,1)S(1)} %collective-permute-done.19.refs_3_), channel_id=1, source_target_pairs={{0,4},{4,0},{1,5},{5,1},{2,6},{6,2},{3,7},{7,3},{8,12},{12,8},{9,1... | collective-permute-start | bytes 3244040 | tf_op jit(solution)/shard_map/ppermute | solution.py:60
  134.3 21.5 %collective-permute-start.20 = (bf16[2,3,64,1408]{3,2,1,0:T(8,128)(2,1)S(1)}, bf16[2,3,64,1408]{3,2,1,0:T(8,128)(2,1)S(1)}, u32[]{:S(2)}, u32[]{:S(2)}) collective-permute-start(bf16[2,3,64,1408]{3,2,1,0:T(8,128)(2,1)S(1)} %collective-permute-done.19.refs_3_), channel_id=1, source_target_pairs={{0,96},{4,28},{8,104},{12,4},{16,112},{20,12},{24,120},{28,20},{32... | collective-permute-start | bytes 3244040 | tf_op jit(solution)/shard_map/ppermute | solution.py:56
  135.5 20.4 %collective-permute-start.18 = (bf16[2,3,64,1408]{3,2,1,0:T(8,128)(2,1)S(1)}, bf16[2,3,64,1408]{3,2,1,0:T(8,128)(2,1)S(1)}, u32[]{:S(2)}, u32[]{:S(2)}) collective-permute-start(bf16[2,3,64,1408]{3,2,1,0:T(8,128)(2,1)S(1)} %collective-permute-done.17.refs_2_), channel_id=1, source_target_pairs={{0,32},{4,12},{8,40},{12,20},{16,48},{20,28},{24,56},{28,4},{32,64... | collective-permute-start | bytes 3244040 | tf_op jit(solution)/shard_map/ppermute | solution.py:55
  139.7 14.2 %collective-permute-start.33 = (bf16[128,2048]{1,0:T(8,128)(2,1)S(1)}, bf16[128,2048]{1,0:T(8,128)(2,1)S(1)}, u32[]{:S(2)}, u32[]{:S(2)}) collective-permute-start(bf16[128,2048]{1,0:T(8,128)(2,1)S(1)} %get-tuple-element.36.refs_0_), channel_id=1, source_target_pairs={{0,1},{1,2},{2,3},{3,0},{4,5},{5,6},{6,7},{7,4},{8,9},{9,10},{10,1... | collective-permute-start | bytes 1572872 | tf_op jit(solution)/shard_map/ppermute | solution.py:518
  141.0 14.3 %collective-permute-start.35 = (bf16[128,2048]{1,0:T(8,128)(2,1)S(1)}, bf16[128,2048]{1,0:T(8,128)(2,1)S(1)}, u32[]{:S(2)}, u32[]{:S(2)}) collective-permute-start(bf16[128,2048]{1,0:T(8,128)(2,1)S(1)} %get-tuple-element.37.refs_1_), channel_id=1, source_target_pairs={{0,3},{1,0},{2,1},{3,2},{4,7},{5,4},{6,5},{7,6},{8,11},{9,8},{10,9... | collective-permute-start | bytes 1572872 | tf_op jit(solution)/shard_map/ppermute | solution.py:519
  155.9 11.5 %collective-permute-start.21 = (bf16[2,3,64,1408]{3,2,1,0:T(8,128)(2,1)S(1)}, bf16[2,3,64,1408]{3,2,1,0:T(8,128)(2,1)S(1)}, u32[]{:S(2)}, u32[]{:S(2)}) collective-permute-start(bf16[2,3,64,1408]{3,2,1,0:T(8,128)(2,1)S(1)} %collective-permute-done.18.refs_0_), channel_id=1, source_target_pairs={{0,4},{4,0},{1,5},{5,1},{2,6},{6,2},{3,7},{7,3},{8,12},{12,8},{9,1... | collective-permute-start | bytes 3244040 | tf_op jit(solution)/shard_map/ppermute | solution.py:60
  157.8 14.3 %collective-permute-start.34 = (bf16[128,2048]{1,0:T(8,128)(2,1)S(1)}, bf16[128,2048]{1,0:T(8,128)(2,1)S(1)}, u32[]{:S(2)}, u32[]{:S(2)}) collective-permute-start(bf16[128,2048]{1,0:T(8,128)(2,1)S(1)} %collective-permute-done.33.refs_0_), channel_id=1, source_target_pairs={{0,1},{1,2},{2,3},{3,0},{4,5},{5,6},{6,7},{7,4},{8,9},{9,10},{10,1... | collective-permute-start | bytes 1572872 | tf_op jit(solution)/shard_map/ppermute | solution.py:520
  159.4 13.1 %collective-permute-start.36 = (bf16[128,2048]{1,0:T(8,128)(2,1)S(1)}, bf16[128,2048]{1,0:T(8,128)(2,1)S(1)}, u32[]{:S(2)}, u32[]{:S(2)}) collective-permute-start(bf16[128,2048]{1,0:T(8,128)(2,1)S(1)} %collective-permute-done.35.refs_1_), channel_id=1, source_target_pairs={{0,3},{1,0},{2,1},{3,2},{4,7},{5,4},{6,5},{7,6},{8,11},{9,8},{10,9... | collective-permute-start | bytes 1572872 | tf_op jit(solution)/shard_map/ppermute | solution.py:521
  160.9 28.8 %collective-permute-start.31 = (bf16[128,2048]{1,0:T(8,128)(2,1)S(1)}, bf16[128,2048]{1,0:T(8,128)(2,1)S(1)}, u32[]{:S(2)}, u32[]{:S(2)}) collective-permute-start(bf16[128,2048]{1,0:T(8,128)(2,1)S(1)} %get-tuple-element.37.refs_1_), channel_id=1, source_target_pairs={{0,1},{1,2},{2,3},{3,0},{4,5},{5,6},{6,7},{7,4},{8,9},{9,10},{10,1... | collective-permute-start | bytes 1572872 | tf_op jit(solution)/shard_map/ppermute | solution.py:522
  164.7 25.0 %collective-permute-start.32 = (bf16[128,2048]{1,0:T(8,128)(2,1)S(1)}, bf16[128,2048]{1,0:T(8,128)(2,1)S(1)}, u32[]{:S(2)}, u32[]{:S(2)}) collective-permute-start(bf16[128,2048]{1,0:T(8,128)(2,1)S(1)} %get-tuple-element.36.refs_0_), channel_id=1, source_target_pairs={{0,3},{1,0},{2,1},{3,2},{4,7},{5,4},{6,5},{7,6},{8,11},{9,8},{10,9... | collective-permute-start | bytes 1572872 | tf_op jit(solution)/shard_map/ppermute | solution.py:523
  178.6 17.2 %collective-permute-start.39 = (bf16[128,2048]{1,0:T(8,128)(2,1)S(1)}, bf16[128,2048]{1,0:T(8,128)(2,1)S(1)}, u32[]{:S(2)}, u32[]{:S(2)}) collective-permute-start(bf16[128,2048]{1,0:T(8,128)(2,1)S(1)} %get-tuple-element.45), channel_id=1, source_target_pairs={{0,3},{1,0},{2,1},{3,2},{4,7},{5,4},{6,5},{7,6},{8,11},{9,8},{10,9... | collective-permute-start | bytes 1572872 | tf_op jit(solution)/shard_map/ppermute | solution.py:538
  180.8 18.0 %collective-permute-start.37 = (bf16[128,2048]{1,0:T(8,128)(2,1)S(1)}, bf16[128,2048]{1,0:T(8,128)(2,1)S(1)}, u32[]{:S(2)}, u32[]{:S(2)}) collective-permute-start(bf16[128,2048]{1,0:T(8,128)(2,1)S(1)} %get-tuple-element.43), channel_id=1, source_target_pairs={{0,1},{1,2},{2,3},{3,0},{4,5},{5,6},{6,7},{7,4},{8,9},{9,10},{10,1... | collective-permute-start | bytes 1572872 | tf_op jit(solution)/shard_map/ppermute | solution.py:537
  186.9 19.2 %collective-permute-start.41 = (bf16[128,2048]{1,0:T(8,128)(2,1)S(1)}, bf16[128,2048]{1,0:T(8,128)(2,1)S(1)}, u32[]{:S(2)}, u32[]{:S(2)}) collective-permute-start(bf16[128,2048]{1,0:T(8,128)(2,1)S(1)} %get-tuple-element.46), channel_id=1, source_target_pairs={{0,3},{1,0},{2,1},{3,2},{4,7},{5,4},{6,5},{7,6},{8,11},{9,8},{10,9... | collective-permute-start | bytes 1572872 | tf_op jit(solution)/shard_map/ppermute | solution.py:536
  189.7 16.5 %collective-permute-start.42 = (bf16[128,2048]{1,0:T(8,128)(2,1)S(1)}, bf16[128,2048]{1,0:T(8,128)(2,1)S(1)}, u32[]{:S(2)}, u32[]{:S(2)}) collective-permute-start(bf16[128,2048]{1,0:T(8,128)(2,1)S(1)} %get-tuple-element.47), channel_id=1, source_target_pairs={{0,1},{1,2},{2,3},{3,0},{4,5},{5,6},{6,7},{7,4},{8,9},{9,10},{10,1... | collective-permute-start | bytes 1572872 | tf_op jit(solution)/shard_map/ppermute | solution.py:535
  196.0 21.4 %collective-permute-start.40 = (bf16[128,2048]{1,0:T(8,128)(2,1)S(1)}, bf16[128,2048]{1,0:T(8,128)(2,1)S(1)}, u32[]{:S(2)}, u32[]{:S(2)}) collective-permute-start(bf16[128,2048]{1,0:T(8,128)(2,1)S(1)} %add_convert_fusion), channel_id=1, source_target_pairs={{0,3},{1,0},{2,1},{3,2},{4,7},{5,4},{6,5},{7,6},{8,11},{9,8},{10,9... | collective-permute-start | bytes 1572872 | tf_op jit(solution)/shard_map/ppermute | solution.py:541
  198.9 18.5 %collective-permute-start.38 = (bf16[128,2048]{1,0:T(8,128)(2,1)S(1)}, bf16[128,2048]{1,0:T(8,128)(2,1)S(1)}, u32[]{:S(2)}, u32[]{:S(2)}) collective-permute-start(bf16[128,2048]{1,0:T(8,128)(2,1)S(1)} %add_convert_fusion.1), channel_id=1, source_target_pairs={{0,1},{1,2},{2,3},{3,0},{4,5},{5,6},{6,7},{7,4},{8,9},{9,10},{10,1... | collective-permute-start | bytes 1572872 | tf_op jit(solution)/shard_map/ppermute | solution.py:540
  (26 other events, 467.1 us)
